TPU v7x, 32 devices: a whole 2x2x4 slice. The times are simulated.
32 devices in a mesh: sp: 8 (over z, x), tp: 4 (over y, core).
Axes of the slice: x: 2, y: 2, z: 4, core: 2. Of those that a mesh axis runs over, the one named last changes fastest.
Arguments:
- tokens: bfloat16 [3072, 2048], P('sp'), may hold values from -6 to 6
- doc_ids: int32 [3072], P('sp'), may hold values from 0 to 2, never falling along the last dimension, each value on 1 to 2048 neighbouring positions
- pre_gain: float32 [2, 2048], replicated, may hold values from 0.1 to 1.9
- value_proj: bfloat16 [2, 2048, 1024], P(None, 'sp', 'tp'), may hold values from -0.1875 to 0.1875
- gate_proj: bfloat16 [2, 2048, 1024], P(None, 'sp', 'tp'), may hold values from -0.1875 to 0.1875
- out_proj: bfloat16 [2, 1024, 2048], P(None, 'tp', 'sp'), may hold values from -0.1875 to 0.1875
- conv_taps: float32 [2, 31, 1024], P(None, None, 'tp'), may hold values from -2.2 to 2.2
- norm_gain: float32 [2, 1024], P(None, 'tp'), may hold values from 0.1 to 1.9
- norm_shift: float32 [2, 1024], P(None, 'tp'), may hold values from -3 to 3
Outputs:
- hidden: bfloat16 [3072, 2048], P('sp')
Inputs may be any that keep to these rules, and one draw needn't show every extreme that they name: `doc_ids`: document numbers never fall along the sequence; each document has 1 to 2048 positions.
All inputs are finite; a program needn't handle non-finite values.
Results may differ from a plain program's by a relative error of at most 0.017.
Values may be sent and summed in bfloat16 or wider, within the bound.
No kernel may reach another device: no remote copies, remote signals or barrier semaphores. Data moves between devices by JAX's collectives and lax.ppermute only.
A program may use at most 64 MiB of HBM per device.

v0:
```python
import functools

import jax
import jax.numpy as jnp
from jax import lax
from jax.experimental import pallas as pl
from jax.experimental.pallas import tpu as pltpu
from jax.sharding import PartitionSpec as P


epsilon = 1e-06
LANES = 128
SUBLANES = 8
HALO_ALIGN = 16
CONV_ROWS = 32
RING_MOST = 8
KERNEL_VMEM = 20 * 2**20


wide = jnp.float32
narrow = jnp.bfloat16


def round_up(value, step):
    return -(-value // step) * step


def in_vmem():
    return pl.BlockSpec(memory_space=pltpu.VMEM)


def in_smem():
    return pl.BlockSpec(memory_space=pltpu.SMEM)


def kernel(body, out_shape, in_specs, scratch_shapes=()):
    return pl.pallas_call(
        body,
        out_shape=out_shape,
        in_specs=in_specs,
        out_specs=jax.tree.map(lambda _: in_vmem(), out_shape),
        scratch_shapes=list(scratch_shapes),
        compiler_params=pltpu.CompilerParams(vmem_limit_bytes=KERNEL_VMEM),
    )


def normed_of(state, gain):
    scale = lax.rsqrt(jnp.mean(state * state, axis=-1, keepdims=True) + epsilon)
    return (state * scale * gain).astype(narrow)


def pack_body(value_ref, gate_ref, out_ref, pair_ref, part_ref):
    pair_ref[0] = value_ref[...]
    pair_ref[1] = gate_ref[...]
    part_ref[...] = out_ref[...]


def packed(layer, value_proj, gate_proj, out_proj):
    arrays = (value_proj, gate_proj, out_proj)
    return pl.pallas_call(
        pack_body,
        grid=(1,),
        out_shape=(
            jax.ShapeDtypeStruct((2,) + value_proj.shape[1:], narrow),
            jax.ShapeDtypeStruct(out_proj.shape[1:], narrow),
        ),
        in_specs=[
            pl.BlockSpec((None,) + a.shape[1:], lambda i, layer=layer: (layer, 0, 0))
            for a in arrays
        ],
        out_specs=(
            pl.BlockSpec((2,) + value_proj.shape[1:], lambda i: (0, 0, 0)),
            pl.BlockSpec(out_proj.shape[1:], lambda i: (0, 0)),
        ),
        compiler_params=pltpu.CompilerParams(vmem_limit_bytes=KERNEL_VMEM),
    )(*arrays)


def norm_body(prev_ref, tokens_ref, gain_ref, normed_ref):
    halo = prev_ref.shape[0]
    gain = gain_ref[0:1, :]
    normed_ref[:halo, :] = normed_of(prev_ref[...].astype(wide), gain)
    normed_ref[halo:, :] = normed_of(tokens_ref[...].astype(wide), gain)


def gated_conv_body(layer, tap_count, tail, table_ref, normed_ref, dist_ref, taps_ref, *refs):
    *pair_refs, centred_ref, stats_ref, acc_ref, shifted_ref, conv_ref = refs
    width = taps_ref.shape[2]
    halves = width // LANES
    rows = normed_ref.shape[0]
    out_rows = centred_ref.shape[0]
    dist_from = dist_ref.shape[0] - out_rows
    depth = pair_refs[0].shape[1]
    for k, pair in enumerate(pair_refs):
        first = 0 if len(pair_refs) == 1 else pl.multiple_of(table_ref[k] * depth, LANES)
        rows_in = normed_ref[:, pl.ds(first, depth)]
        for part in range(2):
            product = jnp.dot(rows_in, pair[part], preferred_element_type=wide)
            if k == 0:
                acc_ref[part] = product
            else:
                acc_ref[part] += product
    for half in range(halves):
        cols = slice(half * LANES, (half + 1) * LANES)
        value = acc_ref[0, :, cols].astype(narrow).astype(wide)
        gate = acc_ref[1, :, cols].astype(narrow).astype(wide)
        gated = (value * jax.nn.sigmoid(gate)).astype(narrow).astype(wide)
        shifted_ref[half, 0, :, :] = gated
    for half in range(halves):
        for shift in range(1, SUBLANES):
            shifted_ref[half, shift, SUBLANES:, :] = shifted_ref[
                half, 0, SUBLANES - shift : rows - shift, :
            ]

    def block(index, carry):
        base = pl.multiple_of(index * CONV_ROWS, CONV_ROWS)
        dist = dist_ref[pl.ds(pl.multiple_of(base + dist_from, CONV_ROWS), CONV_ROWS), :]
        sums = [jnp.zeros((CONV_ROWS, LANES), wide) for _ in range(halves)]
        for tap in range(tap_count):
            inside = dist >= tap
            start = pl.multiple_of(base + (tail - tap // SUBLANES * SUBLANES), SUBLANES)
            for half in range(halves):
                rows_at = shifted_ref[half, tap % SUBLANES, pl.ds(start, CONV_ROWS), :]
                weight = taps_ref[layer, tap : tap + 1, half * LANES : (half + 1) * LANES]
                sums[half] = sums[half] + jnp.where(inside, weight * rows_at, 0.0)
        for half in range(halves):
            conv_ref[half, pl.ds(base, CONV_ROWS), :] = sums[half]
        return carry

    lax.fori_loop(0, out_rows // CONV_ROWS, block, 0)
    total = conv_ref[0]
    for half in range(1, halves):
        total = total + conv_ref[half]
    mean = jnp.sum(total, axis=1, keepdims=True) / width
    square = jnp.zeros((out_rows, LANES), wide)
    for half in range(halves):
        centred = conv_ref[half] - mean
        centred_ref[:, half * LANES : (half + 1) * LANES] = centred.astype(narrow)
        square = square + centred * centred
    square = jnp.sum(square, axis=1, keepdims=True)
    lane = lax.broadcasted_iota(jnp.int32, (out_rows, LANES), 1)
    both = jnp.where(lane == 0, mean, square)
    padded_rows = stats_ref.shape[1]
    if padded_rows != out_rows:
        both = jnp.concatenate([both, jnp.zeros((padded_rows - out_rows, LANES), wide)])
    stats_ref[...] = both.T[:2, :]


def project_body(layer, far, slots, blocks_at, table_ref, stats_ref, gain_ref, shift_ref, *refs):
    far_norm_refs, refs = refs[: far - 1], refs[far - 1 :]
    centred_refs, refs = refs[:far], refs[far:]
    *piece_refs, share_ref, act_ref = refs
    out_rows, width = centred_refs[0].shape
    tp_count = stats_ref.shape[0]
    stats = jnp.concatenate([stats_ref[j] for j in range(tp_count)])
    stats = stats.T[:out_rows, :]
    means = [stats[:, 2 * j : 2 * j + 1] for j in range(tp_count)]
    mean = functools.reduce(jnp.add, means) / tp_count
    square = sum(
        stats[:, 2 * j + 1 : 2 * j + 2] + width * (means[j] - mean) ** 2 for j in range(tp_count)
    )
    scale = lax.rsqrt(square / (width * tp_count) + epsilon)
    for f, centred in enumerate(centred_refs):
        block = table_ref[blocks_at + f]
        own = jnp.zeros_like(mean)
        for j in range(tp_count):
            own = jnp.where(block == j, means[j], own)
        if f == 0:
            gain, shift = gain_ref[layer : layer + 1, :], shift_ref[layer : layer + 1, :]
        else:
            norms = far_norm_refs[f - 1]
            gain, shift = norms[0, layer : layer + 1, :], norms[1, layer : layer + 1, :]
        normal = gain * (centred[...].astype(wide) + (own - mean)) * scale + shift
        act_ref[f] = (normal * jax.nn.sigmoid(normal)).astype(narrow)
    steps = len(slots) // far
    for k in range(steps):
        share = None
        for f in range(far):
            piece, slot = piece_refs[k * far + f], slots[k * far + f]
            matrix = piece[...] if slot is None else piece[slot]
            product = jnp.dot(act_ref[f], matrix, preferred_element_type=wide)
            share = product if share is None else share + product
        cols = share.shape[1]
        first = 0 if steps == 1 else pl.multiple_of(table_ref[k] * cols, LANES)
        share_ref[:, pl.ds(first, cols)] = share.astype(narrow)


def add_body(layer, tail, is_last, state_count, *refs):
    state_refs, refs = refs[:state_count], refs[state_count:]
    if is_last:
        *share_refs, hidden_ref = refs
    else:
        gain_ref, *share_refs, hidden_ref, normed_ref = refs
    skip, at = tail, 0
    for state_ref in state_refs:
        rows = state_ref.shape[0]
        from_row = min(skip, rows)
        skip = skip - from_row
        count = rows - from_row
        if count == 0:
            continue
        branch = share_refs[0][at : at + count, :].astype(wide)
        for share in share_refs[1:]:
            branch = branch + share[at : at + count, :].astype(wide)
        hidden = (
            state_ref[from_row:, :].astype(wide) + branch.astype(narrow).astype(wide)
        ).astype(narrow)
        hidden_ref[at : at + count, :] = hidden
        if not is_last:
            gain = gain_ref[layer + 1 : layer + 2, :]
            normed_ref[at : at + count, :] = normed_of(hidden.astype(wide), gain)
        at = at + count


def ring_tables(count):
    order = list(range(0, count, 2)) + list(range(count - 1, 0, -2))
    forward = [(order[k], order[(k + 1) % count]) for k in range(count)]
    backward = [(target, source) for source, target in forward]
    steps = [0]
    for k in range(1, count // 2 + 1):
        steps.append(-k)
        if len(steps) < count:
            steps.append(k)
    position = {device: k for k, device in enumerate(order)}
    table = [[order[(position[s] + step) % count] for step in steps] for s in range(count)]
    return forward, backward, table


def ring_gathered(value):
    count = lax.axis_size("sp")
    forward, backward, _ = ring_tables(count)
    chunks = []
    ahead = behind = value
    for _ in range(1, count // 2 + 1):
        ahead = lax.ppermute(ahead, "sp", forward)
        chunks.append(ahead)
        if len(chunks) < count - 1:
            behind = lax.ppermute(behind, "sp", backward)
            chunks.append(behind)
    return chunks


def swap_pairs(count, group, step):
    pairs = []
    for source in range(count):
        lead, at = source // (group * step), source // step % group
        pairs.append((source, (lead * group + (at + 1) % group) * step + source % step))
    return pairs


def ringed(sp_count, *widths):
    return sp_count <= RING_MOST and sp_count % 2 == 0 and not any(w % LANES for w in widths)


def tp_groups(tp_count):
    near = 2 if tp_count % 2 == 0 else 1
    return near, tp_count // near


def on_device(
    tokens, doc_ids, pre_gain, value_proj, gate_proj, out_proj, conv_taps, norm_gain, norm_shift
):
    layer_count = value_proj.shape[0]
    tap_count = conv_taps.shape[1]
    row_count, model_width = tokens.shape
    width = conv_taps.shape[2]
    sp_count, tp_count = lax.axis_size("sp"), lax.axis_size("tp")
    near, far = tp_groups(tp_count)
    far_pairs, near_pairs = swap_pairs(tp_count, far, near), swap_pairs(tp_count, near, 1)
    tail = round_up(tap_count - 1, max(HALO_ALIGN, CONV_ROWS))
    halo = tail * layer_count
    in_ring = ringed(sp_count, value_proj.shape[1], out_proj.shape[2])

    def far_values(value):
        values = [value]
        for _ in range(1, far):
            values.append(lax.ppermute(values[-1], "tp", far_pairs))
        return values

    pair_chunks, out_pieces, out_slots = [], [], []
    own_out = far_values(out_proj) if in_ring else None
    for n in range(layer_count):
        pair, part = packed(n, value_proj, gate_proj, out_proj)
        if in_ring:
            pair_chunks.append([pair] + ring_gathered(pair))
            pieces, slots = list(own_out), [n] * far
            for chunk in ring_gathered(part):
                pieces.extend(far_values(chunk))
                slots.extend([None] * far)
        else:
            pair_chunks.append([lax.all_gather(pair, "sp", axis=1, tiled=True)])
            pieces = [lax.all_gather(value, "sp", axis=1, tiled=True) for value in far_values(part)]
            slots = [None] * far
        out_pieces.append(pieces)
        out_slots.append(slots)

    onward = [(source, source + 1) for source in range(sp_count - 1)]
    prev_docs = lax.ppermute(doc_ids[row_count - halo :] + 1, "sp", onward) - 1
    prev_rows = lax.ppermute(tokens[row_count - halo :], "sp", onward)
    far_norm = far_values(jnp.stack([norm_gain, norm_shift]))[1:]
    docs = jnp.concatenate([prev_docs, doc_ids])
    dist = jnp.zeros((row_count + halo - tail,), jnp.int32)
    for offset in range(1, tap_count):
        first = tail - offset
        dist = dist + (docs[first : first + dist.shape[0]] == docs[tail:]).astype(jnp.int32)
    dist = jnp.broadcast_to(dist[:, None], (dist.shape[0], LANES))

    tp_blocks = []
    for j in range(tp_count):
        lead, at = j // (near * far), j // near % far
        tp_blocks.append([(lead * far + (at - f) % far) * near + j % near for f in range(far)])
    sp_blocks = ring_tables(sp_count)[2] if in_ring else [[0]] * sp_count
    blocks_at = len(sp_blocks[0])
    table = jnp.asarray(
        [[sp_blocks[s] + tp_blocks[j] for j in range(tp_count)] for s in range(sp_count)],
        jnp.int32,
    ).reshape(sp_count * tp_count, -1)
    table = lax.dynamic_index_in_dim(table, lax.axis_index(("sp", "tp")), keepdims=False)

    states = (prev_rows, tokens)
    normed = kernel(
        norm_body, jax.ShapeDtypeStruct((halo + row_count, model_width), narrow), [in_vmem()] * 3
    )(prev_rows, tokens, pre_gain)

    for n in range(layer_count):
        rows = normed.shape[0]
        out_rows = rows - tail
        pairs = pair_chunks[n]
        centred, stats = kernel(
            functools.partial(gated_conv_body, n, tap_count, tail),
            (
                jax.ShapeDtypeStruct((out_rows, width), narrow),
                jax.ShapeDtypeStruct((2, round_up(out_rows, LANES)), wide),
            ),
            [in_smem()] + [in_vmem()] * (3 + len(pairs)),
            [
                pltpu.VMEM((2, rows, width), wide),
                pltpu.VMEM((width // LANES, SUBLANES, rows, LANES), wide),
                pltpu.VMEM((width // LANES, out_rows, LANES), wide),
            ],
        )(table, normed, dist, conv_taps, *pairs)
        far_centred = far_values(centred)
        all_stats = lax.all_gather(stats, "tp")
        pieces = out_pieces[n]
        share = kernel(
            functools.partial(project_body, n, far, out_slots[n], blocks_at),
            jax.ShapeDtypeStruct((out_rows, model_width), narrow),
            [in_smem()] + [in_vmem()] * (3 + far - 1 + far + len(pieces)),
            [pltpu.VMEM((far, out_rows, width), narrow)],
        )(table, all_stats, norm_gain, norm_shift, *far_norm, *far_centred, *pieces)
        shares = [share]
        for _ in range(1, near):
            shares.append(lax.ppermute(shares[-1], "tp", near_pairs))
        is_last = n == layer_count - 1
        shape = jax.ShapeDtypeStruct((out_rows, model_width), narrow)
        gains = () if is_last else (pre_gain,)
        result = kernel(
            functools.partial(add_body, n, tail, is_last, len(states)),
            shape if is_last else (shape, shape),
            [in_vmem()] * (len(states) + len(gains) + len(shares)),
        )(*states, *gains, *shares)
        if is_last:
            return result
        hidden, normed = result
        states = (hidden,)


def solution(mesh):
    return jax.shard_map(
        on_device,
        mesh=mesh,
        in_specs=(
            P("sp", None),
            P("sp"),
            P(),
            P(None, "sp", "tp"),
            P(None, "sp", "tp"),
            P(None, "tp", "sp"),
            P(None, None, "tp"),
            P(None, "tp"),
            P(None, "tp"),
        ),
        out_specs=P("sp", None),
        check_vma=False,
    )
```

profile of v0, /device:TPU:0, one launch (start us, length us, event | category | flops | bytes accessed | tf_op | source)
XLA Modules:
  0.0 152.5 jit_solution(9959073503611701324)
XLA Ops:
  2.9 3.1 %collective-permute-start.2 = (bf16[2,256,256]{2,1,0:T(8,128)(2,1)S(1)}, bf16[2,256,256]{2,1,0:T(8,128)(2,1)S(1)}, u32[]{:S(2)}, u32[]{:S(2)}) collective-permute-start(bf16[2,256,256]{2,1,0:T(8,128)(2,1)S(1)} %get-tuple-element.15.refs_0_), channel_id=1, source_target_pairs={{0,8},{8,16},{16,24},{24,28},{28,20},{20,12},{12,4},{4,0},{1,9},{9... | collective-permute-start | bytes 786440 | tf_op jit(solution)/shard_map/ppermute | solution.py:235
  6.0 6.2 %collective-permute-done.2.refs_1_ = bf16[2,256,256]{2,1,0:T(8,128)(2,1)S(1)} collective-permute-done((bf16[2,256,256]{2,1,0:T(8,128)(2,1)S(1)}, bf16[2,256,256]{2,1,0:T(8,128)(2,1)S(1)}, u32[]{:S(2)}, u32[]{:S(2)}) %collective-permute-start.2) | collective-permute-done | bytes 262176 | tf_op jit(solution)/shard_map/ppermute | solution.py:235
  15.0 2.1 %collective-permute-start = (bf16[64,2048]{1,0:T(8,128)(2,1)S(1)}, bf16[64,2048]{1,0:T(8,128)(2,1)S(1)}, u32[]{:S(2)}, u32[]{:S(2)}) collective-permute-start(bf16[64,2048]{1,0:T(8,128)(2,1)S(1)} %slice.128), channel_id=1, source_target_pairs={{0,4},{4,8},{8,12},{12,16},{16,20},{20,24},{24,28},{1,5},{5,9},{9,... | collective-permute-start | bytes 786440 | tf_op jit(solution)/shard_map/ppermute | solution.py:299
  20.1 2.4 %collective-permute-start.6 = (bf16[2,256,256]{2,1,0:T(8,128)(2,1)S(1)}, bf16[2,256,256]{2,1,0:T(8,128)(2,1)S(1)}, u32[]{:S(2)}, u32[]{:S(2)}) collective-permute-start(bf16[2,256,256]{2,1,0:T(8,128)(2,1)S(1)} %collective-permute-done.4.refs_3_), channel_id=1, source_target_pairs={{0,8},{8,16},{16,24},{24,28},{28,20},{20,12},{12,4},{4,0},{1,9},{9... | collective-permute-start | bytes 786440 | tf_op jit(solution)/shard_map/ppermute | solution.py:235
  25.5 2.0 %collective-permute-done.1 = s32[64]{0:T(128)S(1)} collective-permute-done((s32[64]{0:T(128)S(1)}, s32[64]{0:T(128)S(1)}, u32[]{:S(2)}, u32[]{:S(2)}) %collective-permute-start.1) | collective-permute-done | bytes 288 | tf_op jit(solution)/shard_map/ppermute | solution.py:298
  29.0 2.1 %collective-permute-done.9.refs_0_ = f32[2,2,256]{2,1,0:T(2,128)S(1)} collective-permute-done((f32[2,2,256]{2,1,0:T(2,128)S(1)}, f32[2,2,256]{2,1,0:T(2,128)S(1)}, u32[]{:S(2)}, u32[]{:S(2)}) %collective-permute-start.9) | collective-permute-done | bytes 4128 | tf_op jit(solution)/shard_map/ppermute | solution.py:277
  31.1 2.6 %collective-permute-start.14 = (bf16[256,256]{1,0:T(8,128)(2,1)S(1)}, bf16[256,256]{1,0:T(8,128)(2,1)S(1)}, u32[]{:S(2)}, u32[]{:S(2)}) collective-permute-start(bf16[256,256]{1,0:T(8,128)(2,1)S(1)} %get-tuple-element.18), channel_id=1, source_target_pairs={{8,0},{16,8},{24,16},{28,24},{20,28},{12,20},{4,12},{0,4},{9,1},{1... | collective-permute-start | bytes 393224 | tf_op jit(solution)/shard_map/ppermute | solution.py:238
  33.6 1.9 %collective-permute-start.16 = (bf16[256,256]{1,0:T(8,128)(2,1)S(1)}, bf16[256,256]{1,0:T(8,128)(2,1)S(1)}, u32[]{:S(2)}, u32[]{:S(2)}) collective-permute-start(bf16[256,256]{1,0:T(8,128)(2,1)S(1)} %collective-permute-done.12.refs_5_), channel_id=1, source_target_pairs={{0,8},{8,16},{16,24},{24,28},{28,20},{20,12},{12,4},{4,0},{1,9},{9... | collective-permute-start | bytes 393224 | tf_op jit(solution)/shard_map/ppermute | solution.py:235
  37.1 1.9 %collective-permute-done.14.refs_7_ = bf16[256,256]{1,0:T(8,128)(2,1)S(1)} collective-permute-done((bf16[256,256]{1,0:T(8,128)(2,1)S(1)}, bf16[256,256]{1,0:T(8,128)(2,1)S(1)}, u32[]{:S(2)}, u32[]{:S(2)}) %collective-permute-start.14) | collective-permute-done | bytes 131104 | tf_op jit(solution)/shard_map/ppermute | solution.py:238
  39.0 2.3 %collective-permute-start.13 = (bf16[256,256]{1,0:T(8,128)(2,1)S(1)}, bf16[256,256]{1,0:T(8,128)(2,1)S(1)}, u32[]{:S(2)}, u32[]{:S(2)}) collective-permute-start(bf16[256,256]{1,0:T(8,128)(2,1)S(1)} %collective-permute-done.12.refs_5_), channel_id=1, source_target_pairs={{0,2},{1,3},{2,0},{3,1},{4,6},{5,7},{6,4},{7,5},{8,10},{9,11},{10,... | collective-permute-start | bytes 393224 | tf_op jit(solution)/shard_map/ppermute | solution.py:277
  43.6 2.5 %collective-permute-start.8 = (bf16[2,256,256]{2,1,0:T(8,128)(2,1)S(1)}, bf16[2,256,256]{2,1,0:T(8,128)(2,1)S(1)}, u32[]{:S(2)}, u32[]{:S(2)}) collective-permute-start(bf16[2,256,256]{2,1,0:T(8,128)(2,1)S(1)} %collective-permute-done.6.refs_5_), channel_id=1, source_target_pairs={{0,8},{8,16},{16,24},{24,28},{28,20},{20,12},{12,4},{4,0},{1,9},{9... | collective-permute-start | bytes 786440 | tf_op jit(solution)/shard_map/ppermute | solution.py:235
  49.0 2.8 %collective-permute-done.7.refs_6_ = bf16[2,256,256]{2,1,0:T(8,128)(2,1)S(1)} collective-permute-done((bf16[2,256,256]{2,1,0:T(8,128)(2,1)S(1)}, bf16[2,256,256]{2,1,0:T(8,128)(2,1)S(1)}, u32[]{:S(2)}, u32[]{:S(2)}) %collective-permute-start.7) | collective-permute-done | bytes 262176 | tf_op jit(solution)/shard_map/ppermute | solution.py:238
  51.7 2.4 %collective-permute-start.22 = (bf16[256,256]{1,0:T(8,128)(2,1)S(1)}, bf16[256,256]{1,0:T(8,128)(2,1)S(1)}, u32[]{:S(2)}, u32[]{:S(2)}) collective-permute-start(bf16[256,256]{1,0:T(8,128)(2,1)S(1)} %collective-permute-done.18.refs_11_), channel_id=1, source_target_pairs={{8,0},{16,8},{24,16},{28,24},{20,28},{12,20},{4,12},{0,4},{9,1},{1... | collective-permute-start | bytes 393224 | tf_op jit(solution)/shard_map/ppermute | solution.py:238
  58.0 4.0 %shard_map.102 = (bf16[416,256]{1,0:T(8,128)(2,1)S(1)}, f32[2,512]{1,0:T(2,128)S(1)}) custom-call(s32[10]{0:T(128)S(1)} %dynamic-slice_bitcast_fusion.table_ref, bf16[448,2048]{1,0:T(8,128)(2,1)S(1)} %shard_map.100.normed_ref, s32[416,128]{1,0:T(8,128)S(1)} %broadcast_in_dim.2.dist_ref, f32[2,31,256]{2,1,0:T(8,128)S(1)} %copy.13.taps_ref, ...), custom_call_target="tpu_custom_call" | custom-call | tf_op jit(solution)/shard_map/pallas_call | solution.py:329
  66.5 8.2 %all-gather.2.stats_ref = f32[4,2,512]{2,1,0:T(2,128)S(1)} all-gather(f32[1,2,512]{2,1,0:T(2,128)S(1)} %bitcast.8), channel_id=2, replica_groups=mesh['sp'=8,'tp'=4] {'tp'}, dimensions={0}, use_global_device_ids=true | all-gather | bytes 20480 | tf_op jit(solution)/shard_map/all_gather | solution.py:343
  74.7 3.2 %shard_map.103.refs_3_ = bf16[416,2048]{1,0:T(8,128)(2,1)S(1)} custom-call(s32[10]{0:T(128)S(1)} %dynamic-slice_bitcast_fusion.table_ref, f32[4,2,512]{2,1,0:T(2,128)S(1)} %all-gather.2.stats_ref, f32[2,256]{1,0:T(2,128)S(1)} %copy-done.10, f32[2,256]{1,0:T(2,128)S(1)} %copy-done.11, f32[2,2,256]{2,1,0:T(2,128)S(1)} %collective-permute-done.9.refs_0_, ...), custom_call_target="tpu_custom_call" | custom-call | tf_op jit(solution)/shard_map/pallas_call | solution.py:345
  80.4 6.5 %collective-permute-done.27.refs_1_ = bf16[2,256,256]{2,1,0:T(8,128)(2,1)S(1)} collective-permute-done((bf16[2,256,256]{2,1,0:T(8,128)(2,1)S(1)}, bf16[2,256,256]{2,1,0:T(8,128)(2,1)S(1)}, u32[]{:S(2)}, u32[]{:S(2)}) %collective-permute-start.27) | collective-permute-done | bytes 262176 | tf_op jit(solution)/shard_map/ppermute | solution.py:235
  89.0 6.0 %collective-permute-done.29.refs_3_ = bf16[2,256,256]{2,1,0:T(8,128)(2,1)S(1)} collective-permute-done((bf16[2,256,256]{2,1,0:T(8,128)(2,1)S(1)}, bf16[2,256,256]{2,1,0:T(8,128)(2,1)S(1)}, u32[]{:S(2)}, u32[]{:S(2)}) %collective-permute-start.29) | collective-permute-done | bytes 262176 | tf_op jit(solution)/shard_map/ppermute | solution.py:235
  96.2 2.5 %collective-permute-start.35 = (bf16[256,256]{1,0:T(8,128)(2,1)S(1)}, bf16[256,256]{1,0:T(8,128)(2,1)S(1)}, u32[]{:S(2)}, u32[]{:S(2)}) collective-permute-start(bf16[256,256]{1,0:T(8,128)(2,1)S(1)} %get-tuple-element.24), channel_id=1, source_target_pairs={{0,8},{8,16},{16,24},{24,28},{28,20},{20,12},{12,4},{4,0},{1,9},{9... | collective-permute-start | bytes 393224 | tf_op jit(solution)/shard_map/ppermute | solution.py:235
  98.7 7.4 %collective-permute-done.35.refs_5_ = bf16[256,256]{1,0:T(8,128)(2,1)S(1)} collective-permute-done((bf16[256,256]{1,0:T(8,128)(2,1)S(1)}, bf16[256,256]{1,0:T(8,128)(2,1)S(1)}, u32[]{:S(2)}, u32[]{:S(2)}) %collective-permute-start.35) | collective-permute-done | bytes 131104 | tf_op jit(solution)/shard_map/ppermute | solution.py:235
  106.1 2.5 %collective-permute-start.32 = (bf16[2,256,256]{2,1,0:T(8,128)(2,1)S(1)}, bf16[2,256,256]{2,1,0:T(8,128)(2,1)S(1)}, u32[]{:S(2)}, u32[]{:S(2)}) collective-permute-start(bf16[2,256,256]{2,1,0:T(8,128)(2,1)S(1)} %collective-permute-done.30.refs_4_), channel_id=1, source_target_pairs={{8,0},{16,8},{24,16},{28,24},{20,28},{12,20},{4,12},{0,4},{9,1},{1... | collective-permute-start | bytes 786440 | tf_op jit(solution)/shard_map/ppermute | solution.py:238
  108.6 2.1 %collective-permute-start.41 = (bf16[256,256]{1,0:T(8,128)(2,1)S(1)}, bf16[256,256]{1,0:T(8,128)(2,1)S(1)}, u32[]{:S(2)}, u32[]{:S(2)}) collective-permute-start(bf16[256,256]{1,0:T(8,128)(2,1)S(1)} %collective-permute-done.37.refs_7_), channel_id=1, source_target_pairs={{8,0},{16,8},{24,16},{28,24},{20,28},{12,20},{4,12},{0,4},{9,1},{1... | collective-permute-start | bytes 393224 | tf_op jit(solution)/shard_map/ppermute | solution.py:238
  110.6 2.2 %collective-permute-done.39.refs_9_ = bf16[256,256]{1,0:T(8,128)(2,1)S(1)} collective-permute-done((bf16[256,256]{1,0:T(8,128)(2,1)S(1)}, bf16[256,256]{1,0:T(8,128)(2,1)S(1)}, u32[]{:S(2)}, u32[]{:S(2)}) %collective-permute-start.39) | collective-permute-done | bytes 131104 | tf_op jit(solution)/shard_map/ppermute | solution.py:235
  112.9 2.6 %collective-permute-done.41.refs_11_ = bf16[256,256]{1,0:T(8,128)(2,1)S(1)} collective-permute-done((bf16[256,256]{1,0:T(8,128)(2,1)S(1)}, bf16[256,256]{1,0:T(8,128)(2,1)S(1)}, u32[]{:S(2)}, u32[]{:S(2)}) %collective-permute-start.41) | collective-permute-done | bytes 131104 | tf_op jit(solution)/shard_map/ppermute | solution.py:238
  115.5 3.6 %collective-permute-done.43.refs_13_ = bf16[256,256]{1,0:T(8,128)(2,1)S(1)} collective-permute-done((bf16[256,256]{1,0:T(8,128)(2,1)S(1)}, bf16[256,256]{1,0:T(8,128)(2,1)S(1)}, u32[]{:S(2)}, u32[]{:S(2)}) %collective-permute-start.43) | collective-permute-done | bytes 131104 | tf_op jit(solution)/shard_map/ppermute | solution.py:235
  120.9 2.0 %collective-permute-start.40 = (bf16[256,256]{1,0:T(8,128)(2,1)S(1)}, bf16[256,256]{1,0:T(8,128)(2,1)S(1)}, u32[]{:S(2)}, u32[]{:S(2)}) collective-permute-start(bf16[256,256]{1,0:T(8,128)(2,1)S(1)} %collective-permute-done.39.refs_9_), channel_id=1, source_target_pairs={{0,2},{1,3},{2,0},{3,1},{4,6},{5,7},{6,4},{7,5},{8,10},{9,11},{10,... | collective-permute-start | bytes 393224 | tf_op jit(solution)/shard_map/ppermute | solution.py:277
  124.5 3.7 %shard_map.106 = (bf16[384,256]{1,0:T(8,128)(2,1)S(1)}, f32[2,384]{1,0:T(2,128)S(1)}) custom-call(s32[10]{0:T(128)S(1)} %dynamic-slice_bitcast_fusion.table_ref, bf16[416,2048]{1,0:T(8,128)(2,1)S(1)} %get-tuple-element.20.normed_ref, s32[416,128]{1,0:T(8,128)S(1)} %broadcast_in_dim.2.dist_ref, f32[2,31,256]{2,1,0:T(8,128)S(1)} %copy.13.taps_ref, ...), custom_call_target="tpu_custom_call" | custom-call | tf_op jit(solution)/shard_map/pallas_call | solution.py:329
  128.4 2.0 %collective-permute-start.42 = (bf16[256,256]{1,0:T(8,128)(2,1)S(1)}, bf16[256,256]{1,0:T(8,128)(2,1)S(1)}, u32[]{:S(2)}, u32[]{:S(2)}) collective-permute-start(bf16[256,256]{1,0:T(8,128)(2,1)S(1)} %collective-permute-done.41.refs_11_), channel_id=1, source_target_pairs={{0,2},{1,3},{2,0},{3,1},{4,6},{5,7},{6,4},{7,5},{8,10},{9,11},{10,... | collective-permute-start | bytes 393224 | tf_op jit(solution)/shard_map/ppermute | solution.py:277
  130.4 1.9 %collective-permute-start.46 = (bf16[256,256]{1,0:T(8,128)(2,1)S(1)}, bf16[256,256]{1,0:T(8,128)(2,1)S(1)}, u32[]{:S(2)}, u32[]{:S(2)}) collective-permute-start(bf16[256,256]{1,0:T(8,128)(2,1)S(1)} %collective-permute-done.45.refs_15_), channel_id=1, source_target_pairs={{0,2},{1,3},{2,0},{3,1},{4,6},{5,7},{6,4},{7,5},{8,10},{9,11},{10,... | collective-permute-start | bytes 393224 | tf_op jit(solution)/shard_map/ppermute | solution.py:277
  132.4 11.7 %all-gather.3.stats_ref = f32[4,2,384]{2,1,0:T(2,128)S(1)} all-gather(f32[1,2,384]{2,1,0:T(2,128)S(1)} %bitcast.9), channel_id=3, replica_groups=mesh['sp'=8,'tp'=4] {'tp'}, dimensions={0}, use_global_device_ids=true | all-gather | bytes 15360 | tf_op jit(solution)/shard_map/all_gather | solution.py:343
  144.2 3.0 %shard_map.107.refs_1_ = bf16[384,2048]{1,0:T(8,128)(2,1)S(1)} custom-call(s32[10]{0:T(128)S(1)} %dynamic-slice_bitcast_fusion.table_ref, f32[4,2,384]{2,1,0:T(2,128)S(1)} %all-gather.3.stats_ref, f32[2,256]{1,0:T(2,128)S(1)} %copy-done.10, f32[2,256]{1,0:T(2,128)S(1)} %copy-done.11, f32[2,2,256]{2,1,0:T(2,128)S(1)} %collective-permute-done.9.refs_0_, ...), custom_call_target="tpu_custom_call" | custom-call | tf_op jit(solution)/shard_map/pallas_call | solution.py:345
  147.6 3.1 %collective-permute-done.49.refs_2_ = bf16[384,2048]{1,0:T(8,128)(2,1)S(1)} collective-permute-done((bf16[384,2048]{1,0:T(8,128)(2,1)S(1)}, bf16[384,2048]{1,0:T(8,128)(2,1)S(1)}, u32[]{:S(2)}, u32[]{:S(2)}) %collective-permute-start.49) | collective-permute-done | bytes 1572896 | tf_op jit(solution)/shard_map/ppermute | solution.py:353
  (112 shorter events, 39.9 us)
Async XLA Ops:
  2.9 9.3 %collective-permute-start.2 = (bf16[2,256,256]{2,1,0:T(8,128)(2,1)S(1)}, bf16[2,256,256]{2,1,0:T(8,128)(2,1)S(1)}, u32[]{:S(2)}, u32[]{:S(2)}) collective-permute-start(bf16[2,256,256]{2,1,0:T(8,128)(2,1)S(1)} %get-tuple-element.15.refs_0_), channel_id=1, source_target_pairs={{0,8},{8,16},{16,24},{24,28},{28,20},{20,12},{12,4},{4,0},{1,9},{9... | collective-permute-start | bytes 786440 | tf_op jit(solution)/shard_map/ppermute | solution.py:235
  6.0 12.9 %collective-permute-start.3 = (bf16[2,256,256]{2,1,0:T(8,128)(2,1)S(1)}, bf16[2,256,256]{2,1,0:T(8,128)(2,1)S(1)}, u32[]{:S(2)}, u32[]{:S(2)}) collective-permute-start(bf16[2,256,256]{2,1,0:T(8,128)(2,1)S(1)} %get-tuple-element.15.refs_0_), channel_id=1, source_target_pairs={{8,0},{16,8},{24,16},{28,24},{20,28},{12,20},{4,12},{0,4},{9,1},{1... | collective-permute-start | bytes 786440 | tf_op jit(solution)/shard_map/ppermute | solution.py:238
  15.0 26.3 %collective-permute-start = (bf16[64,2048]{1,0:T(8,128)(2,1)S(1)}, bf16[64,2048]{1,0:T(8,128)(2,1)S(1)}, u32[]{:S(2)}, u32[]{:S(2)}) collective-permute-start(bf16[64,2048]{1,0:T(8,128)(2,1)S(1)} %slice.128), channel_id=1, source_target_pairs={{0,4},{4,8},{8,12},{12,16},{16,20},{20,24},{24,28},{1,5},{5,9},{9,... | collective-permute-start | bytes 786440 | tf_op jit(solution)/shard_map/ppermute | solution.py:299
  17.1 16.5 %collective-permute-start.12 = (bf16[256,256]{1,0:T(8,128)(2,1)S(1)}, bf16[256,256]{1,0:T(8,128)(2,1)S(1)}, u32[]{:S(2)}, u32[]{:S(2)}) collective-permute-start(bf16[256,256]{1,0:T(8,128)(2,1)S(1)} %get-tuple-element.18), channel_id=1, source_target_pairs={{0,8},{8,16},{16,24},{24,28},{28,20},{20,12},{12,4},{4,0},{1,9},{9... | collective-permute-start | bytes 393224 | tf_op jit(solution)/shard_map/ppermute | solution.py:235
  18.9 24.4 %collective-permute-start.5 = (bf16[2,256,256]{2,1,0:T(8,128)(2,1)S(1)}, bf16[2,256,256]{2,1,0:T(8,128)(2,1)S(1)}, u32[]{:S(2)}, u32[]{:S(2)}) collective-permute-start(bf16[2,256,256]{2,1,0:T(8,128)(2,1)S(1)} %collective-permute-done.3.refs_2_), channel_id=1, source_target_pairs={{8,0},{16,8},{24,16},{28,24},{20,28},{12,20},{4,12},{0,4},{9,1},{1... | collective-permute-start | bytes 786440 | tf_op jit(solution)/shard_map/ppermute | solution.py:238
  20.1 23.5 %collective-permute-start.6 = (bf16[2,256,256]{2,1,0:T(8,128)(2,1)S(1)}, bf16[2,256,256]{2,1,0:T(8,128)(2,1)S(1)}, u32[]{:S(2)}, u32[]{:S(2)}) collective-permute-start(bf16[2,256,256]{2,1,0:T(8,128)(2,1)S(1)} %collective-permute-done.4.refs_3_), channel_id=1, source_target_pairs={{0,8},{8,16},{16,24},{24,28},{28,20},{20,12},{12,4},{4,0},{1,9},{9... | collective-permute-start | bytes 786440 | tf_op jit(solution)/shard_map/ppermute | solution.py:235
  43.6 11.3 %collective-permute-start.8 = (bf16[2,256,256]{2,1,0:T(8,128)(2,1)S(1)}, bf16[2,256,256]{2,1,0:T(8,128)(2,1)S(1)}, u32[]{:S(2)}, u32[]{:S(2)}) collective-permute-start(bf16[2,256,256]{2,1,0:T(8,128)(2,1)S(1)} %collective-permute-done.6.refs_5_), channel_id=1, source_target_pairs={{0,8},{8,16},{16,24},{24,28},{28,20},{20,12},{12,4},{4,0},{1,9},{9... | collective-permute-start | bytes 786440 | tf_op jit(solution)/shard_map/ppermute | solution.py:235
  46.8 15.6 %collective-permute-start.11 = (bf16[2,256,256]{2,1,0:T(8,128)(2,1)}, bf16[2,256,256]{2,1,0:T(8,128)(2,1)S(1)}, u32[]{:S(2)}, u32[]{:S(2)}) collective-permute-start(bf16[2,256,256]{2,1,0:T(8,128)(2,1)} %refs_3_.3), channel_id=1, source_target_pairs={{0,2},{1,3},{2,0},{3,1},{4,6},{5,7},{6,4},{7,5},{8,10},{9,11},{10,... | collective-permute-start | bytes 786440 | tf_op jit(solution)/shard_map/ppermute | solution.py:277
  47.0 15.0 %collective-permute-start.15 = (bf16[256,256]{1,0:T(8,128)(2,1)S(1)}, bf16[256,256]{1,0:T(8,128)(2,1)S(1)}, u32[]{:S(2)}, u32[]{:S(2)}) collective-permute-start(bf16[256,256]{1,0:T(8,128)(2,1)S(1)} %collective-permute-done.14.refs_7_), channel_id=1, source_target_pairs={{0,2},{1,3},{2,0},{3,1},{4,6},{5,7},{6,4},{7,5},{8,10},{9,11},{10,... | collective-permute-start | bytes 393224 | tf_op jit(solution)/shard_map/ppermute | solution.py:277
  48.8 15.6 %collective-permute-start.17 = (bf16[256,256]{1,0:T(8,128)(2,1)S(1)}, bf16[256,256]{1,0:T(8,128)(2,1)S(1)}, u32[]{:S(2)}, u32[]{:S(2)}) collective-permute-start(bf16[256,256]{1,0:T(8,128)(2,1)S(1)} %collective-permute-done.16.refs_9_), channel_id=1, source_target_pairs={{0,2},{1,3},{2,0},{3,1},{4,6},{5,7},{6,4},{7,5},{8,10},{9,11},{10,... | collective-permute-start | bytes 393224 | tf_op jit(solution)/shard_map/ppermute | solution.py:277
  51.7 12.3 %collective-permute-start.22 = (bf16[256,256]{1,0:T(8,128)(2,1)S(1)}, bf16[256,256]{1,0:T(8,128)(2,1)S(1)}, u32[]{:S(2)}, u32[]{:S(2)}) collective-permute-start(bf16[256,256]{1,0:T(8,128)(2,1)S(1)} %collective-permute-done.18.refs_11_), channel_id=1, source_target_pairs={{8,0},{16,8},{24,16},{28,24},{20,28},{12,20},{4,12},{0,4},{9,1},{1... | collective-permute-start | bytes 393224 | tf_op jit(solution)/shard_map/ppermute | solution.py:238
  54.9 11.2 %collective-permute-start.24 = (bf16[256,256]{1,0:T(8,128)(2,1)S(1)}, bf16[256,256]{1,0:T(8,128)(2,1)S(1)}, u32[]{:S(2)}, u32[]{:S(2)}) collective-permute-start(bf16[256,256]{1,0:T(8,128)(2,1)S(1)} %collective-permute-done.20.refs_13_), channel_id=1, source_target_pairs={{0,8},{8,16},{16,24},{24,28},{28,20},{20,12},{12,4},{4,0},{1,9},{9... | collective-permute-start | bytes 393224 | tf_op jit(solution)/shard_map/ppermute | solution.py:235
  61.9 12.8 %collective-permute-start.10 = (bf16[416,256]{1,0:T(8,128)(2,1)S(1)}, bf16[416,256]{1,0:T(8,128)(2,1)S(1)}, u32[]{:S(2)}, u32[]{:S(2)}) collective-permute-start(bf16[416,256]{1,0:T(8,128)(2,1)S(1)} %get-tuple-element.17.refs_1_), channel_id=1, source_target_pairs={{0,2},{1,3},{2,0},{3,1},{4,6},{5,7},{6,4},{7,5},{8,10},{9,11},{10,... | collective-permute-start | bytes 638984 | tf_op jit(solution)/shard_map/ppermute | solution.py:277
  62.4 12.3 %collective-permute-start.19 = (bf16[256,256]{1,0:T(8,128)(2,1)S(1)}, bf16[256,256]{1,0:T(8,128)(2,1)S(1)}, u32[]{:S(2)}, u32[]{:S(2)}) collective-permute-start(bf16[256,256]{1,0:T(8,128)(2,1)S(1)} %collective-permute-done.18.refs_11_), channel_id=1, source_target_pairs={{0,2},{1,3},{2,0},{3,1},{4,6},{5,7},{6,4},{7,5},{8,10},{9,11},{10,... | collective-permute-start | bytes 393224 | tf_op jit(solution)/shard_map/ppermute | solution.py:277
  64.0 10.6 %collective-permute-start.21 = (bf16[256,256]{1,0:T(8,128)(2,1)S(1)}, bf16[256,256]{1,0:T(8,128)(2,1)S(1)}, u32[]{:S(2)}, u32[]{:S(2)}) collective-permute-start(bf16[256,256]{1,0:T(8,128)(2,1)S(1)} %collective-permute-done.20.refs_13_), channel_id=1, source_target_pairs={{0,2},{1,3},{2,0},{3,1},{4,6},{5,7},{6,4},{7,5},{8,10},{9,11},{10,... | collective-permute-start | bytes 393224 | tf_op jit(solution)/shard_map/ppermute | solution.py:277
  64.4 10.3 %collective-permute-start.23 = (bf16[256,256]{1,0:T(8,128)(2,1)S(1)}, bf16[256,256]{1,0:T(8,128)(2,1)S(1)}, u32[]{:S(2)}, u32[]{:S(2)}) collective-permute-start(bf16[256,256]{1,0:T(8,128)(2,1)S(1)} %collective-permute-done.22.refs_15_), channel_id=1, source_target_pairs={{0,2},{1,3},{2,0},{3,1},{4,6},{5,7},{6,4},{7,5},{8,10},{9,11},{10,... | collective-permute-start | bytes 393224 | tf_op jit(solution)/shard_map/ppermute | solution.py:277
  77.9 45.0 %collective-permute-start.26 = (bf16[416,2048]{1,0:T(8,128)(2,1)S(1)}, bf16[416,2048]{1,0:T(8,128)(2,1)S(1)}, u32[]{:S(2)}, u32[]{:S(2)}) collective-permute-start(bf16[416,2048]{1,0:T(8,128)(2,1)S(1)} %shard_map.103.refs_3_), channel_id=1, source_target_pairs={{0,1},{1,0},{2,3},{3,2},{4,5},{5,4},{6,7},{7,6},{8,9},{9,8},{10,11... | collective-permute-start | bytes 5111816 | tf_op jit(solution)/shard_map/ppermute | solution.py:353
  89.0 17.1 %collective-permute-start.30 = (bf16[2,256,256]{2,1,0:T(8,128)(2,1)S(1)}, bf16[2,256,256]{2,1,0:T(8,128)(2,1)S(1)}, u32[]{:S(2)}, u32[]{:S(2)}) collective-permute-start(bf16[2,256,256]{2,1,0:T(8,128)(2,1)S(1)} %collective-permute-done.28.refs_2_), channel_id=1, source_target_pairs={{8,0},{16,8},{24,16},{28,24},{20,28},{12,20},{4,12},{0,4},{9,1},{1... | collective-permute-start | bytes 786440 | tf_op jit(solution)/shard_map/ppermute | solution.py:238
  95.0 13.5 %collective-permute-start.31 = (bf16[2,256,256]{2,1,0:T(8,128)(2,1)S(1)}, bf16[2,256,256]{2,1,0:T(8,128)(2,1)S(1)}, u32[]{:S(2)}, u32[]{:S(2)}) collective-permute-start(bf16[2,256,256]{2,1,0:T(8,128)(2,1)S(1)} %collective-permute-done.29.refs_3_), channel_id=1, source_target_pairs={{0,8},{8,16},{16,24},{24,28},{28,20},{20,12},{12,4},{4,0},{1,9},{9... | collective-permute-start | bytes 786440 | tf_op jit(solution)/shard_map/ppermute | solution.py:235
  96.2 9.9 %collective-permute-start.35 = (bf16[256,256]{1,0:T(8,128)(2,1)S(1)}, bf16[256,256]{1,0:T(8,128)(2,1)S(1)}, u32[]{:S(2)}, u32[]{:S(2)}) collective-permute-start(bf16[256,256]{1,0:T(8,128)(2,1)S(1)} %get-tuple-element.24), channel_id=1, source_target_pairs={{0,8},{8,16},{16,24},{24,28},{28,20},{20,12},{12,4},{4,0},{1,9},{9... | collective-permute-start | bytes 393224 | tf_op jit(solution)/shard_map/ppermute | solution.py:235
  98.7 9.9 %collective-permute-start.37 = (bf16[256,256]{1,0:T(8,128)(2,1)S(1)}, bf16[256,256]{1,0:T(8,128)(2,1)S(1)}, u32[]{:S(2)}, u32[]{:S(2)}) collective-permute-start(bf16[256,256]{1,0:T(8,128)(2,1)S(1)} %get-tuple-element.24), channel_id=1, source_target_pairs={{8,0},{16,8},{24,16},{28,24},{20,28},{12,20},{4,12},{0,4},{9,1},{1... | collective-permute-start | bytes 393224 | tf_op jit(solution)/shard_map/ppermute | solution.py:238
  106.1 13.1 %collective-permute-start.32 = (bf16[2,256,256]{2,1,0:T(8,128)(2,1)S(1)}, bf16[2,256,256]{2,1,0:T(8,128)(2,1)S(1)}, u32[]{:S(2)}, u32[]{:S(2)}) collective-permute-start(bf16[2,256,256]{2,1,0:T(8,128)(2,1)S(1)} %collective-permute-done.30.refs_4_), channel_id=1, source_target_pairs={{8,0},{16,8},{24,16},{28,24},{20,28},{12,20},{4,12},{0,4},{9,1},{1... | collective-permute-start | bytes 786440 | tf_op jit(solution)/shard_map/ppermute | solution.py:238
  108.5 12.3 %collective-permute-start.33 = (bf16[2,256,256]{2,1,0:T(8,128)(2,1)S(1)}, bf16[2,256,256]{2,1,0:T(8,128)(2,1)S(1)}, u32[]{:S(2)}, u32[]{:S(2)}) collective-permute-start(bf16[2,256,256]{2,1,0:T(8,128)(2,1)S(1)} %collective-permute-done.31.refs_5_), channel_id=1, source_target_pairs={{0,8},{8,16},{16,24},{24,28},{28,20},{20,12},{12,4},{4,0},{1,9},{9... | collective-permute-start | bytes 786440 | tf_op jit(solution)/shard_map/ppermute | solution.py:235
  115.5 12.7 %collective-permute-start.36 = (bf16[256,256]{1,0:T(8,128)(2,1)S(1)}, bf16[256,256]{1,0:T(8,128)(2,1)S(1)}, u32[]{:S(2)}, u32[]{:S(2)}) collective-permute-start(bf16[256,256]{1,0:T(8,128)(2,1)S(1)} %collective-permute-done.35.refs_5_), channel_id=1, source_target_pairs={{0,2},{1,3},{2,0},{3,1},{4,6},{5,7},{6,4},{7,5},{8,10},{9,11},{10,... | collective-permute-start | bytes 393224 | tf_op jit(solution)/shard_map/ppermute | solution.py:277
  119.1 11.2 %collective-permute-start.45 = (bf16[256,256]{1,0:T(8,128)(2,1)S(1)}, bf16[256,256]{1,0:T(8,128)(2,1)S(1)}, u32[]{:S(2)}, u32[]{:S(2)}) collective-permute-start(bf16[256,256]{1,0:T(8,128)(2,1)S(1)} %collective-permute-done.41.refs_11_), channel_id=1, source_target_pairs={{8,0},{16,8},{24,16},{28,24},{20,28},{12,20},{4,12},{0,4},{9,1},{1... | collective-permute-start | bytes 393224 | tf_op jit(solution)/shard_map/ppermute | solution.py:238
  120.9 9.5 %collective-permute-start.40 = (bf16[256,256]{1,0:T(8,128)(2,1)S(1)}, bf16[256,256]{1,0:T(8,128)(2,1)S(1)}, u32[]{:S(2)}, u32[]{:S(2)}) collective-permute-start(bf16[256,256]{1,0:T(8,128)(2,1)S(1)} %collective-permute-done.39.refs_9_), channel_id=1, source_target_pairs={{0,2},{1,3},{2,0},{3,1},{4,6},{5,7},{6,4},{7,5},{8,10},{9,11},{10,... | collective-permute-start | bytes 393224 | tf_op jit(solution)/shard_map/ppermute | solution.py:277
  122.9 9.5 %collective-permute-start.47 = (bf16[256,256]{1,0:T(8,128)(2,1)S(1)}, bf16[256,256]{1,0:T(8,128)(2,1)S(1)}, u32[]{:S(2)}, u32[]{:S(2)}) collective-permute-start(bf16[256,256]{1,0:T(8,128)(2,1)S(1)} %collective-permute-done.43.refs_13_), channel_id=1, source_target_pairs={{0,8},{8,16},{16,24},{24,28},{28,20},{20,12},{12,4},{4,0},{1,9},{9... | collective-permute-start | bytes 393224 | tf_op jit(solution)/shard_map/ppermute | solution.py:235
  128.2 15.9 %collective-permute-start.34 = (bf16[384,256]{1,0:T(8,128)(2,1)S(1)}, bf16[384,256]{1,0:T(8,128)(2,1)S(1)}, u32[]{:S(2)}, u32[]{:S(2)}) collective-permute-start(bf16[384,256]{1,0:T(8,128)(2,1)S(1)} %get-tuple-element.23.refs_1_), channel_id=1, source_target_pairs={{0,2},{1,3},{2,0},{3,1},{4,6},{5,7},{6,4},{7,5},{8,10},{9,11},{10,... | collective-permute-start | bytes 589832 | tf_op jit(solution)/shard_map/ppermute | solution.py:277
  128.4 15.8 %collective-permute-start.42 = (bf16[256,256]{1,0:T(8,128)(2,1)S(1)}, bf16[256,256]{1,0:T(8,128)(2,1)S(1)}, u32[]{:S(2)}, u32[]{:S(2)}) collective-permute-start(bf16[256,256]{1,0:T(8,128)(2,1)S(1)} %collective-permute-done.41.refs_11_), channel_id=1, source_target_pairs={{0,2},{1,3},{2,0},{3,1},{4,6},{5,7},{6,4},{7,5},{8,10},{9,11},{10,... | collective-permute-start | bytes 393224 | tf_op jit(solution)/shard_map/ppermute | solution.py:277
  130.3 13.8 %collective-permute-start.44 = (bf16[256,256]{1,0:T(8,128)(2,1)S(1)}, bf16[256,256]{1,0:T(8,128)(2,1)S(1)}, u32[]{:S(2)}, u32[]{:S(2)}) collective-permute-start(bf16[256,256]{1,0:T(8,128)(2,1)S(1)} %collective-permute-done.43.refs_13_), channel_id=1, source_target_pairs={{0,2},{1,3},{2,0},{3,1},{4,6},{5,7},{6,4},{7,5},{8,10},{9,11},{10,... | collective-permute-start | bytes 393224 | tf_op jit(solution)/shard_map/ppermute | solution.py:277
  130.4 13.7 %collective-permute-start.46 = (bf16[256,256]{1,0:T(8,128)(2,1)S(1)}, bf16[256,256]{1,0:T(8,128)(2,1)S(1)}, u32[]{:S(2)}, u32[]{:S(2)}) collective-permute-start(bf16[256,256]{1,0:T(8,128)(2,1)S(1)} %collective-permute-done.45.refs_15_), channel_id=1, source_target_pairs={{0,2},{1,3},{2,0},{3,1},{4,6},{5,7},{6,4},{7,5},{8,10},{9,11},{10,... | collective-permute-start | bytes 393224 | tf_op jit(solution)/shard_map/ppermute | solution.py:277
  132.4 11.8 %collective-permute-start.48 = (bf16[256,256]{1,0:T(8,128)(2,1)S(1)}, bf16[256,256]{1,0:T(8,128)(2,1)S(1)}, u32[]{:S(2)}, u32[]{:S(2)}) collective-permute-start(bf16[256,256]{1,0:T(8,128)(2,1)S(1)} %collective-permute-done.47.refs_17_), channel_id=1, source_target_pairs={{0,2},{1,3},{2,0},{3,1},{4,6},{5,7},{6,4},{7,5},{8,10},{9,11},{10,... | collective-permute-start | bytes 393224 | tf_op jit(solution)/shard_map/ppermute | solution.py:277
  (30 other events, 287.4 us)
where the time goes:
time: 153 us; the launch traced here: 152 us
  starting transfers between devices  57 us (37%)
  waiting for transfers between devices  47.7 us (31%)
  blocking collectives  19.9 us (13%)
  Pallas kernels  17.8 us (12%)
  local copies, waits for them, and re-layouts  7.61 us (5%)
  other arithmetic  2.32 us (2%)
    ppermute x16, waiting for transfers between devices, ring_gathered(): ahead = lax.ppermute(ahead, 'sp', forward)  32.6 us
    ppermute x16, starting transfers between devices, ring_gathered(): ahead = lax.ppermute(ahead, 'sp', forward)  22.6 us
    all_gather x2, blocking collectives, on_device(): all_stats = lax.all_gather(stats, 'tp')  19.9 us
    ppermute x18, starting transfers between devices, far_values(): values.append(lax.ppermute(values[-1], 'tp', far_pairs))  16.7 us
    ppermute x12, starting transfers between devices, ring_gathered(): behind = lax.ppermute(behind, 'sp', backward)  13.3 us
    ppermute x12, waiting for transfers between devices, ring_gathered(): behind = lax.ppermute(behind, 'sp', backward)  7.79 us
    pallas_call x2, Pallas kernels, on_device(): kernel(functools.partial(gated_conv_body, n, tap_count, tail), (jax.Shape...  7.7 us
    pallas_call x2, Pallas kernels, on_device(): kernel(functools.partial(project_body, n, far, out_slots[n], blocks_at),...  6.16 us
  transfers between devices with their start and end apart: 50, of which 14 were waited for; matrix products, arithmetic and copies ran while one was open for 3% of the time, Pallas kernels for 6%

commit v1 on v0

--- a/solution.py
+++ b/solution.py
@@ -49,31 +49,51 @@
     return (state * scale * gain).astype(narrow)
 
 
-def pack_body(value_ref, gate_ref, out_ref, pair_ref, part_ref):
-    pair_ref[0] = value_ref[...]
-    pair_ref[1] = gate_ref[...]
-    part_ref[...] = out_ref[...]
-
-
-def packed(layer, value_proj, gate_proj, out_proj):
-    arrays = (value_proj, gate_proj, out_proj)
+def copied(sources, targets, sems):
+    copies = [
+        pltpu.make_async_copy(source, target, sems.at[i])
+        for i, (source, target) in enumerate(zip(sources, targets))
+    ]
+    for copy in copies:
+        copy.start()
+    for copy in copies:
+        copy.wait()
+
+
+def pack_body(layer, halo, value_ref, gate_ref, *refs):
+    if halo == 0:
+        pair_ref, sems = refs
+        copied([value_ref.at[layer], gate_ref.at[layer]], [pair_ref.at[0], pair_ref.at[1]], sems)
+        return
+    tokens_ref, gain_ref, shift_ref, pair_ref, tail_ref, norms_ref, sems = refs
+    rows = tokens_ref.shape[0]
+    copied(
+        [
+            value_ref.at[layer],
+            gate_ref.at[layer],
+            tokens_ref.at[pl.ds(rows - halo, halo)],
+            gain_ref,
+            shift_ref,
+        ],
+        [pair_ref.at[0], pair_ref.at[1], tail_ref, norms_ref.at[0], norms_ref.at[1]],
+        sems,
+    )
+
+
+def packed(layer, value_proj, gate_proj, halo=0, extra=()):
+    shapes = [jax.ShapeDtypeStruct((2,) + value_proj.shape[1:], narrow)]
+    if halo:
+        tokens, gain, _ = extra
+        shapes.append(jax.ShapeDtypeStruct((halo, tokens.shape[1]), narrow))
+        shapes.append(jax.ShapeDtypeStruct((2,) + gain.shape, wide))
     return pl.pallas_call(
-        pack_body,
-        grid=(1,),
-        out_shape=(
-            jax.ShapeDtypeStruct((2,) + value_proj.shape[1:], narrow),
-            jax.ShapeDtypeStruct(out_proj.shape[1:], narrow),
-        ),
-        in_specs=[
-            pl.BlockSpec((None,) + a.shape[1:], lambda i, layer=layer: (layer, 0, 0))
-            for a in arrays
-        ],
-        out_specs=(
-            pl.BlockSpec((2,) + value_proj.shape[1:], lambda i: (0, 0, 0)),
-            pl.BlockSpec(out_proj.shape[1:], lambda i: (0, 0)),
-        ),
+        functools.partial(pack_body, layer, halo),
+        out_shape=tuple(shapes),
+        in_specs=[pl.BlockSpec(memory_space=pl.ANY)] * (2 + len(extra)),
+        out_specs=tuple(in_vmem() for _ in shapes),
+        scratch_shapes=[pltpu.SemaphoreType.DMA((5 if halo else 2,))],
         compiler_params=pltpu.CompilerParams(vmem_limit_bytes=KERNEL_VMEM),
-    )(*arrays)
+    )(value_proj, gate_proj, *extra)
 
 
 def norm_body(prev_ref, tokens_ref, gain_ref, normed_ref):
@@ -83,19 +103,24 @@
     normed_ref[halo:, :] = normed_of(tokens_ref[...].astype(wide), gain)
 
 
-def gated_conv_body(layer, tap_count, tail, table_ref, normed_ref, dist_ref, taps_ref, *refs):
+def gated_conv_body(
+    layer, tap_count, tail, split, table_ref, normed_ref, dist_ref, taps_ref, *refs
+):
     *pair_refs, centred_ref, stats_ref, acc_ref, shifted_ref, conv_ref = refs
+    pairs = [(pair.at[0], pair.at[1]) for pair in (pair_refs[:-2] if split else pair_refs)]
+    if split:
+        pairs.append(tuple(pair_refs[-2:]))
     width = taps_ref.shape[2]
     halves = width // LANES
     rows = normed_ref.shape[0]
     out_rows = centred_ref.shape[0]
     dist_from = dist_ref.shape[0] - out_rows
     depth = pair_refs[0].shape[1]
-    for k, pair in enumerate(pair_refs):
-        first = 0 if len(pair_refs) == 1 else pl.multiple_of(table_ref[k] * depth, LANES)
+    for k, pair in enumerate(pairs):
+        first = 0 if len(pairs) == 1 else pl.multiple_of(table_ref[k] * depth, LANES)
         rows_in = normed_ref[:, pl.ds(first, depth)]
         for part in range(2):
-            product = jnp.dot(rows_in, pair[part], preferred_element_type=wide)
+            product = jnp.dot(rows_in, pair[part][...], preferred_element_type=wide)
             if k == 0:
                 acc_ref[part] = product
             else:
@@ -146,25 +171,28 @@
     stats_ref[...] = both.T[:2, :]
 
 
-def project_body(layer, far, slots, blocks_at, table_ref, stats_ref, gain_ref, shift_ref, *refs):
+def summed(values):
+    return functools.reduce(jnp.add, values)
+
+
+def project_body(layer, near, far, slots, table_ref, gain_ref, shift_ref, *refs):
     far_norm_refs, refs = refs[: far - 1], refs[far - 1 :]
+    stats_refs, refs = refs[: far * near], refs[far * near :]
     centred_refs, refs = refs[:far], refs[far:]
     *piece_refs, share_ref, act_ref = refs
     out_rows, width = centred_refs[0].shape
-    tp_count = stats_ref.shape[0]
-    stats = jnp.concatenate([stats_ref[j] for j in range(tp_count)])
+    count = far * near
+    fill = jnp.zeros((round_up(2 * count, SUBLANES) - 2 * count, stats_refs[0].shape[1]), wide)
+    stats = jnp.concatenate([ref[...] for ref in stats_refs] + ([fill] if fill.size else []))
     stats = stats.T[:out_rows, :]
-    means = [stats[:, 2 * j : 2 * j + 1] for j in range(tp_count)]
-    mean = functools.reduce(jnp.add, means) / tp_count
-    square = sum(
-        stats[:, 2 * j + 1 : 2 * j + 2] + width * (means[j] - mean) ** 2 for j in range(tp_count)
-    )
-    scale = lax.rsqrt(square / (width * tp_count) + epsilon)
+    means = [stats[:, 2 * j : 2 * j + 1] for j in range(count)]
+    squares = [stats[:, 2 * j + 1 : 2 * j + 2] for j in range(count)]
+    mean = summed([summed(means[f * near : (f + 1) * near]) for f in range(far)]) / count
+    squares = [square + width * (own - mean) ** 2 for square, own in zip(squares, means)]
+    square = summed([summed(squares[f * near : (f + 1) * near]) for f in range(far)])
+    scale = lax.rsqrt(square / (width * count) + epsilon)
     for f, centred in enumerate(centred_refs):
-        block = table_ref[blocks_at + f]
-        own = jnp.zeros_like(mean)
-        for j in range(tp_count):
-            own = jnp.where(block == j, means[j], own)
+        own = means[f * near]
         if f == 0:
             gain, shift = gain_ref[layer : layer + 1, :], shift_ref[layer : layer + 1, :]
         else:
@@ -231,20 +259,21 @@
     forward, backward, _ = ring_tables(count)
     chunks = []
     ahead = behind = value
-    for _ in range(1, count // 2 + 1):
+    for k in range(1, count // 2 + 1):
+        if 2 * k == count:
+            ahead, behind = ahead[0], behind[1]
         ahead = lax.ppermute(ahead, "sp", forward)
-        chunks.append(ahead)
-        if len(chunks) < count - 1:
-            behind = lax.ppermute(behind, "sp", backward)
-            chunks.append(behind)
+        behind = lax.ppermute(behind, "sp", backward)
+        chunks.extend((ahead, behind))
     return chunks
 
 
-def swap_pairs(count, group, step):
+def group_pairs(count, near, far, near_step, far_step):
     pairs = []
     for source in range(count):
-        lead, at = source // (group * step), source // step % group
-        pairs.append((source, (lead * group + (at + 1) % group) * step + source % step))
+        at_far, at_near = source // near, source % near
+        target = (at_far + far_step) % far * near + (at_near + near_step) % near
+        pairs.append((source, target))
     return pairs
 
 
@@ -266,10 +295,11 @@
     width = conv_taps.shape[2]
     sp_count, tp_count = lax.axis_size("sp"), lax.axis_size("tp")
     near, far = tp_groups(tp_count)
-    far_pairs, near_pairs = swap_pairs(tp_count, far, near), swap_pairs(tp_count, near, 1)
+    far_pairs = group_pairs(tp_count, near, far, 0, 1)
+    near_pairs = group_pairs(tp_count, near, far, 1, 0)
     tail = round_up(tap_count - 1, max(HALO_ALIGN, CONV_ROWS))
     halo = tail * layer_count
-    in_ring = ringed(sp_count, value_proj.shape[1], out_proj.shape[2])
+    in_ring = layer_count == 2 and ringed(sp_count, value_proj.shape[1], out_proj.shape[2])
 
     def far_values(value):
         values = [value]
@@ -277,27 +307,36 @@
             values.append(lax.ppermute(values[-1], "tp", far_pairs))
         return values
 
+    packs = [packed(n, value_proj, gate_proj) for n in range(layer_count - 1)]
+    packs.append(
+        packed(layer_count - 1, value_proj, gate_proj, halo, (tokens, norm_gain, norm_shift))
+    )
+    _, tail_rows, norms = packs[-1]
     pair_chunks, out_pieces, out_slots = [], [], []
-    own_out = far_values(out_proj) if in_ring else None
+    if in_ring:
+        chunks = [out_proj] + ring_gathered(out_proj)
+        chunks = [far_values(chunk) for chunk in chunks]
     for n in range(layer_count):
-        pair, part = packed(n, value_proj, gate_proj, out_proj)
+        pair = packs[n][0]
         if in_ring:
             pair_chunks.append([pair] + ring_gathered(pair))
-            pieces, slots = list(own_out), [n] * far
-            for chunk in ring_gathered(part):
-                pieces.extend(far_values(chunk))
-                slots.extend([None] * far)
+            pieces = [piece for k in range(len(chunks) - 2) for piece in chunks[k]]
+            slots = [n] * len(pieces) + [None] * far
+            pieces.extend(chunks[len(chunks) - 2 + n])
         else:
             pair_chunks.append([lax.all_gather(pair, "sp", axis=1, tiled=True)])
-            pieces = [lax.all_gather(value, "sp", axis=1, tiled=True) for value in far_values(part)]
+            pieces = [
+                lax.all_gather(value, "sp", axis=1, tiled=True)
+                for value in far_values(out_proj[n])
+            ]
             slots = [None] * far
         out_pieces.append(pieces)
         out_slots.append(slots)
 
     onward = [(source, source + 1) for source in range(sp_count - 1)]
     prev_docs = lax.ppermute(doc_ids[row_count - halo :] + 1, "sp", onward) - 1
-    prev_rows = lax.ppermute(tokens[row_count - halo :], "sp", onward)
-    far_norm = far_values(jnp.stack([norm_gain, norm_shift]))[1:]
+    prev_rows = lax.ppermute(tail_rows, "sp", onward)
+    far_norm = far_values(norms)[1:]
     docs = jnp.concatenate([prev_docs, doc_ids])
     dist = jnp.zeros((row_count + halo - tail,), jnp.int32)
     for offset in range(1, tap_count):
@@ -305,17 +344,9 @@
         dist = dist + (docs[first : first + dist.shape[0]] == docs[tail:]).astype(jnp.int32)
     dist = jnp.broadcast_to(dist[:, None], (dist.shape[0], LANES))
 
-    tp_blocks = []
-    for j in range(tp_count):
-        lead, at = j // (near * far), j // near % far
-        tp_blocks.append([(lead * far + (at - f) % far) * near + j % near for f in range(far)])
     sp_blocks = ring_tables(sp_count)[2] if in_ring else [[0]] * sp_count
-    blocks_at = len(sp_blocks[0])
-    table = jnp.asarray(
-        [[sp_blocks[s] + tp_blocks[j] for j in range(tp_count)] for s in range(sp_count)],
-        jnp.int32,
-    ).reshape(sp_count * tp_count, -1)
-    table = lax.dynamic_index_in_dim(table, lax.axis_index(("sp", "tp")), keepdims=False)
+    table = jnp.asarray(sp_blocks, jnp.int32)
+    table = lax.dynamic_index_in_dim(table, lax.axis_index("sp"), keepdims=False)
 
     states = (prev_rows, tokens)
     normed = kernel(
@@ -327,7 +358,7 @@
         out_rows = rows - tail
         pairs = pair_chunks[n]
         centred, stats = kernel(
-            functools.partial(gated_conv_body, n, tap_count, tail),
+            functools.partial(gated_conv_body, n, tap_count, tail, in_ring),
             (
                 jax.ShapeDtypeStruct((out_rows, width), narrow),
                 jax.ShapeDtypeStruct((2, round_up(out_rows, LANES)), wide),
@@ -340,14 +371,17 @@
             ],
         )(table, normed, dist, conv_taps, *pairs)
         far_centred = far_values(centred)
-        all_stats = lax.all_gather(stats, "tp")
+        all_stats = [stats]
+        for place in range(1, tp_count):
+            steps = group_pairs(tp_count, near, far, place % near, place // near)
+            all_stats.append(lax.ppermute(stats, "tp", steps))
         pieces = out_pieces[n]
         share = kernel(
-            functools.partial(project_body, n, far, out_slots[n], blocks_at),
+            functools.partial(project_body, n, near, far, out_slots[n]),
             jax.ShapeDtypeStruct((out_rows, model_width), narrow),
-            [in_smem()] + [in_vmem()] * (3 + far - 1 + far + len(pieces)),
+            [in_smem()] + [in_vmem()] * (2 + far - 1 + tp_count + far + len(pieces)),
             [pltpu.VMEM((far, out_rows, width), narrow)],
-        )(table, all_stats, norm_gain, norm_shift, *far_norm, *far_centred, *pieces)
+        )(table, norm_gain, norm_shift, *far_norm, *all_stats, *far_centred, *pieces)
         shares = [share]
         for _ in range(1, near):
             shares.append(lax.ppermute(shares[-1], "tp", near_pairs))

time: 153 us -> 142 us (0.928)
  blocking collectives: 19.9 us -> 0 us
  starting transfers between devices: 57 us -> 66.4 us
    all_gather x2 -> x0, blocking collectives: 19.9 us -> none  [on_device(): all_stats = lax.all_gather(stats, 'tp')]
    ppermute x16 -> x12, waiting for transfers between devices: 32.6 us -> 16.1 us  [ring_gathered(): ahead = lax.ppermute(ahead, 'sp', forward)]
    ppermute x1 -> x7, waiting for transfers between devices: 0.01 us -> 13.4 us  [the longest x6 12 us: on_device(): all_stats.append(lax.ppermute(stats, 'tp', steps))]
    ppermute x12, waiting for transfers between devices: 7.79 us -> 12 us  [ring_gathered(): behind = lax.ppermute(behind, 'sp', backward)]
    ppermute x16 -> x12, starting transfers between devices: 22.6 us -> 26.4 us  [ring_gathered(): ahead = lax.ppermute(ahead, 'sp', forward)]
    ppermute x12, starting transfers between devices: 13.3 us -> 16.7 us  [ring_gathered(): behind = lax.ppermute(behind, 'sp', backward)]
    ppermute x1 -> x7, starting transfers between devices: 2.12 us -> 5.46 us  [the longest x6 3.11 us: on_device(): all_stats.append(lax.ppermute(stats, 'tp', steps))]
    ppermute x18 -> x12, starting transfers between devices: 16.7 us -> 14.1 us  [far_values(): values.append(lax.ppermute(values[-1], 'tp', far_pairs))]
  transfers between devices with their start and end apart: 50 -> 46, of which waited for: 14 -> 17; matrix products, arithmetic and copies ran while one was open for 3% -> 1% of each run, Pallas kernels for 6% -> 7%
where the time goes in v1:
time: 142 us; the launch traced here: 141 us
  starting transfers between devices  66.4 us (47%)
  waiting for transfers between devices  48.1 us (34%)
  Pallas kernels  18 us (13%)
  local copies, waits for them, and re-layouts  7.46 us (5%)
    ppermute x12, starting transfers between devices, ring_gathered(): ahead = lax.ppermute(ahead, 'sp', forward)  26.4 us
    ppermute x12, starting transfers between devices, ring_gathered(): behind = lax.ppermute(behind, 'sp', backward)  16.7 us
    ppermute x12, waiting for transfers between devices, ring_gathered(): ahead = lax.ppermute(ahead, 'sp', forward)  16.1 us
    ppermute x12, starting transfers between devices, far_values(): values.append(lax.ppermute(values[-1], 'tp', far_pairs))  14.1 us
    ppermute x12, waiting for transfers between devices, ring_gathered(): behind = lax.ppermute(behind, 'sp', backward)  12 us
    ppermute x6, waiting for transfers between devices, on_device(): all_stats.append(lax.ppermute(stats, 'tp', steps))  12 us
    pallas_call x2, Pallas kernels, on_device(): kernel(functools.partial(gated_conv_body, n, tap_count, tail, in_ring), (...  7.92 us
    unnamed x29, local copies, waits for them, and re-layouts  6.6 us
  transfers between devices with their start and end apart: 46, of which 17 were waited for; matrix products, arithmetic and copies ran while one was open for 1% of the time, Pallas kernels for 7%

profile of v1, /device:TPU:0, one launch (start us, length us, event | category | flops | bytes accessed | tf_op | source)
XLA Modules:
  0.0 141.2 jit_solution(3848662114859879834)
XLA Ops:
  2.3 3.0 %collective-permute-start.4 = (bf16[2,256,256]{2,1,0:T(8,128)(2,1)S(1)}, bf16[2,256,256]{2,1,0:T(8,128)(2,1)S(1)}, u32[]{:S(2)}, u32[]{:S(2)}) collective-permute-start(bf16[2,256,256]{2,1,0:T(8,128)(2,1)S(1)} %shard_map.102.refs_0_), channel_id=1, source_target_pairs={{8,0},{16,8},{24,16},{28,24},{20,28},{12,20},{4,12},{0,4},{9,1},{1... | collective-permute-start | bytes 786440 | tf_op jit(solution)/shard_map/ppermute | solution.py:266
  5.5 2.0 %collective-permute-start.16 = (bf16[2,256,256]{2,1,0:T(8,128)(2,1)}, bf16[2,256,256]{2,1,0:T(8,128)(2,1)S(1)}, u32[]{:S(2)}, u32[]{:S(2)}) collective-permute-start(bf16[2,256,256]{2,1,0:T(8,128)(2,1)} %refs_7_.3), channel_id=1, source_target_pairs={{0,8},{8,16},{16,24},{24,28},{28,20},{20,12},{12,4},{4,0},{1,9},{9... | collective-permute-start | bytes 786440 | tf_op jit(solution)/shard_map/ppermute | solution.py:265
  7.5 5.1 %collective-permute-done.4.refs_2_ = bf16[2,256,256]{2,1,0:T(8,128)(2,1)S(1)} collective-permute-done((bf16[2,256,256]{2,1,0:T(8,128)(2,1)S(1)}, bf16[2,256,256]{2,1,0:T(8,128)(2,1)S(1)}, u32[]{:S(2)}, u32[]{:S(2)}) %collective-permute-start.4) | collective-permute-done | bytes 262176 | tf_op jit(solution)/shard_map/ppermute | solution.py:266
  12.5 1.9 %collective-permute-start.6 = (bf16[2,256,256]{2,1,0:T(8,128)(2,1)S(1)}, bf16[2,256,256]{2,1,0:T(8,128)(2,1)S(1)}, u32[]{:S(2)}, u32[]{:S(2)}) collective-permute-start(bf16[2,256,256]{2,1,0:T(8,128)(2,1)S(1)} %collective-permute-done.4.refs_2_), channel_id=1, source_target_pairs={{8,0},{16,8},{24,16},{28,24},{20,28},{12,20},{4,12},{0,4},{9,1},{1... | collective-permute-start | bytes 786440 | tf_op jit(solution)/shard_map/ppermute | solution.py:266
  15.2 3.5 %collective-permute-start.2 = (s32[64]{0:T(128)S(1)}, s32[64]{0:T(128)S(1)}, u32[]{:S(2)}, u32[]{:S(2)}) collective-permute-start(s32[64]{0:T(128)S(1)} %slice_add_fusion), channel_id=1, source_target_pairs={{0,4},{4,8},{8,12},{12,16},{16,20},{20,24},{24,28},{1,5},{5,9},{9,... | collective-permute-start | bytes 776 | tf_op jit(solution)/shard_map/ppermute | solution.py:337
  25.4 1.7 %collective-permute-start.5 = (bf16[2,256,256]{2,1,0:T(8,128)(2,1)S(1)}, bf16[2,256,256]{2,1,0:T(8,128)(2,1)S(1)}, u32[]{:S(2)}, u32[]{:S(2)}) collective-permute-start(bf16[2,256,256]{2,1,0:T(8,128)(2,1)S(1)} %collective-permute-done.3.refs_1_), channel_id=1, source_target_pairs={{0,8},{8,16},{16,24},{24,28},{28,20},{20,12},{12,4},{4,0},{1,9},{9... | collective-permute-start | bytes 786440 | tf_op jit(solution)/shard_map/ppermute | solution.py:265
  27.8 2.4 %collective-permute-start = (bf16[64,2048]{1,0:T(8,128)(2,1)S(1)}, bf16[64,2048]{1,0:T(8,128)(2,1)S(1)}, u32[]{:S(2)}, u32[]{:S(2)}) collective-permute-start(bf16[64,2048]{1,0:T(8,128)(2,1)S(1)} %get-tuple-element.14), channel_id=1, source_target_pairs={{0,4},{4,8},{8,12},{12,16},{16,20},{20,24},{24,28},{1,5},{5,9},{9,... | collective-permute-start | bytes 786440 | tf_op jit(solution)/shard_map/ppermute | solution.py:338
  32.9 2.0 %collective-permute-start.22 = (bf16[2,256,256]{2,1,0:T(8,128)(2,1)S(1)}, bf16[2,256,256]{2,1,0:T(8,128)(2,1)S(1)}, u32[]{:S(2)}, u32[]{:S(2)}) collective-permute-start(bf16[2,256,256]{2,1,0:T(8,128)(2,1)S(1)} %collective-permute-done.18.refs_11_), channel_id=1, source_target_pairs={{8,0},{16,8},{24,16},{28,24},{20,28},{12,20},{4,12},{0,4},{9,1},{1... | collective-permute-start | bytes 786440 | tf_op jit(solution)/shard_map/ppermute | solution.py:266
  38.4 1.6 %collective-permute-done.20.refs_13_ = bf16[2,256,256]{2,1,0:T(8,128)(2,1)S(1)} collective-permute-done((bf16[2,256,256]{2,1,0:T(8,128)(2,1)S(1)}, bf16[2,256,256]{2,1,0:T(8,128)(2,1)S(1)}, u32[]{:S(2)}, u32[]{:S(2)}) %collective-permute-start.20) | collective-permute-done | bytes 262176 | tf_op jit(solution)/shard_map/ppermute | solution.py:265
  46.4 2.5 %collective-permute-start.26 = (bf16[2,256,256]{2,1,0:T(8,128)(2,1)S(1)}, bf16[2,256,256]{2,1,0:T(8,128)(2,1)S(1)}, u32[]{:S(2)}, u32[]{:S(2)}) collective-permute-start(bf16[2,256,256]{2,1,0:T(8,128)(2,1)S(1)} %collective-permute-done.22.refs_15_), channel_id=1, source_target_pairs={{8,0},{16,8},{24,16},{28,24},{20,28},{12,20},{4,12},{0,4},{9,1},{1... | collective-permute-start | bytes 786440 | tf_op jit(solution)/shard_map/ppermute | solution.py:266
  50.1 2.5 %collective-permute-start.10 = (bf16[256,256]{1,0:T(8,128)(2,1)S(1)}, bf16[256,256]{1,0:T(8,128)(2,1)S(1)}, u32[]{:S(2)}, u32[]{:S(2)}) collective-permute-start(bf16[256,256]{1,0:T(8,128)(2,1)S(1)} %slice_bitcast_fusion.4), channel_id=1, source_target_pairs={{8,0},{16,8},{24,16},{28,24},{20,28},{12,20},{4,12},{0,4},{9,1},{1... | collective-permute-start | bytes 393224 | tf_op jit(solution)/shard_map/ppermute | solution.py:266
  52.6 3.6 %collective-permute-start.9 = (bf16[256,256]{1,0:T(8,128)(2,1)S(1)}, bf16[256,256]{1,0:T(8,128)(2,1)S(1)}, u32[]{:S(2)}, u32[]{:S(2)}) collective-permute-start(bf16[256,256]{1,0:T(8,128)(2,1)S(1)} %slice_bitcast_fusion.5), channel_id=1, source_target_pairs={{0,8},{8,16},{16,24},{24,28},{28,20},{20,12},{12,4},{4,0},{1,9},{9... | collective-permute-start | bytes 393224 | tf_op jit(solution)/shard_map/ppermute | solution.py:265
  57.6 5.0 %collective-permute-start.28 = (bf16[256,256]{1,0:T(8,128)(2,1)S(1)}, bf16[256,256]{1,0:T(8,128)(2,1)S(1)}, u32[]{:S(2)}, u32[]{:S(2)}) collective-permute-start(bf16[256,256]{1,0:T(8,128)(2,1)S(1)} %slice_bitcast_fusion.3), channel_id=1, source_target_pairs={{0,8},{8,16},{16,24},{24,28},{28,20},{20,12},{12,4},{4,0},{1,9},{9... | collective-permute-start | bytes 393224 | tf_op jit(solution)/shard_map/ppermute | solution.py:265
  65.6 4.1 %shard_map.103 = (bf16[416,256]{1,0:T(8,128)(2,1)S(1)}, f32[2,512]{1,0:T(2,128)S(1)}) custom-call(s32[8]{0:T(128)S(1)} %dynamic-slice_bitcast_fusion.table_ref, bf16[448,2048]{1,0:T(8,128)(2,1)S(1)} %shard_map.101.normed_ref, s32[416,128]{1,0:T(8,128)S(1)} %broadcast_in_dim.2.dist_ref, f32[2,31,256]{2,1,0:T(8,128)S(1)} %copy.11.taps_ref, ...), custom_call_target="tpu_custom_call" | custom-call | tf_op jit(solution)/shard_map/pallas_call | solution.py:360
  74.2 7.8 %collective-permute-done.12.refs_3_ = f32[2,512]{1,0:T(2,128)S(1)} collective-permute-done((f32[2,512]{1,0:T(2,128)S(1)}, f32[2,512]{1,0:T(2,128)S(1)}, u32[]{:S(2)}, u32[]{:S(2)}) %collective-permute-start.12) | collective-permute-done | bytes 4128 | tf_op jit(solution)/shard_map/ppermute | solution.py:377
  82.0 3.0 %collective-permute-done.13.refs_4_ = f32[2,512]{1,0:T(2,128)S(1)} collective-permute-done((f32[2,512]{1,0:T(2,128)S(1)}, f32[2,512]{1,0:T(2,128)S(1)}, u32[]{:S(2)}, u32[]{:S(2)}) %collective-permute-start.13) | collective-permute-done | bytes 4128 | tf_op jit(solution)/shard_map/ppermute | solution.py:377
  85.0 2.8 %shard_map.104.refs_3_ = bf16[416,2048]{1,0:T(8,128)(2,1)S(1)} custom-call(s32[8]{0:T(128)S(1)} %dynamic-slice_bitcast_fusion.table_ref, f32[2,256]{1,0:T(2,128)S(1)} %copy-done.9, f32[2,256]{1,0:T(2,128)S(1)} %copy-done.11, f32[2,2,256]{2,1,0:T(2,128)S(1)} %collective-permute-done.1.refs_0_, f32[2,512]{1,0:T(2,128)S(1)} %get-tuple-element.16.refs_1_, ...), custom_call_target="tpu_custom_call" | custom-call | tf_op jit(solution)/shard_map/pallas_call | solution.py:379
  87.9 3.5 %collective-permute-start.31 = (bf16[2,256,256]{2,1,0:T(8,128)(2,1)S(1)}, bf16[2,256,256]{2,1,0:T(8,128)(2,1)S(1)}, u32[]{:S(2)}, u32[]{:S(2)}) collective-permute-start(bf16[2,256,256]{2,1,0:T(8,128)(2,1)S(1)} %get-tuple-element.20.refs_0_), channel_id=1, source_target_pairs={{0,8},{8,16},{16,24},{24,28},{28,20},{20,12},{12,4},{4,0},{1,9},{9... | collective-permute-start | bytes 786440 | tf_op jit(solution)/shard_map/ppermute | solution.py:265
  91.4 6.2 %collective-permute-done.31.refs_1_ = bf16[2,256,256]{2,1,0:T(8,128)(2,1)S(1)} collective-permute-done((bf16[2,256,256]{2,1,0:T(8,128)(2,1)S(1)}, bf16[2,256,256]{2,1,0:T(8,128)(2,1)S(1)}, u32[]{:S(2)}, u32[]{:S(2)}) %collective-permute-start.31) | collective-permute-done | bytes 262176 | tf_op jit(solution)/shard_map/ppermute | solution.py:265
  97.6 2.5 %collective-permute-start.33 = (bf16[2,256,256]{2,1,0:T(8,128)(2,1)S(1)}, bf16[2,256,256]{2,1,0:T(8,128)(2,1)S(1)}, u32[]{:S(2)}, u32[]{:S(2)}) collective-permute-start(bf16[2,256,256]{2,1,0:T(8,128)(2,1)S(1)} %collective-permute-done.31.refs_1_), channel_id=1, source_target_pairs={{0,8},{8,16},{16,24},{24,28},{28,20},{20,12},{12,4},{4,0},{1,9},{9... | collective-permute-start | bytes 786440 | tf_op jit(solution)/shard_map/ppermute | solution.py:265
  100.4 5.0 %collective-permute-done.33.refs_3_ = bf16[2,256,256]{2,1,0:T(8,128)(2,1)S(1)} collective-permute-done((bf16[2,256,256]{2,1,0:T(8,128)(2,1)S(1)}, bf16[2,256,256]{2,1,0:T(8,128)(2,1)S(1)}, u32[]{:S(2)}, u32[]{:S(2)}) %collective-permute-start.33) | collective-permute-done | bytes 262176 | tf_op jit(solution)/shard_map/ppermute | solution.py:265
  105.4 2.5 %collective-permute-start.35 = (bf16[2,256,256]{2,1,0:T(8,128)(2,1)S(1)}, bf16[2,256,256]{2,1,0:T(8,128)(2,1)S(1)}, u32[]{:S(2)}, u32[]{:S(2)}) collective-permute-start(bf16[2,256,256]{2,1,0:T(8,128)(2,1)S(1)} %collective-permute-done.33.refs_3_), channel_id=1, source_target_pairs={{0,8},{8,16},{16,24},{24,28},{28,20},{20,12},{12,4},{4,0},{1,9},{9... | collective-permute-start | bytes 786440 | tf_op jit(solution)/shard_map/ppermute | solution.py:265
  109.1 3.3 %collective-permute-done.35.refs_5_ = bf16[2,256,256]{2,1,0:T(8,128)(2,1)S(1)} collective-permute-done((bf16[2,256,256]{2,1,0:T(8,128)(2,1)S(1)}, bf16[2,256,256]{2,1,0:T(8,128)(2,1)S(1)}, u32[]{:S(2)}, u32[]{:S(2)}) %collective-permute-start.35) | collective-permute-done | bytes 262176 | tf_op jit(solution)/shard_map/ppermute | solution.py:265
  112.4 2.5 %collective-permute-start.37 = (bf16[256,256]{1,0:T(8,128)(2,1)S(1)}, bf16[256,256]{1,0:T(8,128)(2,1)S(1)}, u32[]{:S(2)}, u32[]{:S(2)}) collective-permute-start(bf16[256,256]{1,0:T(8,128)(2,1)S(1)} %slice_bitcast_fusion.2), channel_id=1, source_target_pairs={{0,8},{8,16},{16,24},{24,28},{28,20},{20,12},{12,4},{4,0},{1,9},{9... | collective-permute-start | bytes 393224 | tf_op jit(solution)/shard_map/ppermute | solution.py:265
  114.9 1.9 %collective-permute-done.36.refs_6_ = bf16[2,256,256]{2,1,0:T(8,128)(2,1)S(1)} collective-permute-done((bf16[2,256,256]{2,1,0:T(8,128)(2,1)S(1)}, bf16[2,256,256]{2,1,0:T(8,128)(2,1)S(1)}, u32[]{:S(2)}, u32[]{:S(2)}) %collective-permute-start.36) | collective-permute-done | bytes 262176 | tf_op jit(solution)/shard_map/ppermute | solution.py:266
  117.8 2.2 %collective-permute-start.43 = (bf16[256,256]{1,0:T(8,128)(2,1)S(1)}, bf16[256,256]{1,0:T(8,128)(2,1)S(1)}, u32[]{:S(2)}, u32[]{:S(2)}) collective-permute-start(bf16[256,256]{1,0:T(8,128)(2,1)S(1)} %slice_bitcast_fusion), channel_id=1, source_target_pairs={{8,0},{16,8},{24,16},{28,24},{20,28},{12,20},{4,12},{0,4},{9,1},{1... | collective-permute-start | bytes 393224 | tf_op jit(solution)/shard_map/ppermute | solution.py:266
  122.1 3.8 %shard_map.106 = (bf16[384,256]{1,0:T(8,128)(2,1)S(1)}, f32[2,384]{1,0:T(2,128)S(1)}) custom-call(s32[8]{0:T(128)S(1)} %dynamic-slice_bitcast_fusion.table_ref, bf16[416,2048]{1,0:T(8,128)(2,1)S(1)} %get-tuple-element.19.normed_ref, s32[416,128]{1,0:T(8,128)S(1)} %broadcast_in_dim.2.dist_ref, f32[2,31,256]{2,1,0:T(8,128)S(1)} %copy.11.taps_ref, ...), custom_call_target="tpu_custom_call" | custom-call | tf_op jit(solution)/shard_map/pallas_call | solution.py:360
  126.4 1.7 %collective-permute-start.44 = (bf16[256,256]{1,0:T(8,128)(2,1)S(1)}, bf16[256,256]{1,0:T(8,128)(2,1)S(1)}, u32[]{:S(2)}, u32[]{:S(2)}) collective-permute-start(bf16[256,256]{1,0:T(8,128)(2,1)S(1)} %collective-permute-done.43.refs_21_), channel_id=1, source_target_pairs={{0,2},{1,3},{2,0},{3,1},{4,6},{5,7},{6,4},{7,5},{8,10},{9,11},{10,... | collective-permute-start | bytes 393224 | tf_op jit(solution)/shard_map/ppermute | solution.py:307
  129.9 3.2 %collective-permute-done.44.refs_22_ = bf16[256,256]{1,0:T(8,128)(2,1)S(1)} collective-permute-done((bf16[256,256]{1,0:T(8,128)(2,1)S(1)}, bf16[256,256]{1,0:T(8,128)(2,1)S(1)}, u32[]{:S(2)}, u32[]{:S(2)}) %collective-permute-start.44) | collective-permute-done | bytes 131104 | tf_op jit(solution)/shard_map/ppermute | solution.py:307
  133.2 2.6 %shard_map.107.refs_1_ = bf16[384,2048]{1,0:T(8,128)(2,1)S(1)} custom-call(s32[8]{0:T(128)S(1)} %dynamic-slice_bitcast_fusion.table_ref, f32[2,256]{1,0:T(2,128)S(1)} %copy-done.9, f32[2,256]{1,0:T(2,128)S(1)} %copy-done.11, f32[2,2,256]{2,1,0:T(2,128)S(1)} %collective-permute-done.1.refs_0_, f32[2,384]{1,0:T(2,128)S(1)} %get-tuple-element.21.refs_1_, ...), custom_call_target="tpu_custom_call" | custom-call | tf_op jit(solution)/shard_map/pallas_call | solution.py:379
  136.0 3.3 %collective-permute-done.45.refs_2_ = bf16[384,2048]{1,0:T(8,128)(2,1)S(1)} collective-permute-done((bf16[384,2048]{1,0:T(8,128)(2,1)S(1)}, bf16[384,2048]{1,0:T(8,128)(2,1)S(1)}, u32[]{:S(2)}, u32[]{:S(2)}) %collective-permute-start.45) | collective-permute-done | bytes 1572896 | tf_op jit(solution)/shard_map/ppermute | solution.py:387
  139.3 1.9 %shard_map.108 = bf16[384,2048]{1,0:T(8,128)(2,1)} custom-call(bf16[416,2048]{1,0:T(8,128)(2,1)S(1)} %get-tuple-element.18.refs_0_, bf16[384,2048]{1,0:T(8,128)(2,1)S(1)} %shard_map.107.refs_1_, bf16[384,2048]{1,0:T(8,128)(2,1)S(1)} %collective-permute-done.45.refs_2_), custom_call_target="tpu_custom_call" | custom-call | tf_op jit(solution)/shard_map/pallas_call | solution.py:391
  (110 shorter events, 40.3 us)
Async XLA Ops:
  2.3 10.3 %collective-permute-start.4 = (bf16[2,256,256]{2,1,0:T(8,128)(2,1)S(1)}, bf16[2,256,256]{2,1,0:T(8,128)(2,1)S(1)}, u32[]{:S(2)}, u32[]{:S(2)}) collective-permute-start(bf16[2,256,256]{2,1,0:T(8,128)(2,1)S(1)} %shard_map.102.refs_0_), channel_id=1, source_target_pairs={{8,0},{16,8},{24,16},{28,24},{20,28},{12,20},{4,12},{0,4},{9,1},{1... | collective-permute-start | bytes 786440 | tf_op jit(solution)/shard_map/ppermute | solution.py:266
  5.3 20.1 %collective-permute-start.3 = (bf16[2,256,256]{2,1,0:T(8,128)(2,1)S(1)}, bf16[2,256,256]{2,1,0:T(8,128)(2,1)S(1)}, u32[]{:S(2)}, u32[]{:S(2)}) collective-permute-start(bf16[2,256,256]{2,1,0:T(8,128)(2,1)S(1)} %shard_map.102.refs_0_), channel_id=1, source_target_pairs={{0,8},{8,16},{16,24},{24,28},{28,20},{20,12},{12,4},{4,0},{1,9},{9... | collective-permute-start | bytes 786440 | tf_op jit(solution)/shard_map/ppermute | solution.py:265
  5.5 24.8 %collective-permute-start.16 = (bf16[2,256,256]{2,1,0:T(8,128)(2,1)}, bf16[2,256,256]{2,1,0:T(8,128)(2,1)S(1)}, u32[]{:S(2)}, u32[]{:S(2)}) collective-permute-start(bf16[2,256,256]{2,1,0:T(8,128)(2,1)} %refs_7_.3), channel_id=1, source_target_pairs={{0,8},{8,16},{16,24},{24,28},{28,20},{20,12},{12,4},{4,0},{1,9},{9... | collective-permute-start | bytes 786440 | tf_op jit(solution)/shard_map/ppermute | solution.py:265
  7.4 25.5 %collective-permute-start.18 = (bf16[2,256,256]{2,1,0:T(8,128)(2,1)}, bf16[2,256,256]{2,1,0:T(8,128)(2,1)S(1)}, u32[]{:S(2)}, u32[]{:S(2)}) collective-permute-start(bf16[2,256,256]{2,1,0:T(8,128)(2,1)} %refs_7_.3), channel_id=1, source_target_pairs={{8,0},{16,8},{24,16},{28,24},{20,28},{12,20},{4,12},{0,4},{9,1},{1... | collective-permute-start | bytes 786440 | tf_op jit(solution)/shard_map/ppermute | solution.py:266
  12.5 18.9 %collective-permute-start.6 = (bf16[2,256,256]{2,1,0:T(8,128)(2,1)S(1)}, bf16[2,256,256]{2,1,0:T(8,128)(2,1)S(1)}, u32[]{:S(2)}, u32[]{:S(2)}) collective-permute-start(bf16[2,256,256]{2,1,0:T(8,128)(2,1)S(1)} %collective-permute-done.4.refs_2_), channel_id=1, source_target_pairs={{8,0},{16,8},{24,16},{28,24},{20,28},{12,20},{4,12},{0,4},{9,1},{1... | collective-permute-start | bytes 786440 | tf_op jit(solution)/shard_map/ppermute | solution.py:266
  15.2 8.6 %collective-permute-start.2 = (s32[64]{0:T(128)S(1)}, s32[64]{0:T(128)S(1)}, u32[]{:S(2)}, u32[]{:S(2)}) collective-permute-start(s32[64]{0:T(128)S(1)} %slice_add_fusion), channel_id=1, source_target_pairs={{0,4},{4,8},{8,12},{12,16},{16,20},{20,24},{24,28},{1,5},{5,9},{9,... | collective-permute-start | bytes 776 | tf_op jit(solution)/shard_map/ppermute | solution.py:337
  25.4 9.5 %collective-permute-start.5 = (bf16[2,256,256]{2,1,0:T(8,128)(2,1)S(1)}, bf16[2,256,256]{2,1,0:T(8,128)(2,1)S(1)}, u32[]{:S(2)}, u32[]{:S(2)}) collective-permute-start(bf16[2,256,256]{2,1,0:T(8,128)(2,1)S(1)} %collective-permute-done.3.refs_1_), channel_id=1, source_target_pairs={{0,8},{8,16},{16,24},{24,28},{28,20},{20,12},{12,4},{4,0},{1,9},{9... | collective-permute-start | bytes 786440 | tf_op jit(solution)/shard_map/ppermute | solution.py:265
  27.8 9.0 %collective-permute-start = (bf16[64,2048]{1,0:T(8,128)(2,1)S(1)}, bf16[64,2048]{1,0:T(8,128)(2,1)S(1)}, u32[]{:S(2)}, u32[]{:S(2)}) collective-permute-start(bf16[64,2048]{1,0:T(8,128)(2,1)S(1)} %get-tuple-element.14), channel_id=1, source_target_pairs={{0,4},{4,8},{8,12},{12,16},{16,20},{20,24},{24,28},{1,5},{5,9},{9,... | collective-permute-start | bytes 786440 | tf_op jit(solution)/shard_map/ppermute | solution.py:338
  30.2 9.8 %collective-permute-start.20 = (bf16[2,256,256]{2,1,0:T(8,128)(2,1)S(1)}, bf16[2,256,256]{2,1,0:T(8,128)(2,1)S(1)}, u32[]{:S(2)}, u32[]{:S(2)}) collective-permute-start(bf16[2,256,256]{2,1,0:T(8,128)(2,1)S(1)} %collective-permute-done.16.refs_9_), channel_id=1, source_target_pairs={{0,8},{8,16},{16,24},{24,28},{28,20},{20,12},{12,4},{4,0},{1,9},{9... | collective-permute-start | bytes 786440 | tf_op jit(solution)/shard_map/ppermute | solution.py:265
  31.4 10.7 %collective-permute-start.8 = (bf16[2,256,256]{2,1,0:T(8,128)(2,1)S(1)}, bf16[2,256,256]{2,1,0:T(8,128)(2,1)S(1)}, u32[]{:S(2)}, u32[]{:S(2)}) collective-permute-start(bf16[2,256,256]{2,1,0:T(8,128)(2,1)S(1)} %collective-permute-done.6.refs_4_), channel_id=1, source_target_pairs={{8,0},{16,8},{24,16},{28,24},{20,28},{12,20},{4,12},{0,4},{9,1},{1... | collective-permute-start | bytes 786440 | tf_op jit(solution)/shard_map/ppermute | solution.py:266
  32.9 12.0 %collective-permute-start.22 = (bf16[2,256,256]{2,1,0:T(8,128)(2,1)S(1)}, bf16[2,256,256]{2,1,0:T(8,128)(2,1)S(1)}, u32[]{:S(2)}, u32[]{:S(2)}) collective-permute-start(bf16[2,256,256]{2,1,0:T(8,128)(2,1)S(1)} %collective-permute-done.18.refs_11_), channel_id=1, source_target_pairs={{8,0},{16,8},{24,16},{28,24},{20,28},{12,20},{4,12},{0,4},{9,1},{1... | collective-permute-start | bytes 786440 | tf_op jit(solution)/shard_map/ppermute | solution.py:266
  34.9 11.5 %collective-permute-start.7 = (bf16[2,256,256]{2,1,0:T(8,128)(2,1)S(1)}, bf16[2,256,256]{2,1,0:T(8,128)(2,1)S(1)}, u32[]{:S(2)}, u32[]{:S(2)}) collective-permute-start(bf16[2,256,256]{2,1,0:T(8,128)(2,1)S(1)} %collective-permute-done.5.refs_3_), channel_id=1, source_target_pairs={{0,8},{8,16},{16,24},{24,28},{28,20},{20,12},{12,4},{4,0},{1,9},{9... | collective-permute-start | bytes 786440 | tf_op jit(solution)/shard_map/ppermute | solution.py:265
  36.9 12.0 %collective-permute-start.15 = (bf16[2,256,256]{2,1,0:T(8,128)(2,1)S(1)}, bf16[2,256,256]{2,1,0:T(8,128)(2,1)S(1)}, u32[]{:S(2)}, u32[]{:S(2)}) collective-permute-start(bf16[2,256,256]{2,1,0:T(8,128)(2,1)S(1)} %copy-done.6), channel_id=1, source_target_pairs={{0,2},{1,3},{2,0},{3,1},{4,6},{5,7},{6,4},{7,5},{8,10},{9,11},{10,... | collective-permute-start | bytes 786440 | tf_op jit(solution)/shard_map/ppermute | solution.py:307
  40.0 10.1 %collective-permute-start.17 = (bf16[2,256,256]{2,1,0:T(8,128)(2,1)S(1)}, bf16[2,256,256]{2,1,0:T(8,128)(2,1)S(1)}, u32[]{:S(2)}, u32[]{:S(2)}) collective-permute-start(bf16[2,256,256]{2,1,0:T(8,128)(2,1)S(1)} %collective-permute-done.16.refs_9_), channel_id=1, source_target_pairs={{0,2},{1,3},{2,0},{3,1},{4,6},{5,7},{6,4},{7,5},{8,10},{9,11},{10,... | collective-permute-start | bytes 786440 | tf_op jit(solution)/shard_map/ppermute | solution.py:307
  42.1 10.5 %collective-permute-start.24 = (bf16[2,256,256]{2,1,0:T(8,128)(2,1)S(1)}, bf16[2,256,256]{2,1,0:T(8,128)(2,1)S(1)}, u32[]{:S(2)}, u32[]{:S(2)}) collective-permute-start(bf16[2,256,256]{2,1,0:T(8,128)(2,1)S(1)} %collective-permute-done.20.refs_13_), channel_id=1, source_target_pairs={{0,8},{8,16},{16,24},{24,28},{28,20},{20,12},{12,4},{4,0},{1,9},{9... | collective-permute-start | bytes 786440 | tf_op jit(solution)/shard_map/ppermute | solution.py:265
  44.9 11.3 %collective-permute-start.19 = (bf16[2,256,256]{2,1,0:T(8,128)(2,1)S(1)}, bf16[2,256,256]{2,1,0:T(8,128)(2,1)S(1)}, u32[]{:S(2)}, u32[]{:S(2)}) collective-permute-start(bf16[2,256,256]{2,1,0:T(8,128)(2,1)S(1)} %collective-permute-done.18.refs_11_), channel_id=1, source_target_pairs={{0,2},{1,3},{2,0},{3,1},{4,6},{5,7},{6,4},{7,5},{8,10},{9,11},{10,... | collective-permute-start | bytes 786440 | tf_op jit(solution)/shard_map/ppermute | solution.py:307
  46.4 11.2 %collective-permute-start.26 = (bf16[2,256,256]{2,1,0:T(8,128)(2,1)S(1)}, bf16[2,256,256]{2,1,0:T(8,128)(2,1)S(1)}, u32[]{:S(2)}, u32[]{:S(2)}) collective-permute-start(bf16[2,256,256]{2,1,0:T(8,128)(2,1)S(1)} %collective-permute-done.22.refs_15_), channel_id=1, source_target_pairs={{8,0},{16,8},{24,16},{28,24},{20,28},{12,20},{4,12},{0,4},{9,1},{1... | collective-permute-start | bytes 786440 | tf_op jit(solution)/shard_map/ppermute | solution.py:266
  48.9 20.8 %collective-permute-start.21 = (bf16[2,256,256]{2,1,0:T(8,128)(2,1)S(1)}, bf16[2,256,256]{2,1,0:T(8,128)(2,1)S(1)}, u32[]{:S(2)}, u32[]{:S(2)}) collective-permute-start(bf16[2,256,256]{2,1,0:T(8,128)(2,1)S(1)} %collective-permute-done.20.refs_13_), channel_id=1, source_target_pairs={{0,2},{1,3},{2,0},{3,1},{4,6},{5,7},{6,4},{7,5},{8,10},{9,11},{10,... | collective-permute-start | bytes 786440 | tf_op jit(solution)/shard_map/ppermute | solution.py:307
  50.1 12.5 %collective-permute-start.10 = (bf16[256,256]{1,0:T(8,128)(2,1)S(1)}, bf16[256,256]{1,0:T(8,128)(2,1)S(1)}, u32[]{:S(2)}, u32[]{:S(2)}) collective-permute-start(bf16[256,256]{1,0:T(8,128)(2,1)S(1)} %slice_bitcast_fusion.4), channel_id=1, source_target_pairs={{8,0},{16,8},{24,16},{28,24},{20,28},{12,20},{4,12},{0,4},{9,1},{1... | collective-permute-start | bytes 393224 | tf_op jit(solution)/shard_map/ppermute | solution.py:266
  52.6 11.2 %collective-permute-start.9 = (bf16[256,256]{1,0:T(8,128)(2,1)S(1)}, bf16[256,256]{1,0:T(8,128)(2,1)S(1)}, u32[]{:S(2)}, u32[]{:S(2)}) collective-permute-start(bf16[256,256]{1,0:T(8,128)(2,1)S(1)} %slice_bitcast_fusion.5), channel_id=1, source_target_pairs={{0,8},{8,16},{16,24},{24,28},{28,20},{20,12},{12,4},{4,0},{1,9},{9... | collective-permute-start | bytes 393224 | tf_op jit(solution)/shard_map/ppermute | solution.py:265
  56.2 15.6 %collective-permute-start.23 = (bf16[2,256,256]{2,1,0:T(8,128)(2,1)S(1)}, bf16[2,256,256]{2,1,0:T(8,128)(2,1)S(1)}, u32[]{:S(2)}, u32[]{:S(2)}) collective-permute-start(bf16[2,256,256]{2,1,0:T(8,128)(2,1)S(1)} %collective-permute-done.22.refs_15_), channel_id=1, source_target_pairs={{0,2},{1,3},{2,0},{3,1},{4,6},{5,7},{6,4},{7,5},{8,10},{9,11},{10,... | collective-permute-start | bytes 786440 | tf_op jit(solution)/shard_map/ppermute | solution.py:307
  57.6 13.4 %collective-permute-start.28 = (bf16[256,256]{1,0:T(8,128)(2,1)S(1)}, bf16[256,256]{1,0:T(8,128)(2,1)S(1)}, u32[]{:S(2)}, u32[]{:S(2)}) collective-permute-start(bf16[256,256]{1,0:T(8,128)(2,1)S(1)} %slice_bitcast_fusion.3), channel_id=1, source_target_pairs={{0,8},{8,16},{16,24},{24,28},{28,20},{20,12},{12,4},{4,0},{1,9},{9... | collective-permute-start | bytes 393224 | tf_op jit(solution)/shard_map/ppermute | solution.py:265
  62.6 22.4 %collective-permute-start.25 = (bf16[2,256,256]{2,1,0:T(8,128)(2,1)S(1)}, bf16[2,256,256]{2,1,0:T(8,128)(2,1)S(1)}, u32[]{:S(2)}, u32[]{:S(2)}) collective-permute-start(bf16[2,256,256]{2,1,0:T(8,128)(2,1)S(1)} %collective-permute-done.24.refs_17_), channel_id=1, source_target_pairs={{0,2},{1,3},{2,0},{3,1},{4,6},{5,7},{6,4},{7,5},{8,10},{9,11},{10,... | collective-permute-start | bytes 786440 | tf_op jit(solution)/shard_map/ppermute | solution.py:307
  63.8 21.1 %collective-permute-start.27 = (bf16[2,256,256]{2,1,0:T(8,128)(2,1)S(1)}, bf16[2,256,256]{2,1,0:T(8,128)(2,1)S(1)}, u32[]{:S(2)}, u32[]{:S(2)}) collective-permute-start(bf16[2,256,256]{2,1,0:T(8,128)(2,1)S(1)} %collective-permute-done.26.refs_19_), channel_id=1, source_target_pairs={{0,2},{1,3},{2,0},{3,1},{4,6},{5,7},{6,4},{7,5},{8,10},{9,11},{10,... | collective-permute-start | bytes 786440 | tf_op jit(solution)/shard_map/ppermute | solution.py:307
  69.7 15.3 %collective-permute-start.14 = (bf16[416,256]{1,0:T(8,128)(2,1)S(1)}, bf16[416,256]{1,0:T(8,128)(2,1)S(1)}, u32[]{:S(2)}, u32[]{:S(2)}) collective-permute-start(bf16[416,256]{1,0:T(8,128)(2,1)S(1)} %get-tuple-element.17.refs_5_), channel_id=1, source_target_pairs={{0,2},{1,3},{2,0},{3,1},{4,6},{5,7},{6,4},{7,5},{8,10},{9,11},{10,... | collective-permute-start | bytes 638984 | tf_op jit(solution)/shard_map/ppermute | solution.py:307
  71.0 14.0 %collective-permute-start.29 = (bf16[256,256]{1,0:T(8,128)(2,1)S(1)}, bf16[256,256]{1,0:T(8,128)(2,1)S(1)}, u32[]{:S(2)}, u32[]{:S(2)}) collective-permute-start(bf16[256,256]{1,0:T(8,128)(2,1)S(1)} %collective-permute-done.28.refs_21_), channel_id=1, source_target_pairs={{0,2},{1,3},{2,0},{3,1},{4,6},{5,7},{6,4},{7,5},{8,10},{9,11},{10,... | collective-permute-start | bytes 393224 | tf_op jit(solution)/shard_map/ppermute | solution.py:307
  72.9 9.0 %collective-permute-start.12 = (f32[2,512]{1,0:T(2,128)S(1)}, f32[2,512]{1,0:T(2,128)S(1)}, u32[]{:S(2)}, u32[]{:S(2)}) collective-permute-start(f32[2,512]{1,0:T(2,128)S(1)} %get-tuple-element.16.refs_1_), channel_id=1, source_target_pairs={{0,2},{1,3},{2,0},{3,1},{4,6},{5,7},{6,4},{7,5},{8,10},{9,11},{10,... | collective-permute-start | bytes 12296 | tf_op jit(solution)/shard_map/ppermute | solution.py:377
  87.9 32.2 %collective-permute-start.30 = (bf16[416,2048]{1,0:T(8,128)(2,1)S(1)}, bf16[416,2048]{1,0:T(8,128)(2,1)S(1)}, u32[]{:S(2)}, u32[]{:S(2)}) collective-permute-start(bf16[416,2048]{1,0:T(8,128)(2,1)S(1)} %shard_map.104.refs_3_), channel_id=1, source_target_pairs={{0,1},{1,0},{2,3},{3,2},{4,5},{5,4},{6,7},{7,6},{8,9},{9,8},{10,11... | collective-permute-start | bytes 5111816 | tf_op jit(solution)/shard_map/ppermute | solution.py:387
  87.9 9.7 %collective-permute-start.31 = (bf16[2,256,256]{2,1,0:T(8,128)(2,1)S(1)}, bf16[2,256,256]{2,1,0:T(8,128)(2,1)S(1)}, u32[]{:S(2)}, u32[]{:S(2)}) collective-permute-start(bf16[2,256,256]{2,1,0:T(8,128)(2,1)S(1)} %get-tuple-element.20.refs_0_), channel_id=1, source_target_pairs={{0,8},{8,16},{16,24},{24,28},{28,20},{20,12},{12,4},{4,0},{1,9},{9... | collective-permute-start | bytes 786440 | tf_op jit(solution)/shard_map/ppermute | solution.py:265
  91.4 8.9 %collective-permute-start.32 = (bf16[2,256,256]{2,1,0:T(8,128)(2,1)S(1)}, bf16[2,256,256]{2,1,0:T(8,128)(2,1)S(1)}, u32[]{:S(2)}, u32[]{:S(2)}) collective-permute-start(bf16[2,256,256]{2,1,0:T(8,128)(2,1)S(1)} %get-tuple-element.20.refs_0_), channel_id=1, source_target_pairs={{8,0},{16,8},{24,16},{28,24},{20,28},{12,20},{4,12},{0,4},{9,1},{1... | collective-permute-start | bytes 786440 | tf_op jit(solution)/shard_map/ppermute | solution.py:266
  100.4 8.7 %collective-permute-start.34 = (bf16[2,256,256]{2,1,0:T(8,128)(2,1)S(1)}, bf16[2,256,256]{2,1,0:T(8,128)(2,1)S(1)}, u32[]{:S(2)}, u32[]{:S(2)}) collective-permute-start(bf16[2,256,256]{2,1,0:T(8,128)(2,1)S(1)} %collective-permute-done.32.refs_2_), channel_id=1, source_target_pairs={{8,0},{16,8},{24,16},{28,24},{20,28},{12,20},{4,12},{0,4},{9,1},{1... | collective-permute-start | bytes 786440 | tf_op jit(solution)/shard_map/ppermute | solution.py:266
  112.4 9.0 %collective-permute-start.37 = (bf16[256,256]{1,0:T(8,128)(2,1)S(1)}, bf16[256,256]{1,0:T(8,128)(2,1)S(1)}, u32[]{:S(2)}, u32[]{:S(2)}) collective-permute-start(bf16[256,256]{1,0:T(8,128)(2,1)S(1)} %slice_bitcast_fusion.2), channel_id=1, source_target_pairs={{0,8},{8,16},{16,24},{24,28},{28,20},{20,12},{12,4},{4,0},{1,9},{9... | collective-permute-start | bytes 393224 | tf_op jit(solution)/shard_map/ppermute | solution.py:265
  (28 other events, 321.1 us)

commit v2 on v1

--- a/solution.py
+++ b/solution.py
@@ -15,6 +15,8 @@
 CONV_ROWS = 32
 RING_MOST = 8
 KERNEL_VMEM = 20 * 2**20
+PACK_FLOPS = 2 * 10**9
+PACK_BYTES = 8 * 10**6
 
 
 wide = jnp.float32
@@ -29,8 +31,8 @@
     return pl.BlockSpec(memory_space=pltpu.VMEM)
 
 
-def in_smem():
-    return pl.BlockSpec(memory_space=pltpu.SMEM)
+def in_hbm():
+    return pl.BlockSpec(memory_space=pl.ANY)
 
 
 def kernel(body, out_shape, in_specs, scratch_shapes=()):
@@ -60,55 +62,99 @@
         copy.wait()
 
 
-def pack_body(layer, halo, value_ref, gate_ref, *refs):
+def pack_body(layer, halo, near, value_ref, gate_ref, *refs):
     if halo == 0:
         pair_ref, sems = refs
         copied([value_ref.at[layer], gate_ref.at[layer]], [pair_ref.at[0], pair_ref.at[1]], sems)
         return
-    tokens_ref, gain_ref, shift_ref, pair_ref, tail_ref, norms_ref, sems = refs
-    rows = tokens_ref.shape[0]
+    docs_ref, tokens_ref, pair_ref, tail_ref, sems = refs
+    rows, model_width = tokens_ref.shape
+    span = round_up(halo, LANES)
+    docs = docs_ref[...].reshape(1, rows)[:, rows - span :] + 1
+    row = lax.broadcasted_iota(jnp.int32, (LANES, span), 0)
+    docs = jnp.where(row == 0, docs // 256, jnp.where(row == 1, docs % 256, 0))
+    docs = docs.astype(wide).T[span - halo :, :].astype(narrow)
+    part = halo // near
+    place = lax.axis_index("tp") % near
+    for other in range(near):
+
+        @pl.when(place == other)
+        def _(other=other):
+            tail_ref[:, model_width:] = docs[other * part : (other + 1) * part, :]
+
     copied(
         [
             value_ref.at[layer],
             gate_ref.at[layer],
-            tokens_ref.at[pl.ds(rows - halo, halo)],
-            gain_ref,
-            shift_ref,
+            tokens_ref.at[pl.ds(pl.multiple_of(rows - halo + place * part, HALO_ALIGN), part)],
         ],
-        [pair_ref.at[0], pair_ref.at[1], tail_ref, norms_ref.at[0], norms_ref.at[1]],
+        [pair_ref.at[0], pair_ref.at[1], tail_ref.at[:, pl.ds(0, model_width)]],
         sems,
     )
 
 
-def packed(layer, value_proj, gate_proj, halo=0, extra=()):
+def packed(layer, value_proj, gate_proj, halo=0, near=1, extra=()):
     shapes = [jax.ShapeDtypeStruct((2,) + value_proj.shape[1:], narrow)]
     if halo:
-        tokens, gain, _ = extra
-        shapes.append(jax.ShapeDtypeStruct((halo, tokens.shape[1]), narrow))
-        shapes.append(jax.ShapeDtypeStruct((2,) + gain.shape, wide))
+        _, tokens = extra
+        shapes.append(jax.ShapeDtypeStruct((halo // near, tokens.shape[1] + LANES), narrow))
     return pl.pallas_call(
-        functools.partial(pack_body, layer, halo),
+        functools.partial(pack_body, layer, halo, near),
         out_shape=tuple(shapes),
-        in_specs=[pl.BlockSpec(memory_space=pl.ANY)] * (2 + len(extra)),
+        in_specs=[in_hbm()] * 2 + [in_vmem()] * min(1, len(extra)) + [in_hbm()] * (len(extra) - 1),
         out_specs=tuple(in_vmem() for _ in shapes),
-        scratch_shapes=[pltpu.SemaphoreType.DMA((5 if halo else 2,))],
+        scratch_shapes=[pltpu.SemaphoreType.DMA((3 if halo else 2,))],
+        cost_estimate=pl.CostEstimate(flops=PACK_FLOPS, bytes_accessed=PACK_BYTES, transcendentals=0),
         compiler_params=pltpu.CompilerParams(vmem_limit_bytes=KERNEL_VMEM),
     )(value_proj, gate_proj, *extra)
 
 
-def norm_body(prev_ref, tokens_ref, gain_ref, normed_ref):
-    halo = prev_ref.shape[0]
+def norm_body(tail, near, tokens_ref, docs_ref, gain_ref, *refs):
+    prev_refs, (normed_ref, dist_ref, state_ref, run_ref) = refs[:near], refs[near:]
+    row_count, model_width = tokens_ref.shape
+    halo = normed_ref.shape[0] - row_count
+    part = halo // near
+    rows = halo + row_count
+    lead = run_ref.shape[0] - rows
     gain = gain_ref[0:1, :]
-    normed_ref[:halo, :] = normed_of(prev_ref[...].astype(wide), gain)
+    place = lax.axis_index("tp") % near
+    for step, prev_ref in enumerate(prev_refs):
+        first = pl.multiple_of((place - step + near) % near * part, HALO_ALIGN)
+        prev = prev_ref[:, :model_width]
+        state_ref[pl.ds(first, part), :] = prev
+        normed_ref[pl.ds(first, part), :] = normed_of(prev.astype(wide), gain)
+        docs = prev_ref[:, model_width:].astype(wide)
+        docs = jnp.broadcast_to(docs[:, 0:1] * 256 + docs[:, 1:2], (part, LANES))
+        run_ref[pl.ds(pl.multiple_of(lead + first, SUBLANES), part), :] = docs
     normed_ref[halo:, :] = normed_of(tokens_ref[...].astype(wide), gain)
+    own_docs = docs_ref[...].reshape(1, row_count).astype(wide)
+    own_docs = jnp.broadcast_to(own_docs, (SUBLANES, row_count)).T[:, 0:1] + 1
+    run_ref[:lead, :] = jnp.full((lead, LANES), -1.0, wide)
+    run_ref[lead + halo :, :] = jnp.broadcast_to(own_docs, (row_count, LANES))
+    same = run_ref[lead:, :] == run_ref[lead - 1 : lead - 1 + rows, :]
+    run = jnp.where(same, 1.0, 0.0)
+    run_ref[:lead, :] = jnp.zeros((lead, LANES), wide)
+    reach = 1
+    while reach < tail:
+        run_ref[lead:, :] = run
+        run = jnp.where(run == reach, reach + run_ref[lead - reach : lead - reach + rows, :], run)
+        reach = 2 * reach
+    dist_ref[...] = run[tail:, :]
+
+
+def chunk_start(places, k, size):
+    if places is None:
+        return 0
+    count, steps = places
+    return pl.multiple_of(ring_place(count, steps[k]) * size, LANES)
 
 
 def gated_conv_body(
-    layer, tap_count, tail, split, table_ref, normed_ref, dist_ref, taps_ref, *refs
+    layer, tap_count, tail, places, normed_ref, dist_ref, taps_ref, *refs
 ):
     *pair_refs, centred_ref, stats_ref, acc_ref, shifted_ref, conv_ref = refs
-    pairs = [(pair.at[0], pair.at[1]) for pair in (pair_refs[:-2] if split else pair_refs)]
-    if split:
+    pairs = [(pair.at[0], pair.at[1]) for pair in (pair_refs[:-2] if places else pair_refs)]
+    if places:
         pairs.append(tuple(pair_refs[-2:]))
     width = taps_ref.shape[2]
     halves = width // LANES
@@ -117,7 +163,7 @@
     dist_from = dist_ref.shape[0] - out_rows
     depth = pair_refs[0].shape[1]
     for k, pair in enumerate(pairs):
-        first = 0 if len(pairs) == 1 else pl.multiple_of(table_ref[k] * depth, LANES)
+        first = chunk_start(places, k, depth)
         rows_in = normed_ref[:, pl.ds(first, depth)]
         for part in range(2):
             product = jnp.dot(rows_in, pair[part][...], preferred_element_type=wide)
@@ -146,7 +192,7 @@
             start = pl.multiple_of(base + (tail - tap // SUBLANES * SUBLANES), SUBLANES)
             for half in range(halves):
                 rows_at = shifted_ref[half, tap % SUBLANES, pl.ds(start, CONV_ROWS), :]
-                weight = taps_ref[layer, tap : tap + 1, half * LANES : (half + 1) * LANES]
+                weight = taps_ref[tap, layer : layer + 1, half * LANES : (half + 1) * LANES]
                 sums[half] = sums[half] + jnp.where(inside, weight * rows_at, 0.0)
         for half in range(halves):
             conv_ref[half, pl.ds(base, CONV_ROWS), :] = sums[half]
@@ -175,8 +221,8 @@
     return functools.reduce(jnp.add, values)
 
 
-def project_body(layer, near, far, slots, table_ref, gain_ref, shift_ref, *refs):
-    far_norm_refs, refs = refs[: far - 1], refs[far - 1 :]
+def project_body(layer, near, far, slots, places, *refs):
+    gain_refs, shift_refs, refs = refs[:far], refs[far : 2 * far], refs[2 * far :]
     stats_refs, refs = refs[: far * near], refs[far * near :]
     centred_refs, refs = refs[:far], refs[far:]
     *piece_refs, share_ref, act_ref = refs
@@ -193,11 +239,7 @@
     scale = lax.rsqrt(square / (width * count) + epsilon)
     for f, centred in enumerate(centred_refs):
         own = means[f * near]
-        if f == 0:
-            gain, shift = gain_ref[layer : layer + 1, :], shift_ref[layer : layer + 1, :]
-        else:
-            norms = far_norm_refs[f - 1]
-            gain, shift = norms[0, layer : layer + 1, :], norms[1, layer : layer + 1, :]
+        gain, shift = gain_refs[f][layer : layer + 1, :], shift_refs[f][layer : layer + 1, :]
         normal = gain * (centred[...].astype(wide) + (own - mean)) * scale + shift
         act_ref[f] = (normal * jax.nn.sigmoid(normal)).astype(narrow)
     steps = len(slots) // far
@@ -209,7 +251,7 @@
             product = jnp.dot(act_ref[f], matrix, preferred_element_type=wide)
             share = product if share is None else share + product
         cols = share.shape[1]
-        first = 0 if steps == 1 else pl.multiple_of(table_ref[k] * cols, LANES)
+        first = chunk_start(places, k, cols)
         share_ref[:, pl.ds(first, cols)] = share.astype(narrow)
 
 
@@ -220,6 +262,7 @@
     else:
         gain_ref, *share_refs, hidden_ref, normed_ref = refs
     skip, at = tail, 0
+    model_width = hidden_ref.shape[1]
     for state_ref in state_refs:
         rows = state_ref.shape[0]
         from_row = min(skip, rows)
@@ -231,13 +274,23 @@
         for share in share_refs[1:]:
             branch = branch + share[at : at + count, :].astype(wide)
         hidden = (
-            state_ref[from_row:, :].astype(wide) + branch.astype(narrow).astype(wide)
+            state_ref[from_row:, :model_width].astype(wide) + branch.astype(narrow).astype(wide)
         ).astype(narrow)
         hidden_ref[at : at + count, :] = hidden
         if not is_last:
             gain = gain_ref[layer + 1 : layer + 2, :]
             normed_ref[at : at + count, :] = normed_of(hidden.astype(wide), gain)
         at = at + count
+
+
+def ring_place(count, step):
+    index = lax.axis_index("sp")
+    odd = index % 2
+    position = jnp.where(odd == 1, count - 1 - index // 2, index // 2)
+    position = (position + step + count) % count
+    return jnp.where(
+        position < count // 2, 2 * position, 2 * (count - 1 - position) + 1
+    )
 
 
 def ring_tables(count):
@@ -249,9 +302,7 @@
         steps.append(-k)
         if len(steps) < count:
             steps.append(k)
-    position = {device: k for k, device in enumerate(order)}
-    table = [[order[(position[s] + step) % count] for step in steps] for s in range(count)]
-    return forward, backward, table
+    return forward, backward, steps
 
 
 def ring_gathered(value):
@@ -307,11 +358,10 @@
             values.append(lax.ppermute(values[-1], "tp", far_pairs))
         return values
 
+    docs = doc_ids
     packs = [packed(n, value_proj, gate_proj) for n in range(layer_count - 1)]
-    packs.append(
-        packed(layer_count - 1, value_proj, gate_proj, halo, (tokens, norm_gain, norm_shift))
-    )
-    _, tail_rows, norms = packs[-1]
+    packs.append(packed(layer_count - 1, value_proj, gate_proj, halo, near, (docs, tokens)))
+    tail_part = packs[-1][1]
     pair_chunks, out_pieces, out_slots = [], [], []
     if in_ring:
         chunks = [out_proj] + ring_gathered(out_proj)
@@ -334,42 +384,42 @@
         out_slots.append(slots)
 
     onward = [(source, source + 1) for source in range(sp_count - 1)]
-    prev_docs = lax.ppermute(doc_ids[row_count - halo :] + 1, "sp", onward) - 1
-    prev_rows = lax.ppermute(tail_rows, "sp", onward)
-    far_norm = far_values(norms)[1:]
-    docs = jnp.concatenate([prev_docs, doc_ids])
-    dist = jnp.zeros((row_count + halo - tail,), jnp.int32)
-    for offset in range(1, tap_count):
-        first = tail - offset
-        dist = dist + (docs[first : first + dist.shape[0]] == docs[tail:]).astype(jnp.int32)
-    dist = jnp.broadcast_to(dist[:, None], (dist.shape[0], LANES))
-
-    sp_blocks = ring_tables(sp_count)[2] if in_ring else [[0]] * sp_count
-    table = jnp.asarray(sp_blocks, jnp.int32)
-    table = lax.dynamic_index_in_dim(table, lax.axis_index("sp"), keepdims=False)
-
-    states = (prev_rows, tokens)
-    normed = kernel(
-        norm_body, jax.ShapeDtypeStruct((halo + row_count, model_width), narrow), [in_vmem()] * 3
-    )(prev_rows, tokens, pre_gain)
+    prev_parts = [lax.ppermute(tail_part, "sp", onward)]
+    for _ in range(1, near):
+        prev_parts.append(lax.ppermute(prev_parts[-1], "tp", near_pairs))
+    gains, shifts = far_values(norm_gain), far_values(norm_shift)
+    places = (sp_count, ring_tables(sp_count)[2]) if in_ring else None
+
+    taps = jnp.transpose(conv_taps, (1, 0, 2))
+    normed, dist, prev_state = kernel(
+        functools.partial(norm_body, tail, near),
+        (
+            jax.ShapeDtypeStruct((halo + row_count, model_width), narrow),
+            jax.ShapeDtypeStruct((halo + row_count - tail, LANES), wide),
+            jax.ShapeDtypeStruct((halo, model_width), narrow),
+        ),
+        [in_vmem()] * (3 + near),
+        [pltpu.VMEM((tail + halo + row_count, LANES), wide)],
+    )(tokens, docs, pre_gain, *prev_parts)
+    states = (prev_state, tokens)
 
     for n in range(layer_count):
         rows = normed.shape[0]
         out_rows = rows - tail
         pairs = pair_chunks[n]
         centred, stats = kernel(
-            functools.partial(gated_conv_body, n, tap_count, tail, in_ring),
+            functools.partial(gated_conv_body, n, tap_count, tail, places),
             (
                 jax.ShapeDtypeStruct((out_rows, width), narrow),
                 jax.ShapeDtypeStruct((2, round_up(out_rows, LANES)), wide),
             ),
-            [in_smem()] + [in_vmem()] * (3 + len(pairs)),
+            [in_vmem()] * (3 + len(pairs)),
             [
                 pltpu.VMEM((2, rows, width), wide),
                 pltpu.VMEM((width // LANES, SUBLANES, rows, LANES), wide),
                 pltpu.VMEM((width // LANES, out_rows, LANES), wide),
             ],
-        )(table, normed, dist, conv_taps, *pairs)
+        )(normed, dist, taps, *pairs)
         far_centred = far_values(centred)
         all_stats = [stats]
         for place in range(1, tp_count):
@@ -377,22 +427,22 @@
             all_stats.append(lax.ppermute(stats, "tp", steps))
         pieces = out_pieces[n]
         share = kernel(
-            functools.partial(project_body, n, near, far, out_slots[n]),
+            functools.partial(project_body, n, near, far, out_slots[n], places),
             jax.ShapeDtypeStruct((out_rows, model_width), narrow),
-            [in_smem()] + [in_vmem()] * (2 + far - 1 + tp_count + far + len(pieces)),
+            [in_vmem()] * (3 * far + tp_count + len(pieces)),
             [pltpu.VMEM((far, out_rows, width), narrow)],
-        )(table, norm_gain, norm_shift, *far_norm, *all_stats, *far_centred, *pieces)
+        )(*gains, *shifts, *all_stats, *far_centred, *pieces)
         shares = [share]
         for _ in range(1, near):
             shares.append(lax.ppermute(shares[-1], "tp", near_pairs))
         is_last = n == layer_count - 1
         shape = jax.ShapeDtypeStruct((out_rows, model_width), narrow)
-        gains = () if is_last else (pre_gain,)
+        next_gain = () if is_last else (pre_gain,)
         result = kernel(
             functools.partial(add_body, n, tail, is_last, len(states)),
             shape if is_last else (shape, shape),
-            [in_vmem()] * (len(states) + len(gains) + len(shares)),
-        )(*states, *gains, *shares)
+            [in_vmem()] * (len(states) + len(next_gain) + len(shares)),
+        )(*states, *next_gain, *shares)
         if is_last:
             return result
         hidden, normed = result

time: 142 us -> 134 us (0.944)
  waiting for transfers between devices: 48.1 us -> 62 us
  starting transfers between devices: 66.4 us -> 53.7 us
  local copies, waits for them, and re-layouts: 7.46 us -> 2.13 us
  Pallas kernels: 18 us -> 16.1 us
    ppermute x12, starting transfers between devices: 26.4 us -> 9.53 us  [ring_gathered(): ahead = lax.ppermute(ahead, 'sp', forward)]
    ppermute x12, waiting for transfers between devices: 16.1 us -> 25.1 us  [ring_gathered(): ahead = lax.ppermute(ahead, 'sp', forward)]
    ppermute x12 -> x13, waiting for transfers between devices: 3.28 us -> 9.21 us  [far_values(): values.append(lax.ppermute(values[-1], 'tp', far_pairs))]
    ppermute x12, starting transfers between devices: 16.7 us -> 22.4 us  [ring_gathered(): behind = lax.ppermute(behind, 'sp', backward)]
    unnamed x29 -> x18, local copies, waits for them, and re-layouts: 6.6 us -> 2.07 us
    ppermute x6, waiting for transfers between devices: 12 us -> 15.8 us  [on_device(): all_stats.append(lax.ppermute(stats, 'tp', steps))]
    ppermute x2, starting transfers between devices: 5.82 us -> 2.04 us  [the longest x1 1.96 us: on_device(): prev_parts = [lax.ppermute(tail_part, 'sp', onward)]]
    ppermute x12, waiting for transfers between devices: 12 us -> 8.61 us  [ring_gathered(): behind = lax.ppermute(behind, 'sp', backward)]
  transfers between devices with their start and end apart: 46 -> 47, of which waited for: 17 -> 17; matrix products, arithmetic and copies ran while one was open for 1% -> 0% of each run, Pallas kernels for 7% -> 7%
where the time goes in v2:
time: 134 us
  waiting for transfers between devices  62 us (46%)
  starting transfers between devices  53.7 us (40%)
  Pallas kernels  16.1 us (12%)
  local copies, waits for them, and re-layouts  2.13 us (2%)
    ppermute x12, waiting for transfers between devices, ring_gathered(): ahead = lax.ppermute(ahead, 'sp', forward)  25.1 us
    ppermute x12, starting transfers between devices, ring_gathered(): behind = lax.ppermute(behind, 'sp', backward)  22.4 us
    ppermute x13, starting transfers between devices, far_values(): values.append(lax.ppermute(values[-1], 'tp', far_pairs))  15.9 us
    ppermute x6, waiting for transfers between devices, on_device(): all_stats.append(lax.ppermute(stats, 'tp', steps))  15.8 us
    ppermute x12, starting transfers between devices, ring_gathered(): ahead = lax.ppermute(ahead, 'sp', forward)  9.53 us
    ppermute x13, waiting for transfers between devices, far_values(): values.append(lax.ppermute(values[-1], 'tp', far_pairs))  9.21 us
    ppermute x12, waiting for transfers between devices, ring_gathered(): behind = lax.ppermute(behind, 'sp', backward)  8.61 us
    pallas_call x2, Pallas kernels, on_device(): kernel(functools.partial(gated_conv_body, n, tap_count, tail, places), (j...  6.74 us
  transfers between devices with their start and end apart: 47, of which 17 were waited for; matrix products, arithmetic and copies ran while one was open for 0% of the time, Pallas kernels for 7%

profile of v2, /device:TPU:0, one launch (start us, length us, event | category | flops | bytes accessed | tf_op | source)
XLA Modules:
  0.0 134.1 jit_solution(8209899856573257654)
XLA Ops:
  2.4 3.1 %collective-permute-start.4 = (bf16[2,256,256]{2,1,0:T(8,128)(2,1)S(1)}, bf16[2,256,256]{2,1,0:T(8,128)(2,1)S(1)}, u32[]{:S(2)}, u32[]{:S(2)}) collective-permute-start(bf16[2,256,256]{2,1,0:T(8,128)(2,1)S(1)} %shard_map.93.refs_0_), channel_id=1, source_target_pairs={{0,8},{8,16},{16,24},{24,28},{28,20},{20,12},{12,4},{4,0},{1,9},{9... | collective-permute-start | bytes 786440 | tf_op jit(solution)/shard_map/ppermute | solution.py:316
  5.5 2.0 %collective-permute-start.17 = (bf16[2,256,256]{2,1,0:T(8,128)(2,1)S(1)}, bf16[2,256,256]{2,1,0:T(8,128)(2,1)S(1)}, u32[]{:S(2)}, u32[]{:S(2)}) collective-permute-start(bf16[2,256,256]{2,1,0:T(8,128)(2,1)S(1)} %copy-done.1), channel_id=1, source_target_pairs={{0,8},{8,16},{16,24},{24,28},{28,20},{20,12},{12,4},{4,0},{1,9},{9... | collective-permute-start | bytes 786440 | tf_op jit(solution)/shard_map/ppermute | solution.py:316
  7.5 5.0 %collective-permute-done.4.refs_1_ = bf16[2,256,256]{2,1,0:T(8,128)(2,1)S(1)} collective-permute-done((bf16[2,256,256]{2,1,0:T(8,128)(2,1)S(1)}, bf16[2,256,256]{2,1,0:T(8,128)(2,1)S(1)}, u32[]{:S(2)}, u32[]{:S(2)}) %collective-permute-start.4) | collective-permute-done | bytes 262176 | tf_op jit(solution)/shard_map/ppermute | solution.py:316
  12.6 2.1 %collective-permute-start.6 = (bf16[2,256,256]{2,1,0:T(8,128)(2,1)S(1)}, bf16[2,256,256]{2,1,0:T(8,128)(2,1)S(1)}, u32[]{:S(2)}, u32[]{:S(2)}) collective-permute-start(bf16[2,256,256]{2,1,0:T(8,128)(2,1)S(1)} %collective-permute-done.4.refs_1_), channel_id=1, source_target_pairs={{0,8},{8,16},{16,24},{24,28},{28,20},{20,12},{12,4},{4,0},{1,9},{9... | collective-permute-start | bytes 786440 | tf_op jit(solution)/shard_map/ppermute | solution.py:316
  15.2 2.0 %collective-permute-start = (bf16[32,2176]{1,0:T(8,128)(2,1)S(1)}, bf16[32,2176]{1,0:T(8,128)(2,1)S(1)}, u32[]{:S(2)}, u32[]{:S(2)}) collective-permute-start(bf16[32,2176]{1,0:T(8,128)(2,1)S(1)} %get-tuple-element.16), channel_id=1, source_target_pairs={{0,4},{4,8},{8,12},{12,16},{16,20},{20,24},{24,28},{1,5},{5,9},{9,... | collective-permute-start | bytes 417800 | tf_op jit(solution)/shard_map/ppermute | solution.py:387
  17.2 2.1 %collective-permute-start.2 = (f32[2,256]{1,0:T(2,128)S(1)}, f32[2,256]{1,0:T(2,128)S(1)}, u32[]{:S(2)}, u32[]{:S(2)}) collective-permute-start(f32[2,256]{1,0:T(2,128)S(1)} %copy-done.4), channel_id=1, source_target_pairs={{0,2},{1,3},{2,0},{3,1},{4,6},{5,7},{6,4},{7,5},{8,10},{9,11},{10,... | collective-permute-start | bytes 6152 | tf_op jit(solution)/shard_map/ppermute | solution.py:358
  20.9 2.0 %collective-permute-start.3 = (f32[2,256]{1,0:T(2,128)S(1)}, f32[2,256]{1,0:T(2,128)S(1)}, u32[]{:S(2)}, u32[]{:S(2)}) collective-permute-start(f32[2,256]{1,0:T(2,128)S(1)} %copy-done.5), channel_id=1, source_target_pairs={{0,2},{1,3},{2,0},{3,1},{4,6},{5,7},{6,4},{7,5},{8,10},{9,11},{10,... | collective-permute-start | bytes 6152 | tf_op jit(solution)/shard_map/ppermute | solution.py:358
  24.5 3.1 %collective-permute-start.19 = (bf16[2,256,256]{2,1,0:T(8,128)(2,1)S(1)}, bf16[2,256,256]{2,1,0:T(8,128)(2,1)S(1)}, u32[]{:S(2)}, u32[]{:S(2)}) collective-permute-start(bf16[2,256,256]{2,1,0:T(8,128)(2,1)S(1)} %copy-done.1), channel_id=1, source_target_pairs={{8,0},{16,8},{24,16},{28,24},{20,28},{12,20},{4,12},{0,4},{9,1},{1... | collective-permute-start | bytes 786440 | tf_op jit(solution)/shard_map/ppermute | solution.py:317
  31.2 3.1 %collective-permute-done.19.refs_14_ = bf16[2,256,256]{2,1,0:T(8,128)(2,1)S(1)} collective-permute-done((bf16[2,256,256]{2,1,0:T(8,128)(2,1)S(1)}, bf16[2,256,256]{2,1,0:T(8,128)(2,1)S(1)}, u32[]{:S(2)}, u32[]{:S(2)}) %collective-permute-start.19) | collective-permute-done | bytes 262176 | tf_op jit(solution)/shard_map/ppermute | solution.py:317
  34.3 2.5 %collective-permute-start.23 = (bf16[2,256,256]{2,1,0:T(8,128)(2,1)S(1)}, bf16[2,256,256]{2,1,0:T(8,128)(2,1)S(1)}, u32[]{:S(2)}, u32[]{:S(2)}) collective-permute-start(bf16[2,256,256]{2,1,0:T(8,128)(2,1)S(1)} %collective-permute-done.19.refs_14_), channel_id=1, source_target_pairs={{8,0},{16,8},{24,16},{28,24},{20,28},{12,20},{4,12},{0,4},{9,1},{1... | collective-permute-start | bytes 786440 | tf_op jit(solution)/shard_map/ppermute | solution.py:317
  36.8 3.1 %collective-permute-done.7.refs_4_ = bf16[2,256,256]{2,1,0:T(8,128)(2,1)S(1)} collective-permute-done((bf16[2,256,256]{2,1,0:T(8,128)(2,1)S(1)}, bf16[2,256,256]{2,1,0:T(8,128)(2,1)S(1)}, u32[]{:S(2)}, u32[]{:S(2)}) %collective-permute-start.7) | collective-permute-done | bytes 262176 | tf_op jit(solution)/shard_map/ppermute | solution.py:317
  39.9 2.5 %collective-permute-start.9 = (bf16[2,256,256]{2,1,0:T(8,128)(2,1)S(1)}, bf16[2,256,256]{2,1,0:T(8,128)(2,1)S(1)}, u32[]{:S(2)}, u32[]{:S(2)}) collective-permute-start(bf16[2,256,256]{2,1,0:T(8,128)(2,1)S(1)} %collective-permute-done.7.refs_4_), channel_id=1, source_target_pairs={{8,0},{16,8},{24,16},{28,24},{20,28},{12,20},{4,12},{0,4},{9,1},{1... | collective-permute-start | bytes 786440 | tf_op jit(solution)/shard_map/ppermute | solution.py:317
  44.5 1.7 %collective-permute-done.9.refs_6_ = bf16[2,256,256]{2,1,0:T(8,128)(2,1)S(1)} collective-permute-done((bf16[2,256,256]{2,1,0:T(8,128)(2,1)S(1)}, bf16[2,256,256]{2,1,0:T(8,128)(2,1)S(1)}, u32[]{:S(2)}, u32[]{:S(2)}) %collective-permute-start.9) | collective-permute-done | bytes 262176 | tf_op jit(solution)/shard_map/ppermute | solution.py:317
  46.3 2.5 %collective-permute-start.27 = (bf16[2,256,256]{2,1,0:T(8,128)(2,1)S(1)}, bf16[2,256,256]{2,1,0:T(8,128)(2,1)S(1)}, u32[]{:S(2)}, u32[]{:S(2)}) collective-permute-start(bf16[2,256,256]{2,1,0:T(8,128)(2,1)S(1)} %collective-permute-done.23.refs_18_), channel_id=1, source_target_pairs={{8,0},{16,8},{24,16},{28,24},{20,28},{12,20},{4,12},{0,4},{9,1},{1... | collective-permute-start | bytes 786440 | tf_op jit(solution)/shard_map/ppermute | solution.py:317
  50.9 2.8 %collective-permute-done.20.refs_15_ = bf16[2,256,256]{2,1,0:T(8,128)(2,1)S(1)} collective-permute-done((bf16[2,256,256]{2,1,0:T(8,128)(2,1)S(1)}, bf16[2,256,256]{2,1,0:T(8,128)(2,1)S(1)}, u32[]{:S(2)}, u32[]{:S(2)}) %collective-permute-start.20) | collective-permute-done | bytes 262176 | tf_op jit(solution)/shard_map/ppermute | solution.py:358
  53.7 2.0 %collective-permute-start.11 = (bf16[256,256]{1,0:T(8,128)(2,1)S(1)}, bf16[256,256]{1,0:T(8,128)(2,1)S(1)}, u32[]{:S(2)}, u32[]{:S(2)}) collective-permute-start(bf16[256,256]{1,0:T(8,128)(2,1)S(1)} %slice_bitcast_fusion.4), channel_id=1, source_target_pairs={{8,0},{16,8},{24,16},{28,24},{20,28},{12,20},{4,12},{0,4},{9,1},{1... | collective-permute-start | bytes 393224 | tf_op jit(solution)/shard_map/ppermute | solution.py:317
  55.8 2.8 %collective-permute-done.10.refs_7_ = bf16[256,256]{1,0:T(8,128)(2,1)S(1)} collective-permute-done((bf16[256,256]{1,0:T(8,128)(2,1)S(1)}, bf16[256,256]{1,0:T(8,128)(2,1)S(1)}, u32[]{:S(2)}, u32[]{:S(2)}) %collective-permute-start.10) | collective-permute-done | bytes 131104 | tf_op jit(solution)/shard_map/ppermute | solution.py:316
  61.7 3.5 %shard_map.94 = (bf16[416,256]{1,0:T(8,128)(2,1)S(1)}, f32[2,512]{1,0:T(2,128)S(1)}) custom-call(bf16[448,2048]{1,0:T(8,128)(2,1)S(1)} %get-tuple-element.18.normed_ref, f32[416,128]{1,0:T(8,128)S(1)} %get-tuple-element.19.dist_ref, f32[31,2,256]{2,1,0:T(2,128)S(1)} %bitcast.13, bf16[2,256,256]{2,1,0:T(8,128)(2,1)S(1)} %shard_map.93.refs_0_, ...), custom_call_target="tpu_custom_call" | custom-call | tf_op jit(solution)/shard_map/pallas_call | solution.py:410
  69.9 11.6 %collective-permute-done.13.refs_6_ = f32[2,512]{1,0:T(2,128)S(1)} collective-permute-done((f32[2,512]{1,0:T(2,128)S(1)}, f32[2,512]{1,0:T(2,128)S(1)}, u32[]{:S(2)}, u32[]{:S(2)}) %collective-permute-start.13) | collective-permute-done | bytes 4128 | tf_op jit(solution)/shard_map/ppermute | solution.py:427
  81.5 3.0 %collective-permute-done.14.refs_7_ = f32[2,512]{1,0:T(2,128)S(1)} collective-permute-done((f32[2,512]{1,0:T(2,128)S(1)}, f32[2,512]{1,0:T(2,128)S(1)}, u32[]{:S(2)}, u32[]{:S(2)}) %collective-permute-start.14) | collective-permute-done | bytes 4128 | tf_op jit(solution)/shard_map/ppermute | solution.py:427
  84.5 2.3 %shard_map.95.refs_3_ = bf16[416,2048]{1,0:T(8,128)(2,1)S(1)} custom-call(f32[2,256]{1,0:T(2,128)S(1)} %copy-done.4, f32[2,256]{1,0:T(2,128)S(1)} %collective-permute-done.2.refs_1_, f32[2,256]{1,0:T(2,128)S(1)} %copy-done.5, f32[2,256]{1,0:T(2,128)S(1)} %collective-permute-done.3.refs_3_, f32[2,512]{1,0:T(2,128)S(1)} %get-tuple-element.20.refs_4_, ...), custom_call_target="tpu_custom_call" | custom-call | tf_op jit(solution)/shard_map/pallas_call | solution.py:429
  87.0 2.0 %collective-permute-start.33 = (bf16[2,256,256]{2,1,0:T(8,128)(2,1)S(1)}, bf16[2,256,256]{2,1,0:T(8,128)(2,1)S(1)}, u32[]{:S(2)}, u32[]{:S(2)}) collective-permute-start(bf16[2,256,256]{2,1,0:T(8,128)(2,1)S(1)} %get-tuple-element.24.refs_0_), channel_id=1, source_target_pairs={{8,0},{16,8},{24,16},{28,24},{20,28},{12,20},{4,12},{0,4},{9,1},{1... | collective-permute-start | bytes 786440 | tf_op jit(solution)/shard_map/ppermute | solution.py:317
  89.0 6.6 %collective-permute-done.32.refs_1_ = bf16[2,256,256]{2,1,0:T(8,128)(2,1)S(1)} collective-permute-done((bf16[2,256,256]{2,1,0:T(8,128)(2,1)S(1)}, bf16[2,256,256]{2,1,0:T(8,128)(2,1)S(1)}, u32[]{:S(2)}, u32[]{:S(2)}) %collective-permute-start.32) | collective-permute-done | bytes 262176 | tf_op jit(solution)/shard_map/ppermute | solution.py:316
  95.9 1.7 %collective-permute-start.35 = (bf16[2,256,256]{2,1,0:T(8,128)(2,1)S(1)}, bf16[2,256,256]{2,1,0:T(8,128)(2,1)S(1)}, u32[]{:S(2)}, u32[]{:S(2)}) collective-permute-start(bf16[2,256,256]{2,1,0:T(8,128)(2,1)S(1)} %collective-permute-done.33.refs_2_), channel_id=1, source_target_pairs={{8,0},{16,8},{24,16},{28,24},{20,28},{12,20},{4,12},{0,4},{9,1},{1... | collective-permute-start | bytes 786440 | tf_op jit(solution)/shard_map/ppermute | solution.py:317
  97.7 5.7 %collective-permute-done.34.refs_3_ = bf16[2,256,256]{2,1,0:T(8,128)(2,1)S(1)} collective-permute-done((bf16[2,256,256]{2,1,0:T(8,128)(2,1)S(1)}, bf16[2,256,256]{2,1,0:T(8,128)(2,1)S(1)}, u32[]{:S(2)}, u32[]{:S(2)}) %collective-permute-start.34) | collective-permute-done | bytes 262176 | tf_op jit(solution)/shard_map/ppermute | solution.py:316
  105.4 4.9 %collective-permute-done.36.refs_5_ = bf16[2,256,256]{2,1,0:T(8,128)(2,1)S(1)} collective-permute-done((bf16[2,256,256]{2,1,0:T(8,128)(2,1)S(1)}, bf16[2,256,256]{2,1,0:T(8,128)(2,1)S(1)}, u32[]{:S(2)}, u32[]{:S(2)}) %collective-permute-start.36) | collective-permute-done | bytes 262176 | tf_op jit(solution)/shard_map/ppermute | solution.py:316
  112.4 1.8 %collective-permute-start.44 = (bf16[256,256]{1,0:T(8,128)(2,1)S(1)}, bf16[256,256]{1,0:T(8,128)(2,1)S(1)}, u32[]{:S(2)}, u32[]{:S(2)}) collective-permute-start(bf16[256,256]{1,0:T(8,128)(2,1)S(1)} %slice_bitcast_fusion), channel_id=1, source_target_pairs={{8,0},{16,8},{24,16},{28,24},{20,28},{12,20},{4,12},{0,4},{9,1},{1... | collective-permute-start | bytes 393224 | tf_op jit(solution)/shard_map/ppermute | solution.py:317
  116.2 3.2 %shard_map.97 = (bf16[384,256]{1,0:T(8,128)(2,1)S(1)}, f32[2,384]{1,0:T(2,128)S(1)}) custom-call(bf16[416,2048]{1,0:T(8,128)(2,1)S(1)} %get-tuple-element.23.normed_ref, f32[416,128]{1,0:T(8,128)S(1)} %get-tuple-element.19.dist_ref, f32[31,2,256]{2,1,0:T(2,128)S(1)} %bitcast.14, bf16[2,256,256]{2,1,0:T(8,128)(2,1)S(1)} %get-tuple-element.24.refs_0_, ...), custom_call_target="tpu_custom_call" | custom-call | tf_op jit(solution)/shard_map/pallas_call | solution.py:410
  123.4 3.2 %collective-permute-done.45.refs_25_ = bf16[256,256]{1,0:T(8,128)(2,1)S(1)} collective-permute-done((bf16[256,256]{1,0:T(8,128)(2,1)S(1)}, bf16[256,256]{1,0:T(8,128)(2,1)S(1)}, u32[]{:S(2)}, u32[]{:S(2)}) %collective-permute-start.45) | collective-permute-done | bytes 131104 | tf_op jit(solution)/shard_map/ppermute | solution.py:358
  126.7 2.1 %shard_map.98.refs_1_ = bf16[384,2048]{1,0:T(8,128)(2,1)S(1)} custom-call(f32[2,256]{1,0:T(2,128)S(1)} %copy-done.4, f32[2,256]{1,0:T(2,128)S(1)} %collective-permute-done.2.refs_1_, f32[2,256]{1,0:T(2,128)S(1)} %copy-done.5, f32[2,256]{1,0:T(2,128)S(1)} %collective-permute-done.3.refs_3_, f32[2,384]{1,0:T(2,128)S(1)} %get-tuple-element.25.refs_4_, ...), custom_call_target="tpu_custom_call" | custom-call | tf_op jit(solution)/shard_map/pallas_call | solution.py:429
  128.9 3.3 %collective-permute-done.46.refs_2_ = bf16[384,2048]{1,0:T(8,128)(2,1)S(1)} collective-permute-done((bf16[384,2048]{1,0:T(8,128)(2,1)S(1)}, bf16[384,2048]{1,0:T(8,128)(2,1)S(1)}, u32[]{:S(2)}, u32[]{:S(2)}) %collective-permute-start.46) | collective-permute-done | bytes 1572896 | tf_op jit(solution)/shard_map/ppermute | solution.py:437
  132.2 1.9 %shard_map.99 = bf16[384,2048]{1,0:T(8,128)(2,1)} custom-call(bf16[416,2048]{1,0:T(8,128)(2,1)S(1)} %get-tuple-element.22.refs_0_, bf16[384,2048]{1,0:T(8,128)(2,1)S(1)} %shard_map.98.refs_1_, bf16[384,2048]{1,0:T(8,128)(2,1)S(1)} %collective-permute-done.46.refs_2_), custom_call_target="tpu_custom_call" | custom-call | tf_op jit(solution)/shard_map/pallas_call | solution.py:441
  (95 shorter events, 32.5 us)
Async XLA Ops:
  2.4 10.2 %collective-permute-start.4 = (bf16[2,256,256]{2,1,0:T(8,128)(2,1)S(1)}, bf16[2,256,256]{2,1,0:T(8,128)(2,1)S(1)}, u32[]{:S(2)}, u32[]{:S(2)}) collective-permute-start(bf16[2,256,256]{2,1,0:T(8,128)(2,1)S(1)} %shard_map.93.refs_0_), channel_id=1, source_target_pairs={{0,8},{8,16},{16,24},{24,28},{28,20},{20,12},{12,4},{4,0},{1,9},{9... | collective-permute-start | bytes 786440 | tf_op jit(solution)/shard_map/ppermute | solution.py:316
  5.5 22.1 %collective-permute-start.5 = (bf16[2,256,256]{2,1,0:T(8,128)(2,1)S(1)}, bf16[2,256,256]{2,1,0:T(8,128)(2,1)S(1)}, u32[]{:S(2)}, u32[]{:S(2)}) collective-permute-start(bf16[2,256,256]{2,1,0:T(8,128)(2,1)S(1)} %shard_map.93.refs_0_), channel_id=1, source_target_pairs={{8,0},{16,8},{24,16},{28,24},{20,28},{12,20},{4,12},{0,4},{9,1},{1... | collective-permute-start | bytes 786440 | tf_op jit(solution)/shard_map/ppermute | solution.py:317
  5.5 25.2 %collective-permute-start.17 = (bf16[2,256,256]{2,1,0:T(8,128)(2,1)S(1)}, bf16[2,256,256]{2,1,0:T(8,128)(2,1)S(1)}, u32[]{:S(2)}, u32[]{:S(2)}) collective-permute-start(bf16[2,256,256]{2,1,0:T(8,128)(2,1)S(1)} %copy-done.1), channel_id=1, source_target_pairs={{0,8},{8,16},{16,24},{24,28},{28,20},{20,12},{12,4},{4,0},{1,9},{9... | collective-permute-start | bytes 786440 | tf_op jit(solution)/shard_map/ppermute | solution.py:316
  12.6 18.5 %collective-permute-start.6 = (bf16[2,256,256]{2,1,0:T(8,128)(2,1)S(1)}, bf16[2,256,256]{2,1,0:T(8,128)(2,1)S(1)}, u32[]{:S(2)}, u32[]{:S(2)}) collective-permute-start(bf16[2,256,256]{2,1,0:T(8,128)(2,1)S(1)} %collective-permute-done.4.refs_1_), channel_id=1, source_target_pairs={{0,8},{8,16},{16,24},{24,28},{28,20},{20,12},{12,4},{4,0},{1,9},{9... | collective-permute-start | bytes 786440 | tf_op jit(solution)/shard_map/ppermute | solution.py:316
  15.2 13.9 %collective-permute-start = (bf16[32,2176]{1,0:T(8,128)(2,1)S(1)}, bf16[32,2176]{1,0:T(8,128)(2,1)S(1)}, u32[]{:S(2)}, u32[]{:S(2)}) collective-permute-start(bf16[32,2176]{1,0:T(8,128)(2,1)S(1)} %get-tuple-element.16), channel_id=1, source_target_pairs={{0,4},{4,8},{8,12},{12,16},{16,20},{20,24},{24,28},{1,5},{5,9},{9,... | collective-permute-start | bytes 417800 | tf_op jit(solution)/shard_map/ppermute | solution.py:387
  24.5 9.8 %collective-permute-start.19 = (bf16[2,256,256]{2,1,0:T(8,128)(2,1)S(1)}, bf16[2,256,256]{2,1,0:T(8,128)(2,1)S(1)}, u32[]{:S(2)}, u32[]{:S(2)}) collective-permute-start(bf16[2,256,256]{2,1,0:T(8,128)(2,1)S(1)} %copy-done.1), channel_id=1, source_target_pairs={{8,0},{16,8},{24,16},{28,24},{20,28},{12,20},{4,12},{0,4},{9,1},{1... | collective-permute-start | bytes 786440 | tf_op jit(solution)/shard_map/ppermute | solution.py:317
  27.6 12.3 %collective-permute-start.7 = (bf16[2,256,256]{2,1,0:T(8,128)(2,1)S(1)}, bf16[2,256,256]{2,1,0:T(8,128)(2,1)S(1)}, u32[]{:S(2)}, u32[]{:S(2)}) collective-permute-start(bf16[2,256,256]{2,1,0:T(8,128)(2,1)S(1)} %collective-permute-done.5.refs_2_), channel_id=1, source_target_pairs={{8,0},{16,8},{24,16},{28,24},{20,28},{12,20},{4,12},{0,4},{9,1},{1... | collective-permute-start | bytes 786440 | tf_op jit(solution)/shard_map/ppermute | solution.py:317
  29.2 13.2 %collective-permute-start.16 = (bf16[2,256,256]{2,1,0:T(8,128)(2,1)S(1)}, bf16[2,256,256]{2,1,0:T(8,128)(2,1)S(1)}, u32[]{:S(2)}, u32[]{:S(2)}) collective-permute-start(bf16[2,256,256]{2,1,0:T(8,128)(2,1)S(1)} %copy-done.1), channel_id=1, source_target_pairs={{0,2},{1,3},{2,0},{3,1},{4,6},{5,7},{6,4},{7,5},{8,10},{9,11},{10,... | collective-permute-start | bytes 786440 | tf_op jit(solution)/shard_map/ppermute | solution.py:358
  30.7 13.2 %collective-permute-start.21 = (bf16[2,256,256]{2,1,0:T(8,128)(2,1)S(1)}, bf16[2,256,256]{2,1,0:T(8,128)(2,1)S(1)}, u32[]{:S(2)}, u32[]{:S(2)}) collective-permute-start(bf16[2,256,256]{2,1,0:T(8,128)(2,1)S(1)} %collective-permute-done.17.refs_12_), channel_id=1, source_target_pairs={{0,8},{8,16},{16,24},{24,28},{28,20},{20,12},{12,4},{4,0},{1,9},{9... | collective-permute-start | bytes 786440 | tf_op jit(solution)/shard_map/ppermute | solution.py:316
  31.1 13.3 %collective-permute-start.8 = (bf16[2,256,256]{2,1,0:T(8,128)(2,1)S(1)}, bf16[2,256,256]{2,1,0:T(8,128)(2,1)S(1)}, u32[]{:S(2)}, u32[]{:S(2)}) collective-permute-start(bf16[2,256,256]{2,1,0:T(8,128)(2,1)S(1)} %collective-permute-done.6.refs_3_), channel_id=1, source_target_pairs={{0,8},{8,16},{16,24},{24,28},{28,20},{20,12},{12,4},{4,0},{1,9},{9... | collective-permute-start | bytes 786440 | tf_op jit(solution)/shard_map/ppermute | solution.py:316
  34.3 10.2 %collective-permute-start.23 = (bf16[2,256,256]{2,1,0:T(8,128)(2,1)S(1)}, bf16[2,256,256]{2,1,0:T(8,128)(2,1)S(1)}, u32[]{:S(2)}, u32[]{:S(2)}) collective-permute-start(bf16[2,256,256]{2,1,0:T(8,128)(2,1)S(1)} %collective-permute-done.19.refs_14_), channel_id=1, source_target_pairs={{8,0},{16,8},{24,16},{28,24},{20,28},{12,20},{4,12},{0,4},{9,1},{1... | collective-permute-start | bytes 786440 | tf_op jit(solution)/shard_map/ppermute | solution.py:317
  42.4 8.0 %collective-permute-start.18 = (bf16[2,256,256]{2,1,0:T(8,128)(2,1)S(1)}, bf16[2,256,256]{2,1,0:T(8,128)(2,1)S(1)}, u32[]{:S(2)}, u32[]{:S(2)}) collective-permute-start(bf16[2,256,256]{2,1,0:T(8,128)(2,1)S(1)} %collective-permute-done.17.refs_12_), channel_id=1, source_target_pairs={{0,2},{1,3},{2,0},{3,1},{4,6},{5,7},{6,4},{7,5},{8,10},{9,11},{10,... | collective-permute-start | bytes 786440 | tf_op jit(solution)/shard_map/ppermute | solution.py:358
  43.9 9.8 %collective-permute-start.20 = (bf16[2,256,256]{2,1,0:T(8,128)(2,1)S(1)}, bf16[2,256,256]{2,1,0:T(8,128)(2,1)S(1)}, u32[]{:S(2)}, u32[]{:S(2)}) collective-permute-start(bf16[2,256,256]{2,1,0:T(8,128)(2,1)S(1)} %collective-permute-done.19.refs_14_), channel_id=1, source_target_pairs={{0,2},{1,3},{2,0},{3,1},{4,6},{5,7},{6,4},{7,5},{8,10},{9,11},{10,... | collective-permute-start | bytes 786440 | tf_op jit(solution)/shard_map/ppermute | solution.py:358
  44.4 9.3 %collective-permute-start.25 = (bf16[2,256,256]{2,1,0:T(8,128)(2,1)S(1)}, bf16[2,256,256]{2,1,0:T(8,128)(2,1)S(1)}, u32[]{:S(2)}, u32[]{:S(2)}) collective-permute-start(bf16[2,256,256]{2,1,0:T(8,128)(2,1)S(1)} %collective-permute-done.21.refs_16_), channel_id=1, source_target_pairs={{0,8},{8,16},{16,24},{24,28},{28,20},{20,12},{12,4},{4,0},{1,9},{9... | collective-permute-start | bytes 786440 | tf_op jit(solution)/shard_map/ppermute | solution.py:316
  46.3 9.5 %collective-permute-start.27 = (bf16[2,256,256]{2,1,0:T(8,128)(2,1)S(1)}, bf16[2,256,256]{2,1,0:T(8,128)(2,1)S(1)}, u32[]{:S(2)}, u32[]{:S(2)}) collective-permute-start(bf16[2,256,256]{2,1,0:T(8,128)(2,1)S(1)} %collective-permute-done.23.refs_18_), channel_id=1, source_target_pairs={{8,0},{16,8},{24,16},{28,24},{20,28},{12,20},{4,12},{0,4},{9,1},{1... | collective-permute-start | bytes 786440 | tf_op jit(solution)/shard_map/ppermute | solution.py:317
  48.8 16.4 %collective-permute-start.22 = (bf16[2,256,256]{2,1,0:T(8,128)(2,1)S(1)}, bf16[2,256,256]{2,1,0:T(8,128)(2,1)S(1)}, u32[]{:S(2)}, u32[]{:S(2)}) collective-permute-start(bf16[2,256,256]{2,1,0:T(8,128)(2,1)S(1)} %collective-permute-done.21.refs_16_), channel_id=1, source_target_pairs={{0,2},{1,3},{2,0},{3,1},{4,6},{5,7},{6,4},{7,5},{8,10},{9,11},{10,... | collective-permute-start | bytes 786440 | tf_op jit(solution)/shard_map/ppermute | solution.py:358
  50.4 16.9 %collective-permute-start.24 = (bf16[2,256,256]{2,1,0:T(8,128)(2,1)S(1)}, bf16[2,256,256]{2,1,0:T(8,128)(2,1)S(1)}, u32[]{:S(2)}, u32[]{:S(2)}) collective-permute-start(bf16[2,256,256]{2,1,0:T(8,128)(2,1)S(1)} %collective-permute-done.23.refs_18_), channel_id=1, source_target_pairs={{0,2},{1,3},{2,0},{3,1},{4,6},{5,7},{6,4},{7,5},{8,10},{9,11},{10,... | collective-permute-start | bytes 786440 | tf_op jit(solution)/shard_map/ppermute | solution.py:358
  55.7 11.0 %collective-permute-start.29 = (bf16[256,256]{1,0:T(8,128)(2,1)S(1)}, bf16[256,256]{1,0:T(8,128)(2,1)S(1)}, u32[]{:S(2)}, u32[]{:S(2)}) collective-permute-start(bf16[256,256]{1,0:T(8,128)(2,1)S(1)} %slice_bitcast_fusion.3), channel_id=1, source_target_pairs={{0,8},{8,16},{16,24},{24,28},{28,20},{20,12},{12,4},{4,0},{1,9},{9... | collective-permute-start | bytes 393224 | tf_op jit(solution)/shard_map/ppermute | solution.py:316
  58.6 25.9 %collective-permute-start.26 = (bf16[2,256,256]{2,1,0:T(8,128)(2,1)S(1)}, bf16[2,256,256]{2,1,0:T(8,128)(2,1)S(1)}, u32[]{:S(2)}, u32[]{:S(2)}) collective-permute-start(bf16[2,256,256]{2,1,0:T(8,128)(2,1)S(1)} %collective-permute-done.25.refs_20_), channel_id=1, source_target_pairs={{0,2},{1,3},{2,0},{3,1},{4,6},{5,7},{6,4},{7,5},{8,10},{9,11},{10,... | collective-permute-start | bytes 786440 | tf_op jit(solution)/shard_map/ppermute | solution.py:358
  60.2 24.4 %collective-permute-start.28 = (bf16[2,256,256]{2,1,0:T(8,128)(2,1)S(1)}, bf16[2,256,256]{2,1,0:T(8,128)(2,1)S(1)}, u32[]{:S(2)}, u32[]{:S(2)}) collective-permute-start(bf16[2,256,256]{2,1,0:T(8,128)(2,1)S(1)} %collective-permute-done.27.refs_22_), channel_id=1, source_target_pairs={{0,2},{1,3},{2,0},{3,1},{4,6},{5,7},{6,4},{7,5},{8,10},{9,11},{10,... | collective-permute-start | bytes 786440 | tf_op jit(solution)/shard_map/ppermute | solution.py:358
  65.2 19.4 %collective-permute-start.15 = (bf16[416,256]{1,0:T(8,128)(2,1)S(1)}, bf16[416,256]{1,0:T(8,128)(2,1)S(1)}, u32[]{:S(2)}, u32[]{:S(2)}) collective-permute-start(bf16[416,256]{1,0:T(8,128)(2,1)S(1)} %get-tuple-element.21.refs_8_), channel_id=1, source_target_pairs={{0,2},{1,3},{2,0},{3,1},{4,6},{5,7},{6,4},{7,5},{8,10},{9,11},{10,... | collective-permute-start | bytes 638984 | tf_op jit(solution)/shard_map/ppermute | solution.py:358
  66.7 17.8 %collective-permute-start.30 = (bf16[256,256]{1,0:T(8,128)(2,1)S(1)}, bf16[256,256]{1,0:T(8,128)(2,1)S(1)}, u32[]{:S(2)}, u32[]{:S(2)}) collective-permute-start(bf16[256,256]{1,0:T(8,128)(2,1)S(1)} %collective-permute-done.29.refs_24_), channel_id=1, source_target_pairs={{0,2},{1,3},{2,0},{3,1},{4,6},{5,7},{6,4},{7,5},{8,10},{9,11},{10,... | collective-permute-start | bytes 393224 | tf_op jit(solution)/shard_map/ppermute | solution.py:358
  68.4 13.1 %collective-permute-start.13 = (f32[2,512]{1,0:T(2,128)S(1)}, f32[2,512]{1,0:T(2,128)S(1)}, u32[]{:S(2)}, u32[]{:S(2)}) collective-permute-start(f32[2,512]{1,0:T(2,128)S(1)} %get-tuple-element.20.refs_4_), channel_id=1, source_target_pairs={{0,2},{1,3},{2,0},{3,1},{4,6},{5,7},{6,4},{7,5},{8,10},{9,11},{10,... | collective-permute-start | bytes 12296 | tf_op jit(solution)/shard_map/ppermute | solution.py:427
  86.8 27.4 %collective-permute-start.31 = (bf16[416,2048]{1,0:T(8,128)(2,1)S(1)}, bf16[416,2048]{1,0:T(8,128)(2,1)S(1)}, u32[]{:S(2)}, u32[]{:S(2)}) collective-permute-start(bf16[416,2048]{1,0:T(8,128)(2,1)S(1)} %shard_map.95.refs_3_), channel_id=1, source_target_pairs={{0,1},{1,0},{2,3},{3,2},{4,5},{5,4},{6,7},{7,6},{8,9},{9,8},{10,11... | collective-permute-start | bytes 5111816 | tf_op jit(solution)/shard_map/ppermute | solution.py:437
  87.0 8.6 %collective-permute-start.32 = (bf16[2,256,256]{2,1,0:T(8,128)(2,1)S(1)}, bf16[2,256,256]{2,1,0:T(8,128)(2,1)S(1)}, u32[]{:S(2)}, u32[]{:S(2)}) collective-permute-start(bf16[2,256,256]{2,1,0:T(8,128)(2,1)S(1)} %get-tuple-element.24.refs_0_), channel_id=1, source_target_pairs={{0,8},{8,16},{16,24},{24,28},{28,20},{20,12},{12,4},{4,0},{1,9},{9... | collective-permute-start | bytes 786440 | tf_op jit(solution)/shard_map/ppermute | solution.py:316
  87.0 8.9 %collective-permute-start.33 = (bf16[2,256,256]{2,1,0:T(8,128)(2,1)S(1)}, bf16[2,256,256]{2,1,0:T(8,128)(2,1)S(1)}, u32[]{:S(2)}, u32[]{:S(2)}) collective-permute-start(bf16[2,256,256]{2,1,0:T(8,128)(2,1)S(1)} %get-tuple-element.24.refs_0_), channel_id=1, source_target_pairs={{8,0},{16,8},{24,16},{28,24},{20,28},{12,20},{4,12},{0,4},{9,1},{1... | collective-permute-start | bytes 786440 | tf_op jit(solution)/shard_map/ppermute | solution.py:317
  95.6 7.8 %collective-permute-start.34 = (bf16[2,256,256]{2,1,0:T(8,128)(2,1)S(1)}, bf16[2,256,256]{2,1,0:T(8,128)(2,1)S(1)}, u32[]{:S(2)}, u32[]{:S(2)}) collective-permute-start(bf16[2,256,256]{2,1,0:T(8,128)(2,1)S(1)} %collective-permute-done.32.refs_1_), channel_id=1, source_target_pairs={{0,8},{8,16},{16,24},{24,28},{28,20},{20,12},{12,4},{4,0},{1,9},{9... | collective-permute-start | bytes 786440 | tf_op jit(solution)/shard_map/ppermute | solution.py:316
  95.9 8.0 %collective-permute-start.35 = (bf16[2,256,256]{2,1,0:T(8,128)(2,1)S(1)}, bf16[2,256,256]{2,1,0:T(8,128)(2,1)S(1)}, u32[]{:S(2)}, u32[]{:S(2)}) collective-permute-start(bf16[2,256,256]{2,1,0:T(8,128)(2,1)S(1)} %collective-permute-done.33.refs_2_), channel_id=1, source_target_pairs={{8,0},{16,8},{24,16},{28,24},{20,28},{12,20},{4,12},{0,4},{9,1},{1... | collective-permute-start | bytes 786440 | tf_op jit(solution)/shard_map/ppermute | solution.py:317
  103.4 6.9 %collective-permute-start.36 = (bf16[2,256,256]{2,1,0:T(8,128)(2,1)S(1)}, bf16[2,256,256]{2,1,0:T(8,128)(2,1)S(1)}, u32[]{:S(2)}, u32[]{:S(2)}) collective-permute-start(bf16[2,256,256]{2,1,0:T(8,128)(2,1)S(1)} %collective-permute-done.34.refs_3_), channel_id=1, source_target_pairs={{0,8},{8,16},{16,24},{24,28},{28,20},{20,12},{12,4},{4,0},{1,9},{9... | collective-permute-start | bytes 786440 | tf_op jit(solution)/shard_map/ppermute | solution.py:316
  103.9 7.2 %collective-permute-start.37 = (bf16[2,256,256]{2,1,0:T(8,128)(2,1)S(1)}, bf16[2,256,256]{2,1,0:T(8,128)(2,1)S(1)}, u32[]{:S(2)}, u32[]{:S(2)}) collective-permute-start(bf16[2,256,256]{2,1,0:T(8,128)(2,1)S(1)} %collective-permute-done.35.refs_4_), channel_id=1, source_target_pairs={{8,0},{16,8},{24,16},{28,24},{20,28},{12,20},{4,12},{0,4},{9,1},{1... | collective-permute-start | bytes 786440 | tf_op jit(solution)/shard_map/ppermute | solution.py:317
  112.4 8.7 %collective-permute-start.44 = (bf16[256,256]{1,0:T(8,128)(2,1)S(1)}, bf16[256,256]{1,0:T(8,128)(2,1)S(1)}, u32[]{:S(2)}, u32[]{:S(2)}) collective-permute-start(bf16[256,256]{1,0:T(8,128)(2,1)S(1)} %slice_bitcast_fusion), channel_id=1, source_target_pairs={{8,0},{16,8},{24,16},{28,24},{20,28},{12,20},{4,12},{0,4},{9,1},{1... | collective-permute-start | bytes 393224 | tf_op jit(solution)/shard_map/ppermute | solution.py:317
  119.5 7.2 %collective-permute-start.43 = (bf16[384,256]{1,0:T(8,128)(2,1)S(1)}, bf16[384,256]{1,0:T(8,128)(2,1)S(1)}, u32[]{:S(2)}, u32[]{:S(2)}) collective-permute-start(bf16[384,256]{1,0:T(8,128)(2,1)S(1)} %get-tuple-element.26.refs_8_), channel_id=1, source_target_pairs={{0,2},{1,3},{2,0},{3,1},{4,6},{5,7},{6,4},{7,5},{8,10},{9,11},{10,... | collective-permute-start | bytes 589832 | tf_op jit(solution)/shard_map/ppermute | solution.py:358
  (24 other events, 241.7 us)

commit v3 on v2

--- a/solution.py
+++ b/solution.py
@@ -17,6 +17,8 @@
 KERNEL_VMEM = 20 * 2**20
 PACK_FLOPS = 2 * 10**9
 PACK_BYTES = 8 * 10**6
+PRODUCTS_AHEAD = (5, 7)
+SHARE_PARTS = 2
 
 
 wide = jnp.float32
@@ -29,6 +31,10 @@
 
 def in_vmem():
     return pl.BlockSpec(memory_space=pltpu.VMEM)
+
+
+def in_smem():
+    return pl.BlockSpec(memory_space=pltpu.SMEM)
 
 
 def in_hbm():
@@ -40,7 +46,9 @@
         body,
         out_shape=out_shape,
         in_specs=in_specs,
-        out_specs=jax.tree.map(lambda _: in_vmem(), out_shape),
+        out_specs=jax.tree.map(
+            lambda shape: in_smem() if len(shape.shape) == 1 else in_vmem(), out_shape
+        ),
         scratch_shapes=list(scratch_shapes),
         compiler_params=pltpu.CompilerParams(vmem_limit_bytes=KERNEL_VMEM),
     )
@@ -109,8 +117,9 @@
     )(value_proj, gate_proj, *extra)
 
 
-def norm_body(tail, near, tokens_ref, docs_ref, gain_ref, *refs):
-    prev_refs, (normed_ref, dist_ref, state_ref, run_ref) = refs[:near], refs[near:]
+def norm_body(tail, near, tap_count, tokens_ref, docs_ref, gain_ref, *refs):
+    prev_refs, refs = refs[:near], refs[near:]
+    normed_ref, dist_ref, state_ref, flags_ref, run_ref = refs
     row_count, model_width = tokens_ref.shape
     halo = normed_ref.shape[0] - row_count
     part = halo // near
@@ -140,6 +149,9 @@
         run = jnp.where(run == reach, reach + run_ref[lead - reach : lead - reach + rows, :], run)
         reach = 2 * reach
     dist_ref[...] = run[tail:, :]
+    for k in range(flags_ref.shape[0]):
+        least = jnp.min(run[tail + k * CONV_ROWS : tail + (k + 1) * CONV_ROWS, :])
+        flags_ref[k] = (least >= tap_count - 1).astype(jnp.int32)
 
 
 def chunk_start(places, k, size):
@@ -149,28 +161,39 @@
     return pl.multiple_of(ring_place(count, steps[k]) * size, LANES)
 
 
+def add_products(acc_ref, start_ref, normed_ref, pairs, places, first_step):
+    depth = pairs[0][0].shape[0]
+    for k, pair in enumerate(pairs):
+        first = chunk_start(places, first_step + k, depth)
+        rows_in = normed_ref[:, pl.ds(first, depth)]
+        for part in range(2):
+            product = jnp.dot(rows_in, pair[part][...], preferred_element_type=wide)
+            if k == 0:
+                acc_ref[part] = product if start_ref is None else start_ref[part] + product
+            else:
+                acc_ref[part] += product
+
+
+def products_body(places, normed_ref, *refs):
+    *pair_refs, acc_ref = refs
+    pairs = [(pair.at[0], pair.at[1]) for pair in pair_refs]
+    add_products(acc_ref, None, normed_ref, pairs, places, 0)
+
+
 def gated_conv_body(
-    layer, tap_count, tail, places, normed_ref, dist_ref, taps_ref, *refs
+    layer, tap_count, tail, places, done, halved, flags_ref, normed_ref, dist_ref, taps_ref, *refs
 ):
+    start_ref, refs = (refs[0], refs[1:]) if done else (None, refs)
     *pair_refs, centred_ref, stats_ref, acc_ref, shifted_ref, conv_ref = refs
-    pairs = [(pair.at[0], pair.at[1]) for pair in (pair_refs[:-2] if places else pair_refs)]
-    if places:
+    pairs = [(pair.at[0], pair.at[1]) for pair in (pair_refs[:-2] if halved else pair_refs)]
+    if halved:
         pairs.append(tuple(pair_refs[-2:]))
     width = taps_ref.shape[2]
     halves = width // LANES
     rows = normed_ref.shape[0]
-    out_rows = centred_ref.shape[0]
+    out_rows = rows - tail
     dist_from = dist_ref.shape[0] - out_rows
-    depth = pair_refs[0].shape[1]
-    for k, pair in enumerate(pairs):
-        first = chunk_start(places, k, depth)
-        rows_in = normed_ref[:, pl.ds(first, depth)]
-        for part in range(2):
-            product = jnp.dot(rows_in, pair[part][...], preferred_element_type=wide)
-            if k == 0:
-                acc_ref[part] = product
-            else:
-                acc_ref[part] += product
+    add_products(acc_ref, start_ref, normed_ref, pairs, places, done)
     for half in range(halves):
         cols = slice(half * LANES, (half + 1) * LANES)
         value = acc_ref[0, :, cols].astype(narrow).astype(wide)
@@ -185,17 +208,31 @@
 
     def block(index, carry):
         base = pl.multiple_of(index * CONV_ROWS, CONV_ROWS)
-        dist = dist_ref[pl.ds(pl.multiple_of(base + dist_from, CONV_ROWS), CONV_ROWS), :]
-        sums = [jnp.zeros((CONV_ROWS, LANES), wide) for _ in range(halves)]
-        for tap in range(tap_count):
-            inside = dist >= tap
-            start = pl.multiple_of(base + (tail - tap // SUBLANES * SUBLANES), SUBLANES)
+        whole = flags_ref[index + dist_from // CONV_ROWS]
+
+        def convolved(masked):
+            sums = [jnp.zeros((CONV_ROWS, LANES), wide) for _ in range(halves)]
+            if masked:
+                dist = dist_ref[pl.ds(pl.multiple_of(base + dist_from, CONV_ROWS), CONV_ROWS), :]
+            for tap in range(tap_count):
+                start = pl.multiple_of(base + (tail - tap // SUBLANES * SUBLANES), SUBLANES)
+                for half in range(halves):
+                    term = (
+                        taps_ref[tap, layer : layer + 1, half * LANES : (half + 1) * LANES]
+                        * shifted_ref[half, tap % SUBLANES, pl.ds(start, CONV_ROWS), :]
+                    )
+                    sums[half] = sums[half] + (jnp.where(dist >= tap, term, 0.0) if masked else term)
             for half in range(halves):
-                rows_at = shifted_ref[half, tap % SUBLANES, pl.ds(start, CONV_ROWS), :]
-                weight = taps_ref[tap, layer : layer + 1, half * LANES : (half + 1) * LANES]
-                sums[half] = sums[half] + jnp.where(inside, weight * rows_at, 0.0)
-        for half in range(halves):
-            conv_ref[half, pl.ds(base, CONV_ROWS), :] = sums[half]
+                conv_ref[half, pl.ds(base, CONV_ROWS), :] = sums[half]
+
+        @pl.when(whole == 1)
+        def _():
+            convolved(False)
+
+        @pl.when(whole == 0)
+        def _():
+            convolved(True)
+
         return carry
 
     lax.fori_loop(0, out_rows // CONV_ROWS, block, 0)
@@ -221,11 +258,8 @@
     return functools.reduce(jnp.add, values)
 
 
-def project_body(layer, near, far, slots, places, *refs):
-    gain_refs, shift_refs, refs = refs[:far], refs[far : 2 * far], refs[2 * far :]
-    stats_refs, refs = refs[: far * near], refs[far * near :]
-    centred_refs, refs = refs[:far], refs[far:]
-    *piece_refs, share_ref, act_ref = refs
+def activate(layer, near, gain_refs, shift_refs, stats_refs, centred_refs, act_ref):
+    far = len(centred_refs)
     out_rows, width = centred_refs[0].shape
     count = far * near
     fill = jnp.zeros((round_up(2 * count, SUBLANES) - 2 * count, stats_refs[0].shape[1]), wide)
@@ -238,12 +272,22 @@
     square = summed([summed(squares[f * near : (f + 1) * near]) for f in range(far)])
     scale = lax.rsqrt(square / (width * count) + epsilon)
     for f, centred in enumerate(centred_refs):
-        own = means[f * near]
         gain, shift = gain_refs[f][layer : layer + 1, :], shift_refs[f][layer : layer + 1, :]
-        normal = gain * (centred[...].astype(wide) + (own - mean)) * scale + shift
+        normal = gain * (centred[...].astype(wide) + (means[f * near] - mean)) * scale + shift
         act_ref[f] = (normal * jax.nn.sigmoid(normal)).astype(narrow)
-    steps = len(slots) // far
-    for k in range(steps):
+
+
+def project_body(layer, near, far, slots, places, is_first, *refs):
+    if is_first:
+        gain_refs, shift_refs, refs = refs[:far], refs[far : 2 * far], refs[2 * far :]
+        stats_refs, refs = refs[: far * near], refs[far * near :]
+        centred_refs, refs = refs[:far], refs[far:]
+        *piece_refs, share_ref, act_ref = refs
+        activate(layer, near, gain_refs, shift_refs, stats_refs, centred_refs, act_ref)
+    else:
+        act_ref, *piece_refs, share_ref = refs
+    at = 0
+    for k in range(len(slots) // far):
         share = None
         for f in range(far):
             piece, slot = piece_refs[k * far + f], slots[k * far + f]
@@ -251,36 +295,68 @@
             product = jnp.dot(act_ref[f], matrix, preferred_element_type=wide)
             share = product if share is None else share + product
         cols = share.shape[1]
-        first = chunk_start(places, k, cols)
+        first = at if places is None else chunk_start(places, k, cols)
         share_ref[:, pl.ds(first, cols)] = share.astype(narrow)
-
-
-def add_body(layer, tail, is_last, state_count, *refs):
+        at = at + cols
+
+
+def add_body(layer, tail, with_norm, state_count, *refs):
     state_refs, refs = refs[:state_count], refs[state_count:]
-    if is_last:
+    if with_norm:
+        gain_ref, *share_refs, hidden_ref, normed_ref = refs
+    else:
         *share_refs, hidden_ref = refs
-    else:
-        gain_ref, *share_refs, hidden_ref, normed_ref = refs
-    skip, at = tail, 0
-    model_width = hidden_ref.shape[1]
+    skip, row = tail, 0
     for state_ref in state_refs:
-        rows = state_ref.shape[0]
-        from_row = min(skip, rows)
+        from_row = min(skip, state_ref.shape[0])
         skip = skip - from_row
-        count = rows - from_row
+        count = state_ref.shape[0] - from_row
         if count == 0:
             continue
-        branch = share_refs[0][at : at + count, :].astype(wide)
-        for share in share_refs[1:]:
-            branch = branch + share[at : at + count, :].astype(wide)
-        hidden = (
-            state_ref[from_row:, :model_width].astype(wide) + branch.astype(narrow).astype(wide)
-        ).astype(narrow)
-        hidden_ref[at : at + count, :] = hidden
-        if not is_last:
+        branch = summed([ref[row : row + count, :].astype(wide) for ref in share_refs])
+        state = state_ref[from_row:, :].astype(wide)
+        hidden = (state + branch.astype(narrow).astype(wide)).astype(narrow)
+        hidden_ref[row : row + count, :] = hidden
+        if with_norm:
             gain = gain_ref[layer + 1 : layer + 2, :]
-            normed_ref[at : at + count, :] = normed_of(hidden.astype(wide), gain)
-        at = at + count
+            normed_ref[row : row + count, :] = normed_of(hidden.astype(wide), gain)
+        row = row + count
+
+
+def add_part_body(tail, places, first_step, steps, has_rest, *refs):
+    state_ref, *share_refs = refs[: -3 - has_rest]
+    hidden_ref, sum_ref, sems = refs[-3:]
+    cols = share_refs[0].shape[1] // steps
+    copies = []
+    for k in range(steps):
+        at = slice(k * cols, (k + 1) * cols)
+        start = chunk_start(places, first_step + k, cols)
+        branch = summed([ref[:, at].astype(wide) for ref in share_refs])
+        state = state_ref[tail:, pl.ds(start, cols)].astype(wide)
+        sum_ref[:, at] = (state + branch.astype(narrow).astype(wide)).astype(narrow)
+        copies.append(
+            pltpu.make_async_copy(
+                sum_ref.at[:, pl.ds(k * cols, cols)], hidden_ref.at[:, pl.ds(start, cols)], sems.at[k]
+            )
+        )
+        copies[-1].start()
+    for copy in copies:
+        copy.wait()
+
+
+def added_part(tail, places, first_step, steps, state, shares, rest, shape):
+    return pl.pallas_call(
+        functools.partial(add_part_body, tail, places, first_step, steps, len(rest)),
+        out_shape=shape,
+        in_specs=[in_vmem()] * (1 + len(shares)) + [pl.BlockSpec(memory_space=pl.ANY)] * len(rest),
+        out_specs=pl.BlockSpec(memory_space=pl.ANY),
+        scratch_shapes=[
+            pltpu.VMEM(shares[0].shape, narrow),
+            pltpu.SemaphoreType.DMA((steps,)),
+        ],
+        input_output_aliases={1 + len(shares): 0} if rest else {},
+        compiler_params=pltpu.CompilerParams(vmem_limit_bytes=KERNEL_VMEM),
+    )(state, *shares, *rest)
 
 
 def ring_place(count, step):
@@ -391,12 +467,13 @@
     places = (sp_count, ring_tables(sp_count)[2]) if in_ring else None
 
     taps = jnp.transpose(conv_taps, (1, 0, 2))
-    normed, dist, prev_state = kernel(
-        functools.partial(norm_body, tail, near),
+    normed, dist, prev_state, flags = kernel(
+        functools.partial(norm_body, tail, near, tap_count),
         (
             jax.ShapeDtypeStruct((halo + row_count, model_width), narrow),
             jax.ShapeDtypeStruct((halo + row_count - tail, LANES), wide),
             jax.ShapeDtypeStruct((halo, model_width), narrow),
+            jax.ShapeDtypeStruct(((halo + row_count - tail) // CONV_ROWS,), jnp.int32),
         ),
         [in_vmem()] * (3 + near),
         [pltpu.VMEM((tail + halo + row_count, LANES), wide)],
@@ -407,39 +484,77 @@
         rows = normed.shape[0]
         out_rows = rows - tail
         pairs = pair_chunks[n]
+        done = PRODUCTS_AHEAD[n % 2] if in_ring else 0
+        start = ()
+        if done:
+            start = (
+                kernel(
+                    functools.partial(products_body, places),
+                    jax.ShapeDtypeStruct((2, rows, width), wide),
+                    [in_vmem()] * (1 + done),
+                )(normed, *pairs[:done]),
+            )
         centred, stats = kernel(
-            functools.partial(gated_conv_body, n, tap_count, tail, places),
+            functools.partial(gated_conv_body, n, tap_count, tail, places, done, in_ring),
             (
                 jax.ShapeDtypeStruct((out_rows, width), narrow),
                 jax.ShapeDtypeStruct((2, round_up(out_rows, LANES)), wide),
             ),
-            [in_vmem()] * (3 + len(pairs)),
+            [in_smem()] + [in_vmem()] * (3 + len(start) + len(pairs) - done),
             [
                 pltpu.VMEM((2, rows, width), wide),
                 pltpu.VMEM((width // LANES, SUBLANES, rows, LANES), wide),
                 pltpu.VMEM((width // LANES, out_rows, LANES), wide),
             ],
-        )(normed, dist, taps, *pairs)
-        far_centred = far_values(centred)
+        )(flags, normed, dist, taps, *start, *pairs[done:])
         all_stats = [stats]
         for place in range(1, tp_count):
             steps = group_pairs(tp_count, near, far, place % near, place // near)
             all_stats.append(lax.ppermute(stats, "tp", steps))
         pieces = out_pieces[n]
-        share = kernel(
-            functools.partial(project_body, n, near, far, out_slots[n], places),
-            jax.ShapeDtypeStruct((out_rows, model_width), narrow),
-            [in_vmem()] * (3 * far + tp_count + len(pieces)),
-            [pltpu.VMEM((far, out_rows, width), narrow)],
-        )(*gains, *shifts, *all_stats, *far_centred, *pieces)
-        shares = [share]
-        for _ in range(1, near):
-            shares.append(lax.ppermute(shares[-1], "tp", near_pairs))
+        far_centred = far_values(centred)
+        chunk_count = len(pieces) // far
         is_last = n == layer_count - 1
+        part_count = SHARE_PARTS if is_last and n > 0 and chunk_count % SHARE_PARTS == 0 else 1
+        shares, act = [], ()
+        for part in range(part_count):
+            own = slice(
+                part * chunk_count // part_count * far, (part + 1) * chunk_count // part_count * far
+            )
+            shape = jax.ShapeDtypeStruct((out_rows, model_width // part_count), narrow)
+            act_shape = jax.ShapeDtypeStruct((far, out_rows, width), narrow)
+            keeps_act = part_count > 1 and not act
+            inputs = act or (*gains, *shifts, *all_stats, *far_centred)
+            share, *rest = kernel(
+                functools.partial(
+                    project_body,
+                    n,
+                    near,
+                    far,
+                    out_slots[n][own],
+                    places if part_count == 1 else None,
+                    not act,
+                ),
+                (shape,) + ((act_shape,) if keeps_act else ()),
+                [in_vmem()] * (len(inputs) + len(pieces[own])),
+                [] if act or keeps_act else [pltpu.VMEM(act_shape.shape, narrow)],
+            )(*inputs, *pieces[own])
+            act = act or tuple(rest)
+            shares.append(share)
+            for _ in range(1, near):
+                shares.append(lax.ppermute(shares[-1], "tp", near_pairs))
         shape = jax.ShapeDtypeStruct((out_rows, model_width), narrow)
+        if part_count > 1:
+            rest, steps = (), chunk_count // part_count
+            for part in range(part_count):
+                own = shares[part * near : (part + 1) * near]
+                rest = (
+                    added_part(tail, places, part * steps, steps, states[0], own, rest, shape),
+                )
+            return rest[0]
         next_gain = () if is_last else (pre_gain,)
         result = kernel(
-            functools.partial(add_body, n, tail, is_last, len(states)),
+            functools.partial(add_body, n, tail, not is_last, len(states)),
             shape if is_last else (shape, shape),
             [in_vmem()] * (len(states) + len(next_gain) + len(shares)),
         )(*states, *next_gain, *shares)

time: 134 us -> 133 us (level)
  waiting for transfers between devices: 62 us -> 58.1 us
  Pallas kernels: 16.1 us -> 17.9 us
    ppermute x13, waiting for transfers between devices: 9.21 us -> 5.96 us  [far_values(): values.append(lax.ppermute(values[-1], 'tp', far_pairs))]
    ppermute x2 -> x3, waiting for transfers between devices: 3.3 us -> 1.13 us  [on_device(): shares.append(lax.ppermute(shares[-1], 'tp', near_pairs))]
    ppermute x6, waiting for transfers between devices: 15.8 us -> 17.9 us  [on_device(): all_stats.append(lax.ppermute(stats, 'tp', steps))]
    pallas_call x7 -> x11, Pallas kernels: 15.2 us -> 17.1 us  [the longest x2 5.62 us: on_device(): kernel(functools.partial(gated_conv_body, n, tap_count, tail, places, don...]
  transfers between devices with their start and end apart: 47 -> 48, of which waited for: 17 -> 16; matrix products, arithmetic and copies ran while one was open for 0% -> 0% of each run, Pallas kernels for 7% -> 11%
where the time goes in v3:
time: 133 us
  waiting for transfers between devices  58.1 us (44%)
  starting transfers between devices  54 us (41%)
  Pallas kernels  17.9 us (13%)
  local copies, waits for them, and re-layouts  2.17 us (2%)
    ppermute x12, waiting for transfers between devices, ring_gathered(): ahead = lax.ppermute(ahead, 'sp', forward)  25.1 us
    ppermute x12, starting transfers between devices, ring_gathered(): behind = lax.ppermute(behind, 'sp', backward)  22.4 us
    ppermute x6, waiting for transfers between devices, on_device(): all_stats.append(lax.ppermute(stats, 'tp', steps))  17.9 us
    ppermute x13, starting transfers between devices, far_values(): values.append(lax.ppermute(values[-1], 'tp', far_pairs))  15.9 us
    ppermute x12, starting transfers between devices, ring_gathered(): ahead = lax.ppermute(ahead, 'sp', forward)  9.53 us
    ppermute x12, waiting for transfers between devices, ring_gathered(): behind = lax.ppermute(behind, 'sp', backward)  7.99 us
    ppermute x13, waiting for transfers between devices, far_values(): values.append(lax.ppermute(values[-1], 'tp', far_pairs))  5.96 us
    pallas_call x2, Pallas kernels, on_device(): kernel(functools.partial(gated_conv_body, n, tap_count, tail, places, don...  5.62 us
  transfers between devices with their start and end apart: 48, of which 16 were waited for; matrix products, arithmetic and copies ran while one was open for 0% of the time, Pallas kernels for 11%

profile of v3, /device:TPU:0, one launch (start us, length us, event | category | flops | bytes accessed | tf_op | source)
XLA Modules:
  0.0 132.6 jit_solution(15666385351531947509)
XLA Ops:
  2.4 3.1 %collective-permute-start.4 = (bf16[2,256,256]{2,1,0:T(8,128)(2,1)S(1)}, bf16[2,256,256]{2,1,0:T(8,128)(2,1)S(1)}, u32[]{:S(2)}, u32[]{:S(2)}) collective-permute-start(bf16[2,256,256]{2,1,0:T(8,128)(2,1)S(1)} %shard_map.93.refs_0_), channel_id=1, source_target_pairs={{0,8},{8,16},{16,24},{24,28},{28,20},{20,12},{12,4},{4,0},{1,9},{9... | collective-permute-start | bytes 786440 | tf_op jit(solution)/shard_map/ppermute | solution.py:392
  5.5 2.0 %collective-permute-start.17 = (bf16[2,256,256]{2,1,0:T(8,128)(2,1)S(1)}, bf16[2,256,256]{2,1,0:T(8,128)(2,1)S(1)}, u32[]{:S(2)}, u32[]{:S(2)}) collective-permute-start(bf16[2,256,256]{2,1,0:T(8,128)(2,1)S(1)} %copy-done.1), channel_id=1, source_target_pairs={{0,8},{8,16},{16,24},{24,28},{28,20},{20,12},{12,4},{4,0},{1,9},{9... | collective-permute-start | bytes 786440 | tf_op jit(solution)/shard_map/ppermute | solution.py:392
  7.5 5.0 %collective-permute-done.4.refs_1_ = bf16[2,256,256]{2,1,0:T(8,128)(2,1)S(1)} collective-permute-done((bf16[2,256,256]{2,1,0:T(8,128)(2,1)S(1)}, bf16[2,256,256]{2,1,0:T(8,128)(2,1)S(1)}, u32[]{:S(2)}, u32[]{:S(2)}) %collective-permute-start.4) | collective-permute-done | bytes 262176 | tf_op jit(solution)/shard_map/ppermute | solution.py:392
  12.6 2.1 %collective-permute-start.6 = (bf16[2,256,256]{2,1,0:T(8,128)(2,1)S(1)}, bf16[2,256,256]{2,1,0:T(8,128)(2,1)S(1)}, u32[]{:S(2)}, u32[]{:S(2)}) collective-permute-start(bf16[2,256,256]{2,1,0:T(8,128)(2,1)S(1)} %collective-permute-done.4.refs_1_), channel_id=1, source_target_pairs={{0,8},{8,16},{16,24},{24,28},{28,20},{20,12},{12,4},{4,0},{1,9},{9... | collective-permute-start | bytes 786440 | tf_op jit(solution)/shard_map/ppermute | solution.py:392
  15.2 1.8 %collective-permute-start = (bf16[32,2176]{1,0:T(8,128)(2,1)S(1)}, bf16[32,2176]{1,0:T(8,128)(2,1)S(1)}, u32[]{:S(2)}, u32[]{:S(2)}) collective-permute-start(bf16[32,2176]{1,0:T(8,128)(2,1)S(1)} %get-tuple-element.19), channel_id=1, source_target_pairs={{0,4},{4,8},{8,12},{12,16},{16,20},{20,24},{24,28},{1,5},{5,9},{9,... | collective-permute-start | bytes 417800 | tf_op jit(solution)/shard_map/ppermute | solution.py:463
  17.1 2.1 %collective-permute-start.2 = (f32[2,256]{1,0:T(2,128)S(1)}, f32[2,256]{1,0:T(2,128)S(1)}, u32[]{:S(2)}, u32[]{:S(2)}) collective-permute-start(f32[2,256]{1,0:T(2,128)S(1)} %copy-done.4), channel_id=1, source_target_pairs={{0,2},{1,3},{2,0},{3,1},{4,6},{5,7},{6,4},{7,5},{8,10},{9,11},{10,... | collective-permute-start | bytes 6152 | tf_op jit(solution)/shard_map/ppermute | solution.py:434
  20.8 2.0 %collective-permute-start.3 = (f32[2,256]{1,0:T(2,128)S(1)}, f32[2,256]{1,0:T(2,128)S(1)}, u32[]{:S(2)}, u32[]{:S(2)}) collective-permute-start(f32[2,256]{1,0:T(2,128)S(1)} %copy-done.5), channel_id=1, source_target_pairs={{0,2},{1,3},{2,0},{3,1},{4,6},{5,7},{6,4},{7,5},{8,10},{9,11},{10,... | collective-permute-start | bytes 6152 | tf_op jit(solution)/shard_map/ppermute | solution.py:434
  24.3 3.1 %collective-permute-start.19 = (bf16[2,256,256]{2,1,0:T(8,128)(2,1)S(1)}, bf16[2,256,256]{2,1,0:T(8,128)(2,1)S(1)}, u32[]{:S(2)}, u32[]{:S(2)}) collective-permute-start(bf16[2,256,256]{2,1,0:T(8,128)(2,1)S(1)} %copy-done.1), channel_id=1, source_target_pairs={{8,0},{16,8},{24,16},{28,24},{20,28},{12,20},{4,12},{0,4},{9,1},{1... | collective-permute-start | bytes 786440 | tf_op jit(solution)/shard_map/ppermute | solution.py:393
  31.0 3.1 %collective-permute-done.19.refs_14_ = bf16[2,256,256]{2,1,0:T(8,128)(2,1)S(1)} collective-permute-done((bf16[2,256,256]{2,1,0:T(8,128)(2,1)S(1)}, bf16[2,256,256]{2,1,0:T(8,128)(2,1)S(1)}, u32[]{:S(2)}, u32[]{:S(2)}) %collective-permute-start.19) | collective-permute-done | bytes 262176 | tf_op jit(solution)/shard_map/ppermute | solution.py:393
  34.1 2.5 %collective-permute-start.23 = (bf16[2,256,256]{2,1,0:T(8,128)(2,1)S(1)}, bf16[2,256,256]{2,1,0:T(8,128)(2,1)S(1)}, u32[]{:S(2)}, u32[]{:S(2)}) collective-permute-start(bf16[2,256,256]{2,1,0:T(8,128)(2,1)S(1)} %collective-permute-done.19.refs_14_), channel_id=1, source_target_pairs={{8,0},{16,8},{24,16},{28,24},{20,28},{12,20},{4,12},{0,4},{9,1},{1... | collective-permute-start | bytes 786440 | tf_op jit(solution)/shard_map/ppermute | solution.py:393
  36.6 3.1 %collective-permute-done.7.refs_4_ = bf16[2,256,256]{2,1,0:T(8,128)(2,1)S(1)} collective-permute-done((bf16[2,256,256]{2,1,0:T(8,128)(2,1)S(1)}, bf16[2,256,256]{2,1,0:T(8,128)(2,1)S(1)}, u32[]{:S(2)}, u32[]{:S(2)}) %collective-permute-start.7) | collective-permute-done | bytes 262176 | tf_op jit(solution)/shard_map/ppermute | solution.py:393
  39.7 2.5 %collective-permute-start.9 = (bf16[2,256,256]{2,1,0:T(8,128)(2,1)S(1)}, bf16[2,256,256]{2,1,0:T(8,128)(2,1)S(1)}, u32[]{:S(2)}, u32[]{:S(2)}) collective-permute-start(bf16[2,256,256]{2,1,0:T(8,128)(2,1)S(1)} %collective-permute-done.7.refs_4_), channel_id=1, source_target_pairs={{8,0},{16,8},{24,16},{28,24},{20,28},{12,20},{4,12},{0,4},{9,1},{1... | collective-permute-start | bytes 786440 | tf_op jit(solution)/shard_map/ppermute | solution.py:393
  44.4 1.7 %collective-permute-done.9.refs_2_ = bf16[2,256,256]{2,1,0:T(8,128)(2,1)S(1)} collective-permute-done((bf16[2,256,256]{2,1,0:T(8,128)(2,1)S(1)}, bf16[2,256,256]{2,1,0:T(8,128)(2,1)S(1)}, u32[]{:S(2)}, u32[]{:S(2)}) %collective-permute-start.9) | collective-permute-done | bytes 262176 | tf_op jit(solution)/shard_map/ppermute | solution.py:393
  46.1 2.5 %collective-permute-start.27 = (bf16[2,256,256]{2,1,0:T(8,128)(2,1)S(1)}, bf16[2,256,256]{2,1,0:T(8,128)(2,1)S(1)}, u32[]{:S(2)}, u32[]{:S(2)}) collective-permute-start(bf16[2,256,256]{2,1,0:T(8,128)(2,1)S(1)} %collective-permute-done.23.refs_18_.refs_1_), channel_id=1, source_target_pairs={{8,0},{16,8},{24,16},{28,24},{20,28},{12,20},{4,12},{0,4},{9,1},{1... | collective-permute-start | bytes 786440 | tf_op jit(solution)/shard_map/ppermute | solution.py:393
  50.7 2.8 %collective-permute-done.20.refs_15_ = bf16[2,256,256]{2,1,0:T(8,128)(2,1)S(1)} collective-permute-done((bf16[2,256,256]{2,1,0:T(8,128)(2,1)S(1)}, bf16[2,256,256]{2,1,0:T(8,128)(2,1)S(1)}, u32[]{:S(2)}, u32[]{:S(2)}) %collective-permute-start.20) | collective-permute-done | bytes 262176 | tf_op jit(solution)/shard_map/ppermute | solution.py:434
  53.5 2.0 %collective-permute-start.11 = (bf16[256,256]{1,0:T(8,128)(2,1)S(1)}, bf16[256,256]{1,0:T(8,128)(2,1)S(1)}, u32[]{:S(2)}, u32[]{:S(2)}) collective-permute-start(bf16[256,256]{1,0:T(8,128)(2,1)S(1)} %slice_bitcast_fusion.4), channel_id=1, source_target_pairs={{8,0},{16,8},{24,16},{28,24},{20,28},{12,20},{4,12},{0,4},{9,1},{1... | collective-permute-start | bytes 393224 | tf_op jit(solution)/shard_map/ppermute | solution.py:393
  55.6 2.8 %collective-permute-done.10.refs_3_ = bf16[256,256]{1,0:T(8,128)(2,1)S(1)} collective-permute-done((bf16[256,256]{1,0:T(8,128)(2,1)S(1)}, bf16[256,256]{1,0:T(8,128)(2,1)S(1)}, u32[]{:S(2)}, u32[]{:S(2)}) %collective-permute-start.10) | collective-permute-done | bytes 131104 | tf_op jit(solution)/shard_map/ppermute | solution.py:392
  60.5 1.7 %shard_map.92 = (bf16[448,2048]{1,0:T(8,128)(2,1)S(1)}, f32[416,128]{1,0:T(8,128)S(1)}, bf16[64,2048]{1,0:T(8,128)(2,1)S(1)}, s32[13]{0:T(128)S(1)}) custom-call(bf16[384,2048]{1,0:T(8,128)(2,1)S(1)} %copy-done, s32[384]{0:T(512)S(1)} %copy-done.6, f32[2,2048]{1,0:T(2,128)S(1)} %copy-done.3, bf16[32,2176]{1,0:T(8,128)(2,1)S(1)} %collective-permute-done.refs_0_, ...), custom_call_target="tpu_custom_call" | custom-call | tf_op jit(solution)/shard_map/pallas_call | solution.py:470
  63.1 3.0 %shard_map.95 = (bf16[416,256]{1,0:T(8,128)(2,1)S(1)}, f32[2,512]{1,0:T(2,128)S(1)}) custom-call(s32[13]{0:T(128)S(1)} %get-tuple-element.21.flags_ref, bf16[448,2048]{1,0:T(8,128)(2,1)S(1)} %get-tuple-element.22.normed_ref, f32[416,128]{1,0:T(8,128)S(1)} %get-tuple-element.23.dist_ref, f32[31,2,256]{2,1,0:T(2,128)S(1)} %bitcast.13, ...), custom_call_target="tpu_custom_call" | custom-call | tf_op jit(solution)/shard_map/pallas_call | solution.py:497
  70.9 10.5 %collective-permute-done.13.refs_6_ = f32[2,512]{1,0:T(2,128)S(1)} collective-permute-done((f32[2,512]{1,0:T(2,128)S(1)}, f32[2,512]{1,0:T(2,128)S(1)}, u32[]{:S(2)}, u32[]{:S(2)}) %collective-permute-start.13) | collective-permute-done | bytes 4128 | tf_op jit(solution)/shard_map/ppermute | solution.py:513
  81.3 3.0 %collective-permute-done.14.refs_7_ = f32[2,512]{1,0:T(2,128)S(1)} collective-permute-done((f32[2,512]{1,0:T(2,128)S(1)}, f32[2,512]{1,0:T(2,128)S(1)}, u32[]{:S(2)}, u32[]{:S(2)}) %collective-permute-start.14) | collective-permute-done | bytes 4128 | tf_op jit(solution)/shard_map/ppermute | solution.py:513
  84.4 2.3 %shard_map.96.refs_3_ = bf16[416,2048]{1,0:T(8,128)(2,1)S(1)} custom-call(f32[2,256]{1,0:T(2,128)S(1)} %copy-done.4, f32[2,256]{1,0:T(2,128)S(1)} %collective-permute-done.2.refs_1_, f32[2,256]{1,0:T(2,128)S(1)} %copy-done.5, f32[2,256]{1,0:T(2,128)S(1)} %collective-permute-done.3.refs_3_, f32[2,512]{1,0:T(2,128)S(1)} %get-tuple-element.24.refs_4_, ...), custom_call_target="tpu_custom_call" | custom-call | tf_op jit(solution)/shard_map/pallas_call | solution.py:528
  86.9 2.0 %collective-permute-start.33 = (bf16[2,256,256]{2,1,0:T(8,128)(2,1)S(1)}, bf16[2,256,256]{2,1,0:T(8,128)(2,1)S(1)}, u32[]{:S(2)}, u32[]{:S(2)}) collective-permute-start(bf16[2,256,256]{2,1,0:T(8,128)(2,1)S(1)} %get-tuple-element.28.refs_0_), channel_id=1, source_target_pairs={{8,0},{16,8},{24,16},{28,24},{20,28},{12,20},{4,12},{0,4},{9,1},{1... | collective-permute-start | bytes 786440 | tf_op jit(solution)/shard_map/ppermute | solution.py:393
  88.9 6.6 %collective-permute-done.32.refs_1_ = bf16[2,256,256]{2,1,0:T(8,128)(2,1)S(1)} collective-permute-done((bf16[2,256,256]{2,1,0:T(8,128)(2,1)S(1)}, bf16[2,256,256]{2,1,0:T(8,128)(2,1)S(1)}, u32[]{:S(2)}, u32[]{:S(2)}) %collective-permute-start.32) | collective-permute-done | bytes 262176 | tf_op jit(solution)/shard_map/ppermute | solution.py:392
  95.8 1.7 %collective-permute-start.35 = (bf16[2,256,256]{2,1,0:T(8,128)(2,1)S(1)}, bf16[2,256,256]{2,1,0:T(8,128)(2,1)S(1)}, u32[]{:S(2)}, u32[]{:S(2)}) collective-permute-start(bf16[2,256,256]{2,1,0:T(8,128)(2,1)S(1)} %collective-permute-done.33.refs_2_), channel_id=1, source_target_pairs={{8,0},{16,8},{24,16},{28,24},{20,28},{12,20},{4,12},{0,4},{9,1},{1... | collective-permute-start | bytes 786440 | tf_op jit(solution)/shard_map/ppermute | solution.py:393
  97.5 5.7 %collective-permute-done.34.refs_3_ = bf16[2,256,256]{2,1,0:T(8,128)(2,1)S(1)} collective-permute-done((bf16[2,256,256]{2,1,0:T(8,128)(2,1)S(1)}, bf16[2,256,256]{2,1,0:T(8,128)(2,1)S(1)}, u32[]{:S(2)}, u32[]{:S(2)}) %collective-permute-start.34) | collective-permute-done | bytes 262176 | tf_op jit(solution)/shard_map/ppermute | solution.py:392
  105.3 4.9 %collective-permute-done.36.refs_5_ = bf16[2,256,256]{2,1,0:T(8,128)(2,1)S(1)} collective-permute-done((bf16[2,256,256]{2,1,0:T(8,128)(2,1)S(1)}, bf16[2,256,256]{2,1,0:T(8,128)(2,1)S(1)}, u32[]{:S(2)}, u32[]{:S(2)}) %collective-permute-start.36) | collective-permute-done | bytes 262176 | tf_op jit(solution)/shard_map/ppermute | solution.py:392
  112.3 1.8 %collective-permute-start.44 = (bf16[256,256]{1,0:T(8,128)(2,1)S(1)}, bf16[256,256]{1,0:T(8,128)(2,1)S(1)}, u32[]{:S(2)}, u32[]{:S(2)}) collective-permute-start(bf16[256,256]{1,0:T(8,128)(2,1)S(1)} %slice_bitcast_fusion), channel_id=1, source_target_pairs={{8,0},{16,8},{24,16},{28,24},{20,28},{12,20},{4,12},{0,4},{9,1},{1... | collective-permute-start | bytes 393224 | tf_op jit(solution)/shard_map/ppermute | solution.py:393
  116.4 2.6 %shard_map.99 = (bf16[384,256]{1,0:T(8,128)(2,1)S(1)}, f32[2,384]{1,0:T(2,128)S(1)}) custom-call(s32[13]{0:T(128)S(1)} %get-tuple-element.21.flags_ref, bf16[416,2048]{1,0:T(8,128)(2,1)S(1)} %get-tuple-element.27.normed_ref, f32[416,128]{1,0:T(8,128)S(1)} %get-tuple-element.23.dist_ref, f32[31,2,256]{2,1,0:T(2,128)S(1)} %bitcast.14, ...), custom_call_target="tpu_custom_call" | custom-call | tf_op jit(solution)/shard_map/pallas_call | solution.py:497
  119.0 1.7 %collective-permute-start.43 = (bf16[384,256]{1,0:T(8,128)(2,1)S(1)}, bf16[384,256]{1,0:T(8,128)(2,1)S(1)}, u32[]{:S(2)}, u32[]{:S(2)}) collective-permute-start(bf16[384,256]{1,0:T(8,128)(2,1)S(1)} %get-tuple-element.30.refs_8_), channel_id=1, source_target_pairs={{0,2},{1,3},{2,0},{3,1},{4,6},{5,7},{6,4},{7,5},{8,10},{9,11},{10,... | collective-permute-start | bytes 589832 | tf_op jit(solution)/shard_map/ppermute | solution.py:434
  123.0 3.3 %collective-permute-done.41.refs_6_ = f32[2,384]{1,0:T(2,128)S(1)} collective-permute-done((f32[2,384]{1,0:T(2,128)S(1)}, f32[2,384]{1,0:T(2,128)S(1)}, u32[]{:S(2)}, u32[]{:S(2)}) %collective-permute-start.41) | collective-permute-done | bytes 3104 | tf_op jit(solution)/shard_map/ppermute | solution.py:513
  126.2 1.6 %shard_map.100 = (bf16[384,1024]{1,0:T(8,128)(2,1)S(1)}, bf16[2,384,256]{2,1,0:T(8,128)(2,1)S(1)}) custom-call(f32[2,256]{1,0:T(2,128)S(1)} %copy-done.4, f32[2,256]{1,0:T(2,128)S(1)} %collective-permute-done.2.refs_1_, f32[2,256]{1,0:T(2,128)S(1)} %copy-done.5, f32[2,256]{1,0:T(2,128)S(1)} %collective-permute-done.3.refs_3_, ...), custom_call_target="tpu_custom_call" | custom-call | tf_op jit(solution)/shard_map/pallas_call | solution.py:528
  (101 shorter events, 35.4 us)
Async XLA Ops:
  2.4 10.2 %collective-permute-start.4 = (bf16[2,256,256]{2,1,0:T(8,128)(2,1)S(1)}, bf16[2,256,256]{2,1,0:T(8,128)(2,1)S(1)}, u32[]{:S(2)}, u32[]{:S(2)}) collective-permute-start(bf16[2,256,256]{2,1,0:T(8,128)(2,1)S(1)} %shard_map.93.refs_0_), channel_id=1, source_target_pairs={{0,8},{8,16},{16,24},{24,28},{28,20},{20,12},{12,4},{4,0},{1,9},{9... | collective-permute-start | bytes 786440 | tf_op jit(solution)/shard_map/ppermute | solution.py:392
  5.5 21.9 %collective-permute-start.5 = (bf16[2,256,256]{2,1,0:T(8,128)(2,1)S(1)}, bf16[2,256,256]{2,1,0:T(8,128)(2,1)S(1)}, u32[]{:S(2)}, u32[]{:S(2)}) collective-permute-start(bf16[2,256,256]{2,1,0:T(8,128)(2,1)S(1)} %shard_map.93.refs_0_), channel_id=1, source_target_pairs={{8,0},{16,8},{24,16},{28,24},{20,28},{12,20},{4,12},{0,4},{9,1},{1... | collective-permute-start | bytes 786440 | tf_op jit(solution)/shard_map/ppermute | solution.py:393
  5.5 25.0 %collective-permute-start.17 = (bf16[2,256,256]{2,1,0:T(8,128)(2,1)S(1)}, bf16[2,256,256]{2,1,0:T(8,128)(2,1)S(1)}, u32[]{:S(2)}, u32[]{:S(2)}) collective-permute-start(bf16[2,256,256]{2,1,0:T(8,128)(2,1)S(1)} %copy-done.1), channel_id=1, source_target_pairs={{0,8},{8,16},{16,24},{24,28},{28,20},{20,12},{12,4},{4,0},{1,9},{9... | collective-permute-start | bytes 786440 | tf_op jit(solution)/shard_map/ppermute | solution.py:392
  12.6 18.4 %collective-permute-start.6 = (bf16[2,256,256]{2,1,0:T(8,128)(2,1)S(1)}, bf16[2,256,256]{2,1,0:T(8,128)(2,1)S(1)}, u32[]{:S(2)}, u32[]{:S(2)}) collective-permute-start(bf16[2,256,256]{2,1,0:T(8,128)(2,1)S(1)} %collective-permute-done.4.refs_1_), channel_id=1, source_target_pairs={{0,8},{8,16},{16,24},{24,28},{28,20},{20,12},{12,4},{4,0},{1,9},{9... | collective-permute-start | bytes 786440 | tf_op jit(solution)/shard_map/ppermute | solution.py:392
  15.2 13.8 %collective-permute-start = (bf16[32,2176]{1,0:T(8,128)(2,1)S(1)}, bf16[32,2176]{1,0:T(8,128)(2,1)S(1)}, u32[]{:S(2)}, u32[]{:S(2)}) collective-permute-start(bf16[32,2176]{1,0:T(8,128)(2,1)S(1)} %get-tuple-element.19), channel_id=1, source_target_pairs={{0,4},{4,8},{8,12},{12,16},{16,20},{20,24},{24,28},{1,5},{5,9},{9,... | collective-permute-start | bytes 417800 | tf_op jit(solution)/shard_map/ppermute | solution.py:463
  24.3 9.8 %collective-permute-start.19 = (bf16[2,256,256]{2,1,0:T(8,128)(2,1)S(1)}, bf16[2,256,256]{2,1,0:T(8,128)(2,1)S(1)}, u32[]{:S(2)}, u32[]{:S(2)}) collective-permute-start(bf16[2,256,256]{2,1,0:T(8,128)(2,1)S(1)} %copy-done.1), channel_id=1, source_target_pairs={{8,0},{16,8},{24,16},{28,24},{20,28},{12,20},{4,12},{0,4},{9,1},{1... | collective-permute-start | bytes 786440 | tf_op jit(solution)/shard_map/ppermute | solution.py:393
  27.4 12.3 %collective-permute-start.7 = (bf16[2,256,256]{2,1,0:T(8,128)(2,1)S(1)}, bf16[2,256,256]{2,1,0:T(8,128)(2,1)S(1)}, u32[]{:S(2)}, u32[]{:S(2)}) collective-permute-start(bf16[2,256,256]{2,1,0:T(8,128)(2,1)S(1)} %collective-permute-done.5.refs_2_), channel_id=1, source_target_pairs={{8,0},{16,8},{24,16},{28,24},{20,28},{12,20},{4,12},{0,4},{9,1},{1... | collective-permute-start | bytes 786440 | tf_op jit(solution)/shard_map/ppermute | solution.py:393
  29.0 13.2 %collective-permute-start.16 = (bf16[2,256,256]{2,1,0:T(8,128)(2,1)S(1)}, bf16[2,256,256]{2,1,0:T(8,128)(2,1)S(1)}, u32[]{:S(2)}, u32[]{:S(2)}) collective-permute-start(bf16[2,256,256]{2,1,0:T(8,128)(2,1)S(1)} %copy-done.1), channel_id=1, source_target_pairs={{0,2},{1,3},{2,0},{3,1},{4,6},{5,7},{6,4},{7,5},{8,10},{9,11},{10,... | collective-permute-start | bytes 786440 | tf_op jit(solution)/shard_map/ppermute | solution.py:434
  30.6 13.2 %collective-permute-start.21 = (bf16[2,256,256]{2,1,0:T(8,128)(2,1)S(1)}, bf16[2,256,256]{2,1,0:T(8,128)(2,1)S(1)}, u32[]{:S(2)}, u32[]{:S(2)}) collective-permute-start(bf16[2,256,256]{2,1,0:T(8,128)(2,1)S(1)} %collective-permute-done.17.refs_12_), channel_id=1, source_target_pairs={{0,8},{8,16},{16,24},{24,28},{28,20},{20,12},{12,4},{4,0},{1,9},{9... | collective-permute-start | bytes 786440 | tf_op jit(solution)/shard_map/ppermute | solution.py:392
  31.0 13.3 %collective-permute-start.8 = (bf16[2,256,256]{2,1,0:T(8,128)(2,1)S(1)}, bf16[2,256,256]{2,1,0:T(8,128)(2,1)S(1)}, u32[]{:S(2)}, u32[]{:S(2)}) collective-permute-start(bf16[2,256,256]{2,1,0:T(8,128)(2,1)S(1)} %collective-permute-done.6.refs_3_), channel_id=1, source_target_pairs={{0,8},{8,16},{16,24},{24,28},{28,20},{20,12},{12,4},{4,0},{1,9},{9... | collective-permute-start | bytes 786440 | tf_op jit(solution)/shard_map/ppermute | solution.py:392
  34.1 10.2 %collective-permute-start.23 = (bf16[2,256,256]{2,1,0:T(8,128)(2,1)S(1)}, bf16[2,256,256]{2,1,0:T(8,128)(2,1)S(1)}, u32[]{:S(2)}, u32[]{:S(2)}) collective-permute-start(bf16[2,256,256]{2,1,0:T(8,128)(2,1)S(1)} %collective-permute-done.19.refs_14_), channel_id=1, source_target_pairs={{8,0},{16,8},{24,16},{28,24},{20,28},{12,20},{4,12},{0,4},{9,1},{1... | collective-permute-start | bytes 786440 | tf_op jit(solution)/shard_map/ppermute | solution.py:393
  42.2 8.0 %collective-permute-start.18 = (bf16[2,256,256]{2,1,0:T(8,128)(2,1)S(1)}, bf16[2,256,256]{2,1,0:T(8,128)(2,1)S(1)}, u32[]{:S(2)}, u32[]{:S(2)}) collective-permute-start(bf16[2,256,256]{2,1,0:T(8,128)(2,1)S(1)} %collective-permute-done.17.refs_12_), channel_id=1, source_target_pairs={{0,2},{1,3},{2,0},{3,1},{4,6},{5,7},{6,4},{7,5},{8,10},{9,11},{10,... | collective-permute-start | bytes 786440 | tf_op jit(solution)/shard_map/ppermute | solution.py:434
  43.8 9.8 %collective-permute-start.20 = (bf16[2,256,256]{2,1,0:T(8,128)(2,1)S(1)}, bf16[2,256,256]{2,1,0:T(8,128)(2,1)S(1)}, u32[]{:S(2)}, u32[]{:S(2)}) collective-permute-start(bf16[2,256,256]{2,1,0:T(8,128)(2,1)S(1)} %collective-permute-done.19.refs_14_), channel_id=1, source_target_pairs={{0,2},{1,3},{2,0},{3,1},{4,6},{5,7},{6,4},{7,5},{8,10},{9,11},{10,... | collective-permute-start | bytes 786440 | tf_op jit(solution)/shard_map/ppermute | solution.py:434
  44.3 9.3 %collective-permute-start.25 = (bf16[2,256,256]{2,1,0:T(8,128)(2,1)S(1)}, bf16[2,256,256]{2,1,0:T(8,128)(2,1)S(1)}, u32[]{:S(2)}, u32[]{:S(2)}) collective-permute-start(bf16[2,256,256]{2,1,0:T(8,128)(2,1)S(1)} %collective-permute-done.21.refs_16_), channel_id=1, source_target_pairs={{0,8},{8,16},{16,24},{24,28},{28,20},{20,12},{12,4},{4,0},{1,9},{9... | collective-permute-start | bytes 786440 | tf_op jit(solution)/shard_map/ppermute | solution.py:392
  46.1 9.5 %collective-permute-start.27 = (bf16[2,256,256]{2,1,0:T(8,128)(2,1)S(1)}, bf16[2,256,256]{2,1,0:T(8,128)(2,1)S(1)}, u32[]{:S(2)}, u32[]{:S(2)}) collective-permute-start(bf16[2,256,256]{2,1,0:T(8,128)(2,1)S(1)} %collective-permute-done.23.refs_18_.refs_1_), channel_id=1, source_target_pairs={{8,0},{16,8},{24,16},{28,24},{20,28},{12,20},{4,12},{0,4},{9,1},{1... | collective-permute-start | bytes 786440 | tf_op jit(solution)/shard_map/ppermute | solution.py:393
  48.6 17.5 %collective-permute-start.22 = (bf16[2,256,256]{2,1,0:T(8,128)(2,1)S(1)}, bf16[2,256,256]{2,1,0:T(8,128)(2,1)S(1)}, u32[]{:S(2)}, u32[]{:S(2)}) collective-permute-start(bf16[2,256,256]{2,1,0:T(8,128)(2,1)S(1)} %collective-permute-done.21.refs_16_), channel_id=1, source_target_pairs={{0,2},{1,3},{2,0},{3,1},{4,6},{5,7},{6,4},{7,5},{8,10},{9,11},{10,... | collective-permute-start | bytes 786440 | tf_op jit(solution)/shard_map/ppermute | solution.py:434
  50.2 18.0 %collective-permute-start.24 = (bf16[2,256,256]{2,1,0:T(8,128)(2,1)S(1)}, bf16[2,256,256]{2,1,0:T(8,128)(2,1)S(1)}, u32[]{:S(2)}, u32[]{:S(2)}) collective-permute-start(bf16[2,256,256]{2,1,0:T(8,128)(2,1)S(1)} %collective-permute-done.23.refs_18_.refs_1_), channel_id=1, source_target_pairs={{0,2},{1,3},{2,0},{3,1},{4,6},{5,7},{6,4},{7,5},{8,10},{9,11},{10,... | collective-permute-start | bytes 786440 | tf_op jit(solution)/shard_map/ppermute | solution.py:434
  55.6 12.1 %collective-permute-start.29 = (bf16[256,256]{1,0:T(8,128)(2,1)S(1)}, bf16[256,256]{1,0:T(8,128)(2,1)S(1)}, u32[]{:S(2)}, u32[]{:S(2)}) collective-permute-start(bf16[256,256]{1,0:T(8,128)(2,1)S(1)} %slice_bitcast_fusion.3), channel_id=1, source_target_pairs={{0,8},{8,16},{16,24},{24,28},{28,20},{20,12},{12,4},{4,0},{1,9},{9... | collective-permute-start | bytes 393224 | tf_op jit(solution)/shard_map/ppermute | solution.py:392
  58.5 25.9 %collective-permute-start.26 = (bf16[2,256,256]{2,1,0:T(8,128)(2,1)S(1)}, bf16[2,256,256]{2,1,0:T(8,128)(2,1)S(1)}, u32[]{:S(2)}, u32[]{:S(2)}) collective-permute-start(bf16[2,256,256]{2,1,0:T(8,128)(2,1)S(1)} %collective-permute-done.25.refs_20_.refs_3_), channel_id=1, source_target_pairs={{0,2},{1,3},{2,0},{3,1},{4,6},{5,7},{6,4},{7,5},{8,10},{9,11},{10,... | collective-permute-start | bytes 786440 | tf_op jit(solution)/shard_map/ppermute | solution.py:434
  60.0 24.4 %collective-permute-start.28 = (bf16[2,256,256]{2,1,0:T(8,128)(2,1)S(1)}, bf16[2,256,256]{2,1,0:T(8,128)(2,1)S(1)}, u32[]{:S(2)}, u32[]{:S(2)}) collective-permute-start(bf16[2,256,256]{2,1,0:T(8,128)(2,1)S(1)} %collective-permute-done.27.refs_22_.refs_5_), channel_id=1, source_target_pairs={{0,2},{1,3},{2,0},{3,1},{4,6},{5,7},{6,4},{7,5},{8,10},{9,11},{10,... | collective-permute-start | bytes 786440 | tf_op jit(solution)/shard_map/ppermute | solution.py:434
  66.1 18.3 %collective-permute-start.15 = (bf16[416,256]{1,0:T(8,128)(2,1)S(1)}, bf16[416,256]{1,0:T(8,128)(2,1)S(1)}, u32[]{:S(2)}, u32[]{:S(2)}) collective-permute-start(bf16[416,256]{1,0:T(8,128)(2,1)S(1)} %get-tuple-element.25.refs_8_), channel_id=1, source_target_pairs={{0,2},{1,3},{2,0},{3,1},{4,6},{5,7},{6,4},{7,5},{8,10},{9,11},{10,... | collective-permute-start | bytes 638984 | tf_op jit(solution)/shard_map/ppermute | solution.py:434
  67.7 16.7 %collective-permute-start.30 = (bf16[256,256]{1,0:T(8,128)(2,1)S(1)}, bf16[256,256]{1,0:T(8,128)(2,1)S(1)}, u32[]{:S(2)}, u32[]{:S(2)}) collective-permute-start(bf16[256,256]{1,0:T(8,128)(2,1)S(1)} %collective-permute-done.29.refs_24_), channel_id=1, source_target_pairs={{0,2},{1,3},{2,0},{3,1},{4,6},{5,7},{6,4},{7,5},{8,10},{9,11},{10,... | collective-permute-start | bytes 393224 | tf_op jit(solution)/shard_map/ppermute | solution.py:434
  69.4 12.0 %collective-permute-start.13 = (f32[2,512]{1,0:T(2,128)S(1)}, f32[2,512]{1,0:T(2,128)S(1)}, u32[]{:S(2)}, u32[]{:S(2)}) collective-permute-start(f32[2,512]{1,0:T(2,128)S(1)} %get-tuple-element.24.refs_4_), channel_id=1, source_target_pairs={{0,2},{1,3},{2,0},{3,1},{4,6},{5,7},{6,4},{7,5},{8,10},{9,11},{10,... | collective-permute-start | bytes 12296 | tf_op jit(solution)/shard_map/ppermute | solution.py:513
  86.7 27.4 %collective-permute-start.31 = (bf16[416,2048]{1,0:T(8,128)(2,1)S(1)}, bf16[416,2048]{1,0:T(8,128)(2,1)S(1)}, u32[]{:S(2)}, u32[]{:S(2)}) collective-permute-start(bf16[416,2048]{1,0:T(8,128)(2,1)S(1)} %shard_map.96.refs_3_), channel_id=1, source_target_pairs={{0,1},{1,0},{2,3},{3,2},{4,5},{5,4},{6,7},{7,6},{8,9},{9,8},{10,11... | collective-permute-start | bytes 5111816 | tf_op jit(solution)/shard_map/ppermute | solution.py:545
  86.9 8.6 %collective-permute-start.32 = (bf16[2,256,256]{2,1,0:T(8,128)(2,1)S(1)}, bf16[2,256,256]{2,1,0:T(8,128)(2,1)S(1)}, u32[]{:S(2)}, u32[]{:S(2)}) collective-permute-start(bf16[2,256,256]{2,1,0:T(8,128)(2,1)S(1)} %get-tuple-element.28.refs_0_), channel_id=1, source_target_pairs={{0,8},{8,16},{16,24},{24,28},{28,20},{20,12},{12,4},{4,0},{1,9},{9... | collective-permute-start | bytes 786440 | tf_op jit(solution)/shard_map/ppermute | solution.py:392
  86.9 8.9 %collective-permute-start.33 = (bf16[2,256,256]{2,1,0:T(8,128)(2,1)S(1)}, bf16[2,256,256]{2,1,0:T(8,128)(2,1)S(1)}, u32[]{:S(2)}, u32[]{:S(2)}) collective-permute-start(bf16[2,256,256]{2,1,0:T(8,128)(2,1)S(1)} %get-tuple-element.28.refs_0_), channel_id=1, source_target_pairs={{8,0},{16,8},{24,16},{28,24},{20,28},{12,20},{4,12},{0,4},{9,1},{1... | collective-permute-start | bytes 786440 | tf_op jit(solution)/shard_map/ppermute | solution.py:393
  95.5 7.8 %collective-permute-start.34 = (bf16[2,256,256]{2,1,0:T(8,128)(2,1)S(1)}, bf16[2,256,256]{2,1,0:T(8,128)(2,1)S(1)}, u32[]{:S(2)}, u32[]{:S(2)}) collective-permute-start(bf16[2,256,256]{2,1,0:T(8,128)(2,1)S(1)} %collective-permute-done.32.refs_1_), channel_id=1, source_target_pairs={{0,8},{8,16},{16,24},{24,28},{28,20},{20,12},{12,4},{4,0},{1,9},{9... | collective-permute-start | bytes 786440 | tf_op jit(solution)/shard_map/ppermute | solution.py:392
  95.8 8.0 %collective-permute-start.35 = (bf16[2,256,256]{2,1,0:T(8,128)(2,1)S(1)}, bf16[2,256,256]{2,1,0:T(8,128)(2,1)S(1)}, u32[]{:S(2)}, u32[]{:S(2)}) collective-permute-start(bf16[2,256,256]{2,1,0:T(8,128)(2,1)S(1)} %collective-permute-done.33.refs_2_), channel_id=1, source_target_pairs={{8,0},{16,8},{24,16},{28,24},{20,28},{12,20},{4,12},{0,4},{9,1},{1... | collective-permute-start | bytes 786440 | tf_op jit(solution)/shard_map/ppermute | solution.py:393
  103.8 7.2 %collective-permute-start.37 = (bf16[2,256,256]{2,1,0:T(8,128)(2,1)S(1)}, bf16[2,256,256]{2,1,0:T(8,128)(2,1)S(1)}, u32[]{:S(2)}, u32[]{:S(2)}) collective-permute-start(bf16[2,256,256]{2,1,0:T(8,128)(2,1)S(1)} %collective-permute-done.35.refs_4_), channel_id=1, source_target_pairs={{8,0},{16,8},{24,16},{28,24},{20,28},{12,20},{4,12},{0,4},{9,1},{1... | collective-permute-start | bytes 786440 | tf_op jit(solution)/shard_map/ppermute | solution.py:393
  112.3 8.4 %collective-permute-start.44 = (bf16[256,256]{1,0:T(8,128)(2,1)S(1)}, bf16[256,256]{1,0:T(8,128)(2,1)S(1)}, u32[]{:S(2)}, u32[]{:S(2)}) collective-permute-start(bf16[256,256]{1,0:T(8,128)(2,1)S(1)} %slice_bitcast_fusion), channel_id=1, source_target_pairs={{8,0},{16,8},{24,16},{28,24},{20,28},{12,20},{4,12},{0,4},{9,1},{1... | collective-permute-start | bytes 393224 | tf_op jit(solution)/shard_map/ppermute | solution.py:393
  119.0 7.2 %collective-permute-start.43 = (bf16[384,256]{1,0:T(8,128)(2,1)S(1)}, bf16[384,256]{1,0:T(8,128)(2,1)S(1)}, u32[]{:S(2)}, u32[]{:S(2)}) collective-permute-start(bf16[384,256]{1,0:T(8,128)(2,1)S(1)} %get-tuple-element.30.refs_8_), channel_id=1, source_target_pairs={{0,2},{1,3},{2,0},{3,1},{4,6},{5,7},{6,4},{7,5},{8,10},{9,11},{10,... | collective-permute-start | bytes 589832 | tf_op jit(solution)/shard_map/ppermute | solution.py:434
  120.7 7.4 %collective-permute-start.45 = (bf16[256,256]{1,0:T(8,128)(2,1)S(1)}, bf16[256,256]{1,0:T(8,128)(2,1)S(1)}, u32[]{:S(2)}, u32[]{:S(2)}) collective-permute-start(bf16[256,256]{1,0:T(8,128)(2,1)S(1)} %collective-permute-done.44.refs_7_), channel_id=1, source_target_pairs={{0,2},{1,3},{2,0},{3,1},{4,6},{5,7},{6,4},{7,5},{8,10},{9,11},{10,... | collective-permute-start | bytes 393224 | tf_op jit(solution)/shard_map/ppermute | solution.py:434
  (25 other events, 196.7 us)

commit v4 on v3

--- a/solution.py
+++ b/solution.py
@@ -12,9 +12,9 @@
 LANES = 128
 SUBLANES = 8
 HALO_ALIGN = 16
-CONV_ROWS = 32
+CONV_MOST = 64
 RING_MOST = 8
-KERNEL_VMEM = 20 * 2**20
+KERNEL_VMEM = 12 * 2**20
 PACK_FLOPS = 2 * 10**9
 PACK_BYTES = 8 * 10**6
 PRODUCTS_AHEAD = (5, 7)
@@ -117,7 +117,7 @@
     )(value_proj, gate_proj, *extra)
 
 
-def norm_body(tail, near, tap_count, tokens_ref, docs_ref, gain_ref, *refs):
+def norm_body(tail, near, tap_count, blocks, tokens_ref, docs_ref, gain_ref, *refs):
     prev_refs, refs = refs[:near], refs[near:]
     normed_ref, dist_ref, state_ref, flags_ref, run_ref = refs
     row_count, model_width = tokens_ref.shape
@@ -149,9 +149,8 @@
         run = jnp.where(run == reach, reach + run_ref[lead - reach : lead - reach + rows, :], run)
         reach = 2 * reach
     dist_ref[...] = run[tail:, :]
-    for k in range(flags_ref.shape[0]):
-        least = jnp.min(run[tail + k * CONV_ROWS : tail + (k + 1) * CONV_ROWS, :])
-        flags_ref[k] = (least >= tap_count - 1).astype(jnp.int32)
+    for k, (first, size) in enumerate(blocks):
+        flags_ref[k] = (jnp.min(run[first : first + size, :]) >= tap_count - 1).astype(jnp.int32)
 
 
 def chunk_start(places, k, size):
@@ -180,8 +179,12 @@
     add_products(acc_ref, None, normed_ref, pairs, places, 0)
 
 
+def conv_block(rows):
+    return max(size for size in range(SUBLANES, CONV_MOST + 1, SUBLANES) if rows % size == 0)
+
+
 def gated_conv_body(
-    layer, tap_count, tail, places, done, halved, flags_ref, normed_ref, dist_ref, taps_ref, *refs
+    layer, tap_count, tail, places, done, halved, flags_from, flags_ref, normed_ref, dist_ref, taps_ref, *refs
 ):
     start_ref, refs = (refs[0], refs[1:]) if done else (None, refs)
     *pair_refs, centred_ref, stats_ref, acc_ref, shifted_ref, conv_ref = refs
@@ -206,24 +209,30 @@
                 half, 0, SUBLANES - shift : rows - shift, :
             ]
 
+    size = conv_block(out_rows)
+
     def block(index, carry):
-        base = pl.multiple_of(index * CONV_ROWS, CONV_ROWS)
-        whole = flags_ref[index + dist_from // CONV_ROWS]
+        base = pl.multiple_of(index * size, SUBLANES)
+        whole = flags_ref[flags_from + index]
 
         def convolved(masked):
-            sums = [jnp.zeros((CONV_ROWS, LANES), wide) for _ in range(halves)]
             if masked:
-                dist = dist_ref[pl.ds(pl.multiple_of(base + dist_from, CONV_ROWS), CONV_ROWS), :]
-            for tap in range(tap_count):
-                start = pl.multiple_of(base + (tail - tap // SUBLANES * SUBLANES), SUBLANES)
-                for half in range(halves):
-                    term = (
-                        taps_ref[tap, layer : layer + 1, half * LANES : (half + 1) * LANES]
-                        * shifted_ref[half, tap % SUBLANES, pl.ds(start, CONV_ROWS), :]
-                    )
-                    sums[half] = sums[half] + (jnp.where(dist >= tap, term, 0.0) if masked else term)
+                dist = dist_ref[pl.ds(pl.multiple_of(base + dist_from, SUBLANES), size), :]
             for half in range(halves):
-                conv_ref[half, pl.ds(base, CONV_ROWS), :] = sums[half]
+                cols = slice(half * LANES, (half + 1) * LANES)
+                total = jnp.zeros((size, LANES), wide)
+                for shift in range(min(SUBLANES, tap_count)):
+                    most = (tap_count - 1 - shift) // SUBLANES * SUBLANES
+                    start = pl.multiple_of(base + (tail - most), SUBLANES)
+                    window = shifted_ref[half, shift, pl.ds(start, size + most), :]
+                    for back in range(0, most + 1, SUBLANES):
+                        tap = back + shift
+                        term = (
+                            taps_ref[tap, layer : layer + 1, cols]
+                            * window[most - back : most - back + size, :]
+                        )
+                        total = total + (jnp.where(dist >= tap, term, 0.0) if masked else term)
+                conv_ref[half, pl.ds(base, size), :] = total
 
         @pl.when(whole == 1)
         def _():
@@ -235,7 +244,7 @@
 
         return carry
 
-    lax.fori_loop(0, out_rows // CONV_ROWS, block, 0)
+    lax.fori_loop(0, out_rows // size, block, 0)
     total = conv_ref[0]
     for half in range(1, halves):
         total = total + conv_ref[half]
@@ -262,18 +271,22 @@
     far = len(centred_refs)
     out_rows, width = centred_refs[0].shape
     count = far * near
-    fill = jnp.zeros((round_up(2 * count, SUBLANES) - 2 * count, stats_refs[0].shape[1]), wide)
-    stats = jnp.concatenate([ref[...] for ref in stats_refs] + ([fill] if fill.size else []))
-    stats = stats.T[:out_rows, :]
-    means = [stats[:, 2 * j : 2 * j + 1] for j in range(count)]
-    squares = [stats[:, 2 * j + 1 : 2 * j + 2] for j in range(count)]
+    means = [ref[0:1, :] for ref in stats_refs]
     mean = summed([summed(means[f * near : (f + 1) * near]) for f in range(far)]) / count
-    squares = [square + width * (own - mean) ** 2 for square, own in zip(squares, means)]
+    squares = [
+        ref[1:2, :] + width * (own - mean) ** 2 for ref, own in zip(stats_refs, means)
+    ]
     square = summed([summed(squares[f * near : (f + 1) * near]) for f in range(far)])
-    scale = lax.rsqrt(square / (width * count) + epsilon)
+    lines = [lax.rsqrt(square / (width * count) + epsilon)]
+    lines.extend(means[f * near] - mean for f in range(far))
+    fill = round_up(len(lines), SUBLANES) - len(lines)
+    lines.extend([jnp.zeros_like(mean)] * fill)
+    columns = jnp.concatenate(lines).T[:out_rows, :]
+    scale = columns[:, 0:1]
     for f, centred in enumerate(centred_refs):
         gain, shift = gain_refs[f][layer : layer + 1, :], shift_refs[f][layer : layer + 1, :]
-        normal = gain * (centred[...].astype(wide) + (means[f * near] - mean)) * scale + shift
+        offset = columns[:, 1 + f : 2 + f]
+        normal = gain * (centred[...].astype(wide) + offset) * scale + shift
         act_ref[f] = (normal * jax.nn.sigmoid(normal)).astype(narrow)
 
 
@@ -424,7 +437,7 @@
     near, far = tp_groups(tp_count)
     far_pairs = group_pairs(tp_count, near, far, 0, 1)
     near_pairs = group_pairs(tp_count, near, far, 1, 0)
-    tail = round_up(tap_count - 1, max(HALO_ALIGN, CONV_ROWS))
+    tail = round_up(tap_count - 1, max(HALO_ALIGN, 2 * HALO_ALIGN))
     halo = tail * layer_count
     in_ring = layer_count == 2 and ringed(sp_count, value_proj.shape[1], out_proj.shape[2])
 
@@ -467,13 +480,19 @@
     places = (sp_count, ring_tables(sp_count)[2]) if in_ring else None
 
     taps = jnp.transpose(conv_taps, (1, 0, 2))
+    blocks, flags_from = [], []
+    for n in range(layer_count):
+        flags_from.append(len(blocks))
+        first = tail * (n + 1)
+        size = conv_block(halo + row_count - first)
+        blocks.extend((at, size) for at in range(first, halo + row_count, size))
     normed, dist, prev_state, flags = kernel(
-        functools.partial(norm_body, tail, near, tap_count),
+        functools.partial(norm_body, tail, near, tap_count, blocks),
         (
             jax.ShapeDtypeStruct((halo + row_count, model_width), narrow),
             jax.ShapeDtypeStruct((halo + row_count - tail, LANES), wide),
             jax.ShapeDtypeStruct((halo, model_width), narrow),
-            jax.ShapeDtypeStruct(((halo + row_count - tail) // CONV_ROWS,), jnp.int32),
+            jax.ShapeDtypeStruct((len(blocks),), jnp.int32),
         ),
         [in_vmem()] * (3 + near),
         [pltpu.VMEM((tail + halo + row_count, LANES), wide)],
@@ -495,7 +514,9 @@
                 )(normed, *pairs[:done]),
             )
         centred, stats = kernel(
-            functools.partial(gated_conv_body, n, tap_count, tail, places, done, in_ring),
+            functools.partial(
+                gated_conv_body, n, tap_count, tail, places, done, in_ring, flags_from[n]
+            ),
             (
                 jax.ShapeDtypeStruct((out_rows, width), narrow),
                 jax.ShapeDtypeStruct((2, round_up(out_rows, LANES)), wide),

time: 133 us -> 131 us (0.985)
  Pallas kernels: 17.9 us -> 16.2 us
    pallas_call x3, Pallas kernels: 4.48 us -> 2.98 us  [on_device(): kernel(functools.partial(project_body, n, near, far, out_slots[n][own], p...]
  transfers between devices with their start and end apart: 48 -> 48, of which waited for: 16 -> 16; matrix products, arithmetic and copies ran while one was open for 0% -> 0% of each run, Pallas kernels for 11% -> 10%
where the time goes in v4:
time: 131 us
  waiting for transfers between devices  58.1 us (44%)
  starting transfers between devices  54 us (41%)
  Pallas kernels  16.2 us (12%)
  local copies, waits for them, and re-layouts  2.18 us (2%)
    ppermute x12, waiting for transfers between devices, ring_gathered(): ahead = lax.ppermute(ahead, 'sp', forward)  25.1 us
    ppermute x12, starting transfers between devices, ring_gathered(): behind = lax.ppermute(behind, 'sp', backward)  22.4 us
    ppermute x6, waiting for transfers between devices, on_device(): all_stats.append(lax.ppermute(stats, 'tp', steps))  18 us
    ppermute x13, starting transfers between devices, far_values(): values.append(lax.ppermute(values[-1], 'tp', far_pairs))  15.9 us
    ppermute x12, starting transfers between devices, ring_gathered(): ahead = lax.ppermute(ahead, 'sp', forward)  9.53 us
    ppermute x12, waiting for transfers between devices, ring_gathered(): behind = lax.ppermute(behind, 'sp', backward)  7.99 us
    ppermute x13, waiting for transfers between devices, far_values(): values.append(lax.ppermute(values[-1], 'tp', far_pairs))  5.96 us
    pallas_call x2, Pallas kernels, on_device(): kernel(functools.partial(gated_conv_body, n, tap_count, tail, places, don...  5.36 us
  transfers between devices with their start and end apart: 48, of which 16 were waited for; matrix products, arithmetic and copies ran while one was open for 0% of the time, Pallas kernels for 10%

profile of v4, /device:TPU:0, one launch (start us, length us, event | category | flops | bytes accessed | tf_op | source)
XLA Modules:
  0.0 130.9 jit_solution(10193882675255655701)
XLA Ops:
  2.4 3.1 %collective-permute-start.4 = (bf16[2,256,256]{2,1,0:T(8,128)(2,1)S(1)}, bf16[2,256,256]{2,1,0:T(8,128)(2,1)S(1)}, u32[]{:S(2)}, u32[]{:S(2)}) collective-permute-start(bf16[2,256,256]{2,1,0:T(8,128)(2,1)S(1)} %shard_map.93.refs_0_), channel_id=1, source_target_pairs={{0,8},{8,16},{16,24},{24,28},{28,20},{20,12},{12,4},{4,0},{1,9},{9... | collective-permute-start | bytes 786440 | tf_op jit(solution)/shard_map/ppermute | solution.py:405
  5.5 2.0 %collective-permute-start.17 = (bf16[2,256,256]{2,1,0:T(8,128)(2,1)S(1)}, bf16[2,256,256]{2,1,0:T(8,128)(2,1)S(1)}, u32[]{:S(2)}, u32[]{:S(2)}) collective-permute-start(bf16[2,256,256]{2,1,0:T(8,128)(2,1)S(1)} %copy-done.1), channel_id=1, source_target_pairs={{0,8},{8,16},{16,24},{24,28},{28,20},{20,12},{12,4},{4,0},{1,9},{9... | collective-permute-start | bytes 786440 | tf_op jit(solution)/shard_map/ppermute | solution.py:405
  7.5 5.0 %collective-permute-done.4.refs_1_ = bf16[2,256,256]{2,1,0:T(8,128)(2,1)S(1)} collective-permute-done((bf16[2,256,256]{2,1,0:T(8,128)(2,1)S(1)}, bf16[2,256,256]{2,1,0:T(8,128)(2,1)S(1)}, u32[]{:S(2)}, u32[]{:S(2)}) %collective-permute-start.4) | collective-permute-done | bytes 262176 | tf_op jit(solution)/shard_map/ppermute | solution.py:405
  12.6 2.1 %collective-permute-start.6 = (bf16[2,256,256]{2,1,0:T(8,128)(2,1)S(1)}, bf16[2,256,256]{2,1,0:T(8,128)(2,1)S(1)}, u32[]{:S(2)}, u32[]{:S(2)}) collective-permute-start(bf16[2,256,256]{2,1,0:T(8,128)(2,1)S(1)} %collective-permute-done.4.refs_1_), channel_id=1, source_target_pairs={{0,8},{8,16},{16,24},{24,28},{28,20},{20,12},{12,4},{4,0},{1,9},{9... | collective-permute-start | bytes 786440 | tf_op jit(solution)/shard_map/ppermute | solution.py:405
  15.2 1.8 %collective-permute-start = (bf16[32,2176]{1,0:T(8,128)(2,1)S(1)}, bf16[32,2176]{1,0:T(8,128)(2,1)S(1)}, u32[]{:S(2)}, u32[]{:S(2)}) collective-permute-start(bf16[32,2176]{1,0:T(8,128)(2,1)S(1)} %get-tuple-element.19), channel_id=1, source_target_pairs={{0,4},{4,8},{8,12},{12,16},{16,20},{20,24},{24,28},{1,5},{5,9},{9,... | collective-permute-start | bytes 417800 | tf_op jit(solution)/shard_map/ppermute | solution.py:476
  17.1 2.1 %collective-permute-start.2 = (f32[2,256]{1,0:T(2,128)S(1)}, f32[2,256]{1,0:T(2,128)S(1)}, u32[]{:S(2)}, u32[]{:S(2)}) collective-permute-start(f32[2,256]{1,0:T(2,128)S(1)} %copy-done.4), channel_id=1, source_target_pairs={{0,2},{1,3},{2,0},{3,1},{4,6},{5,7},{6,4},{7,5},{8,10},{9,11},{10,... | collective-permute-start | bytes 6152 | tf_op jit(solution)/shard_map/ppermute | solution.py:447
  20.8 2.0 %collective-permute-start.3 = (f32[2,256]{1,0:T(2,128)S(1)}, f32[2,256]{1,0:T(2,128)S(1)}, u32[]{:S(2)}, u32[]{:S(2)}) collective-permute-start(f32[2,256]{1,0:T(2,128)S(1)} %copy-done.5), channel_id=1, source_target_pairs={{0,2},{1,3},{2,0},{3,1},{4,6},{5,7},{6,4},{7,5},{8,10},{9,11},{10,... | collective-permute-start | bytes 6152 | tf_op jit(solution)/shard_map/ppermute | solution.py:447
  24.3 3.1 %collective-permute-start.19 = (bf16[2,256,256]{2,1,0:T(8,128)(2,1)S(1)}, bf16[2,256,256]{2,1,0:T(8,128)(2,1)S(1)}, u32[]{:S(2)}, u32[]{:S(2)}) collective-permute-start(bf16[2,256,256]{2,1,0:T(8,128)(2,1)S(1)} %copy-done.1), channel_id=1, source_target_pairs={{8,0},{16,8},{24,16},{28,24},{20,28},{12,20},{4,12},{0,4},{9,1},{1... | collective-permute-start | bytes 786440 | tf_op jit(solution)/shard_map/ppermute | solution.py:406
  27.4 1.6 %collective-permute-start.7 = (bf16[2,256,256]{2,1,0:T(8,128)(2,1)S(1)}, bf16[2,256,256]{2,1,0:T(8,128)(2,1)S(1)}, u32[]{:S(2)}, u32[]{:S(2)}) collective-permute-start(bf16[2,256,256]{2,1,0:T(8,128)(2,1)S(1)} %collective-permute-done.5.refs_2_), channel_id=1, source_target_pairs={{8,0},{16,8},{24,16},{28,24},{20,28},{12,20},{4,12},{0,4},{9,1},{1... | collective-permute-start | bytes 786440 | tf_op jit(solution)/shard_map/ppermute | solution.py:406
  31.0 3.1 %collective-permute-done.19.refs_14_ = bf16[2,256,256]{2,1,0:T(8,128)(2,1)S(1)} collective-permute-done((bf16[2,256,256]{2,1,0:T(8,128)(2,1)S(1)}, bf16[2,256,256]{2,1,0:T(8,128)(2,1)S(1)}, u32[]{:S(2)}, u32[]{:S(2)}) %collective-permute-start.19) | collective-permute-done | bytes 262176 | tf_op jit(solution)/shard_map/ppermute | solution.py:406
  34.1 2.5 %collective-permute-start.23 = (bf16[2,256,256]{2,1,0:T(8,128)(2,1)S(1)}, bf16[2,256,256]{2,1,0:T(8,128)(2,1)S(1)}, u32[]{:S(2)}, u32[]{:S(2)}) collective-permute-start(bf16[2,256,256]{2,1,0:T(8,128)(2,1)S(1)} %collective-permute-done.19.refs_14_), channel_id=1, source_target_pairs={{8,0},{16,8},{24,16},{28,24},{20,28},{12,20},{4,12},{0,4},{9,1},{1... | collective-permute-start | bytes 786440 | tf_op jit(solution)/shard_map/ppermute | solution.py:406
  36.6 3.1 %collective-permute-done.7.refs_4_ = bf16[2,256,256]{2,1,0:T(8,128)(2,1)S(1)} collective-permute-done((bf16[2,256,256]{2,1,0:T(8,128)(2,1)S(1)}, bf16[2,256,256]{2,1,0:T(8,128)(2,1)S(1)}, u32[]{:S(2)}, u32[]{:S(2)}) %collective-permute-start.7) | collective-permute-done | bytes 262176 | tf_op jit(solution)/shard_map/ppermute | solution.py:406
  39.7 2.5 %collective-permute-start.9 = (bf16[2,256,256]{2,1,0:T(8,128)(2,1)S(1)}, bf16[2,256,256]{2,1,0:T(8,128)(2,1)S(1)}, u32[]{:S(2)}, u32[]{:S(2)}) collective-permute-start(bf16[2,256,256]{2,1,0:T(8,128)(2,1)S(1)} %collective-permute-done.7.refs_4_), channel_id=1, source_target_pairs={{8,0},{16,8},{24,16},{28,24},{20,28},{12,20},{4,12},{0,4},{9,1},{1... | collective-permute-start | bytes 786440 | tf_op jit(solution)/shard_map/ppermute | solution.py:406
  44.4 1.7 %collective-permute-done.9.refs_2_ = bf16[2,256,256]{2,1,0:T(8,128)(2,1)S(1)} collective-permute-done((bf16[2,256,256]{2,1,0:T(8,128)(2,1)S(1)}, bf16[2,256,256]{2,1,0:T(8,128)(2,1)S(1)}, u32[]{:S(2)}, u32[]{:S(2)}) %collective-permute-start.9) | collective-permute-done | bytes 262176 | tf_op jit(solution)/shard_map/ppermute | solution.py:406
  46.1 2.5 %collective-permute-start.27 = (bf16[2,256,256]{2,1,0:T(8,128)(2,1)S(1)}, bf16[2,256,256]{2,1,0:T(8,128)(2,1)S(1)}, u32[]{:S(2)}, u32[]{:S(2)}) collective-permute-start(bf16[2,256,256]{2,1,0:T(8,128)(2,1)S(1)} %collective-permute-done.23.refs_18_.refs_1_), channel_id=1, source_target_pairs={{8,0},{16,8},{24,16},{28,24},{20,28},{12,20},{4,12},{0,4},{9,1},{1... | collective-permute-start | bytes 786440 | tf_op jit(solution)/shard_map/ppermute | solution.py:406
  50.7 2.8 %collective-permute-done.20.refs_15_ = bf16[2,256,256]{2,1,0:T(8,128)(2,1)S(1)} collective-permute-done((bf16[2,256,256]{2,1,0:T(8,128)(2,1)S(1)}, bf16[2,256,256]{2,1,0:T(8,128)(2,1)S(1)}, u32[]{:S(2)}, u32[]{:S(2)}) %collective-permute-start.20) | collective-permute-done | bytes 262176 | tf_op jit(solution)/shard_map/ppermute | solution.py:447
  53.5 2.0 %collective-permute-start.11 = (bf16[256,256]{1,0:T(8,128)(2,1)S(1)}, bf16[256,256]{1,0:T(8,128)(2,1)S(1)}, u32[]{:S(2)}, u32[]{:S(2)}) collective-permute-start(bf16[256,256]{1,0:T(8,128)(2,1)S(1)} %slice_bitcast_fusion.4), channel_id=1, source_target_pairs={{8,0},{16,8},{24,16},{28,24},{20,28},{12,20},{4,12},{0,4},{9,1},{1... | collective-permute-start | bytes 393224 | tf_op jit(solution)/shard_map/ppermute | solution.py:406
  55.6 2.8 %collective-permute-done.10.refs_3_ = bf16[256,256]{1,0:T(8,128)(2,1)S(1)} collective-permute-done((bf16[256,256]{1,0:T(8,128)(2,1)S(1)}, bf16[256,256]{1,0:T(8,128)(2,1)S(1)}, u32[]{:S(2)}, u32[]{:S(2)}) %collective-permute-start.10) | collective-permute-done | bytes 131104 | tf_op jit(solution)/shard_map/ppermute | solution.py:405
  60.5 1.7 %shard_map.92 = (bf16[448,2048]{1,0:T(8,128)(2,1)S(1)}, f32[416,128]{1,0:T(8,128)S(1)}, bf16[64,2048]{1,0:T(8,128)(2,1)S(1)}, s32[19]{0:T(128)S(1)}) custom-call(bf16[384,2048]{1,0:T(8,128)(2,1)S(1)} %copy-done, s32[384]{0:T(512)S(1)} %copy-done.6, f32[2,2048]{1,0:T(2,128)S(1)} %copy-done.3, bf16[32,2176]{1,0:T(8,128)(2,1)S(1)} %collective-permute-done.refs_0_, ...), custom_call_target="tpu_custom_call" | custom-call | tf_op jit(solution)/shard_map/pallas_call | solution.py:489
  63.1 3.0 %shard_map.95 = (bf16[416,256]{1,0:T(8,128)(2,1)S(1)}, f32[2,512]{1,0:T(2,128)S(1)}) custom-call(s32[19]{0:T(128)S(1)} %get-tuple-element.21.flags_ref, bf16[448,2048]{1,0:T(8,128)(2,1)S(1)} %get-tuple-element.22.normed_ref, f32[416,128]{1,0:T(8,128)S(1)} %get-tuple-element.23.dist_ref, f32[31,2,256]{2,1,0:T(2,128)S(1)} %bitcast.13, ...), custom_call_target="tpu_custom_call" | custom-call | tf_op jit(solution)/shard_map/pallas_call | solution.py:516
  70.8 10.5 %collective-permute-done.13.refs_6_ = f32[2,512]{1,0:T(2,128)S(1)} collective-permute-done((f32[2,512]{1,0:T(2,128)S(1)}, f32[2,512]{1,0:T(2,128)S(1)}, u32[]{:S(2)}, u32[]{:S(2)}) %collective-permute-start.13) | collective-permute-done | bytes 4128 | tf_op jit(solution)/shard_map/ppermute | solution.py:534
  81.3 3.0 %collective-permute-done.14.refs_7_ = f32[2,512]{1,0:T(2,128)S(1)} collective-permute-done((f32[2,512]{1,0:T(2,128)S(1)}, f32[2,512]{1,0:T(2,128)S(1)}, u32[]{:S(2)}, u32[]{:S(2)}) %collective-permute-start.14) | collective-permute-done | bytes 4128 | tf_op jit(solution)/shard_map/ppermute | solution.py:534
  86.1 2.0 %collective-permute-start.33 = (bf16[2,256,256]{2,1,0:T(8,128)(2,1)S(1)}, bf16[2,256,256]{2,1,0:T(8,128)(2,1)S(1)}, u32[]{:S(2)}, u32[]{:S(2)}) collective-permute-start(bf16[2,256,256]{2,1,0:T(8,128)(2,1)S(1)} %get-tuple-element.28.refs_0_), channel_id=1, source_target_pairs={{8,0},{16,8},{24,16},{28,24},{20,28},{12,20},{4,12},{0,4},{9,1},{1... | collective-permute-start | bytes 786440 | tf_op jit(solution)/shard_map/ppermute | solution.py:406
  88.1 6.6 %collective-permute-done.32.refs_1_ = bf16[2,256,256]{2,1,0:T(8,128)(2,1)S(1)} collective-permute-done((bf16[2,256,256]{2,1,0:T(8,128)(2,1)S(1)}, bf16[2,256,256]{2,1,0:T(8,128)(2,1)S(1)}, u32[]{:S(2)}, u32[]{:S(2)}) %collective-permute-start.32) | collective-permute-done | bytes 262176 | tf_op jit(solution)/shard_map/ppermute | solution.py:405
  95.0 1.7 %collective-permute-start.35 = (bf16[2,256,256]{2,1,0:T(8,128)(2,1)S(1)}, bf16[2,256,256]{2,1,0:T(8,128)(2,1)S(1)}, u32[]{:S(2)}, u32[]{:S(2)}) collective-permute-start(bf16[2,256,256]{2,1,0:T(8,128)(2,1)S(1)} %collective-permute-done.33.refs_2_), channel_id=1, source_target_pairs={{8,0},{16,8},{24,16},{28,24},{20,28},{12,20},{4,12},{0,4},{9,1},{1... | collective-permute-start | bytes 786440 | tf_op jit(solution)/shard_map/ppermute | solution.py:406
  96.7 5.7 %collective-permute-done.34.refs_3_ = bf16[2,256,256]{2,1,0:T(8,128)(2,1)S(1)} collective-permute-done((bf16[2,256,256]{2,1,0:T(8,128)(2,1)S(1)}, bf16[2,256,256]{2,1,0:T(8,128)(2,1)S(1)}, u32[]{:S(2)}, u32[]{:S(2)}) %collective-permute-start.34) | collective-permute-done | bytes 262176 | tf_op jit(solution)/shard_map/ppermute | solution.py:405
  104.5 4.9 %collective-permute-done.36.refs_5_ = bf16[2,256,256]{2,1,0:T(8,128)(2,1)S(1)} collective-permute-done((bf16[2,256,256]{2,1,0:T(8,128)(2,1)S(1)}, bf16[2,256,256]{2,1,0:T(8,128)(2,1)S(1)}, u32[]{:S(2)}, u32[]{:S(2)}) %collective-permute-start.36) | collective-permute-done | bytes 262176 | tf_op jit(solution)/shard_map/ppermute | solution.py:405
  111.5 1.8 %collective-permute-start.44 = (bf16[256,256]{1,0:T(8,128)(2,1)S(1)}, bf16[256,256]{1,0:T(8,128)(2,1)S(1)}, u32[]{:S(2)}, u32[]{:S(2)}) collective-permute-start(bf16[256,256]{1,0:T(8,128)(2,1)S(1)} %slice_bitcast_fusion), channel_id=1, source_target_pairs={{8,0},{16,8},{24,16},{28,24},{20,28},{12,20},{4,12},{0,4},{9,1},{1... | collective-permute-start | bytes 393224 | tf_op jit(solution)/shard_map/ppermute | solution.py:406
  115.6 2.4 %shard_map.99 = (bf16[384,256]{1,0:T(8,128)(2,1)S(1)}, f32[2,384]{1,0:T(2,128)S(1)}) custom-call(s32[19]{0:T(128)S(1)} %get-tuple-element.21.flags_ref, bf16[416,2048]{1,0:T(8,128)(2,1)S(1)} %get-tuple-element.27.normed_ref, f32[416,128]{1,0:T(8,128)S(1)} %get-tuple-element.23.dist_ref, f32[31,2,256]{2,1,0:T(2,128)S(1)} %bitcast.14, ...), custom_call_target="tpu_custom_call" | custom-call | tf_op jit(solution)/shard_map/pallas_call | solution.py:516
  118.0 1.7 %collective-permute-start.43 = (bf16[384,256]{1,0:T(8,128)(2,1)S(1)}, bf16[384,256]{1,0:T(8,128)(2,1)S(1)}, u32[]{:S(2)}, u32[]{:S(2)}) collective-permute-start(bf16[384,256]{1,0:T(8,128)(2,1)S(1)} %get-tuple-element.30.refs_8_), channel_id=1, source_target_pairs={{0,2},{1,3},{2,0},{3,1},{4,6},{5,7},{6,4},{7,5},{8,10},{9,11},{10,... | collective-permute-start | bytes 589832 | tf_op jit(solution)/shard_map/ppermute | solution.py:447
  120.1 1.6 %collective-permute-start.41 = (f32[2,384]{1,0:T(2,128)S(1)}, f32[2,384]{1,0:T(2,128)S(1)}, u32[]{:S(2)}, u32[]{:S(2)}) collective-permute-start(f32[2,384]{1,0:T(2,128)S(1)} %get-tuple-element.29.refs_4_), channel_id=1, source_target_pairs={{0,2},{1,3},{2,0},{3,1},{4,6},{5,7},{6,4},{7,5},{8,10},{9,11},{10,... | collective-permute-start | bytes 9224 | tf_op jit(solution)/shard_map/ppermute | solution.py:534
  122.0 3.3 %collective-permute-done.41.refs_6_ = f32[2,384]{1,0:T(2,128)S(1)} collective-permute-done((f32[2,384]{1,0:T(2,128)S(1)}, f32[2,384]{1,0:T(2,128)S(1)}, u32[]{:S(2)}, u32[]{:S(2)}) %collective-permute-start.41) | collective-permute-done | bytes 3104 | tf_op jit(solution)/shard_map/ppermute | solution.py:534
  (101 shorter events, 34.6 us)
Async XLA Ops:
  2.4 10.2 %collective-permute-start.4 = (bf16[2,256,256]{2,1,0:T(8,128)(2,1)S(1)}, bf16[2,256,256]{2,1,0:T(8,128)(2,1)S(1)}, u32[]{:S(2)}, u32[]{:S(2)}) collective-permute-start(bf16[2,256,256]{2,1,0:T(8,128)(2,1)S(1)} %shard_map.93.refs_0_), channel_id=1, source_target_pairs={{0,8},{8,16},{16,24},{24,28},{28,20},{20,12},{12,4},{4,0},{1,9},{9... | collective-permute-start | bytes 786440 | tf_op jit(solution)/shard_map/ppermute | solution.py:405
  5.5 21.9 %collective-permute-start.5 = (bf16[2,256,256]{2,1,0:T(8,128)(2,1)S(1)}, bf16[2,256,256]{2,1,0:T(8,128)(2,1)S(1)}, u32[]{:S(2)}, u32[]{:S(2)}) collective-permute-start(bf16[2,256,256]{2,1,0:T(8,128)(2,1)S(1)} %shard_map.93.refs_0_), channel_id=1, source_target_pairs={{8,0},{16,8},{24,16},{28,24},{20,28},{12,20},{4,12},{0,4},{9,1},{1... | collective-permute-start | bytes 786440 | tf_op jit(solution)/shard_map/ppermute | solution.py:406
  5.5 25.0 %collective-permute-start.17 = (bf16[2,256,256]{2,1,0:T(8,128)(2,1)S(1)}, bf16[2,256,256]{2,1,0:T(8,128)(2,1)S(1)}, u32[]{:S(2)}, u32[]{:S(2)}) collective-permute-start(bf16[2,256,256]{2,1,0:T(8,128)(2,1)S(1)} %copy-done.1), channel_id=1, source_target_pairs={{0,8},{8,16},{16,24},{24,28},{28,20},{20,12},{12,4},{4,0},{1,9},{9... | collective-permute-start | bytes 786440 | tf_op jit(solution)/shard_map/ppermute | solution.py:405
  12.6 18.4 %collective-permute-start.6 = (bf16[2,256,256]{2,1,0:T(8,128)(2,1)S(1)}, bf16[2,256,256]{2,1,0:T(8,128)(2,1)S(1)}, u32[]{:S(2)}, u32[]{:S(2)}) collective-permute-start(bf16[2,256,256]{2,1,0:T(8,128)(2,1)S(1)} %collective-permute-done.4.refs_1_), channel_id=1, source_target_pairs={{0,8},{8,16},{16,24},{24,28},{28,20},{20,12},{12,4},{4,0},{1,9},{9... | collective-permute-start | bytes 786440 | tf_op jit(solution)/shard_map/ppermute | solution.py:405
  15.2 13.8 %collective-permute-start = (bf16[32,2176]{1,0:T(8,128)(2,1)S(1)}, bf16[32,2176]{1,0:T(8,128)(2,1)S(1)}, u32[]{:S(2)}, u32[]{:S(2)}) collective-permute-start(bf16[32,2176]{1,0:T(8,128)(2,1)S(1)} %get-tuple-element.19), channel_id=1, source_target_pairs={{0,4},{4,8},{8,12},{12,16},{16,20},{20,24},{24,28},{1,5},{5,9},{9,... | collective-permute-start | bytes 417800 | tf_op jit(solution)/shard_map/ppermute | solution.py:476
  24.3 9.8 %collective-permute-start.19 = (bf16[2,256,256]{2,1,0:T(8,128)(2,1)S(1)}, bf16[2,256,256]{2,1,0:T(8,128)(2,1)S(1)}, u32[]{:S(2)}, u32[]{:S(2)}) collective-permute-start(bf16[2,256,256]{2,1,0:T(8,128)(2,1)S(1)} %copy-done.1), channel_id=1, source_target_pairs={{8,0},{16,8},{24,16},{28,24},{20,28},{12,20},{4,12},{0,4},{9,1},{1... | collective-permute-start | bytes 786440 | tf_op jit(solution)/shard_map/ppermute | solution.py:406
  27.4 12.3 %collective-permute-start.7 = (bf16[2,256,256]{2,1,0:T(8,128)(2,1)S(1)}, bf16[2,256,256]{2,1,0:T(8,128)(2,1)S(1)}, u32[]{:S(2)}, u32[]{:S(2)}) collective-permute-start(bf16[2,256,256]{2,1,0:T(8,128)(2,1)S(1)} %collective-permute-done.5.refs_2_), channel_id=1, source_target_pairs={{8,0},{16,8},{24,16},{28,24},{20,28},{12,20},{4,12},{0,4},{9,1},{1... | collective-permute-start | bytes 786440 | tf_op jit(solution)/shard_map/ppermute | solution.py:406
  29.0 13.2 %collective-permute-start.16 = (bf16[2,256,256]{2,1,0:T(8,128)(2,1)S(1)}, bf16[2,256,256]{2,1,0:T(8,128)(2,1)S(1)}, u32[]{:S(2)}, u32[]{:S(2)}) collective-permute-start(bf16[2,256,256]{2,1,0:T(8,128)(2,1)S(1)} %copy-done.1), channel_id=1, source_target_pairs={{0,2},{1,3},{2,0},{3,1},{4,6},{5,7},{6,4},{7,5},{8,10},{9,11},{10,... | collective-permute-start | bytes 786440 | tf_op jit(solution)/shard_map/ppermute | solution.py:447
  30.6 13.2 %collective-permute-start.21 = (bf16[2,256,256]{2,1,0:T(8,128)(2,1)S(1)}, bf16[2,256,256]{2,1,0:T(8,128)(2,1)S(1)}, u32[]{:S(2)}, u32[]{:S(2)}) collective-permute-start(bf16[2,256,256]{2,1,0:T(8,128)(2,1)S(1)} %collective-permute-done.17.refs_12_), channel_id=1, source_target_pairs={{0,8},{8,16},{16,24},{24,28},{28,20},{20,12},{12,4},{4,0},{1,9},{9... | collective-permute-start | bytes 786440 | tf_op jit(solution)/shard_map/ppermute | solution.py:405
  31.0 13.3 %collective-permute-start.8 = (bf16[2,256,256]{2,1,0:T(8,128)(2,1)S(1)}, bf16[2,256,256]{2,1,0:T(8,128)(2,1)S(1)}, u32[]{:S(2)}, u32[]{:S(2)}) collective-permute-start(bf16[2,256,256]{2,1,0:T(8,128)(2,1)S(1)} %collective-permute-done.6.refs_3_), channel_id=1, source_target_pairs={{0,8},{8,16},{16,24},{24,28},{28,20},{20,12},{12,4},{4,0},{1,9},{9... | collective-permute-start | bytes 786440 | tf_op jit(solution)/shard_map/ppermute | solution.py:405
  34.1 10.2 %collective-permute-start.23 = (bf16[2,256,256]{2,1,0:T(8,128)(2,1)S(1)}, bf16[2,256,256]{2,1,0:T(8,128)(2,1)S(1)}, u32[]{:S(2)}, u32[]{:S(2)}) collective-permute-start(bf16[2,256,256]{2,1,0:T(8,128)(2,1)S(1)} %collective-permute-done.19.refs_14_), channel_id=1, source_target_pairs={{8,0},{16,8},{24,16},{28,24},{20,28},{12,20},{4,12},{0,4},{9,1},{1... | collective-permute-start | bytes 786440 | tf_op jit(solution)/shard_map/ppermute | solution.py:406
  42.2 8.0 %collective-permute-start.18 = (bf16[2,256,256]{2,1,0:T(8,128)(2,1)S(1)}, bf16[2,256,256]{2,1,0:T(8,128)(2,1)S(1)}, u32[]{:S(2)}, u32[]{:S(2)}) collective-permute-start(bf16[2,256,256]{2,1,0:T(8,128)(2,1)S(1)} %collective-permute-done.17.refs_12_), channel_id=1, source_target_pairs={{0,2},{1,3},{2,0},{3,1},{4,6},{5,7},{6,4},{7,5},{8,10},{9,11},{10,... | collective-permute-start | bytes 786440 | tf_op jit(solution)/shard_map/ppermute | solution.py:447
  43.8 9.8 %collective-permute-start.20 = (bf16[2,256,256]{2,1,0:T(8,128)(2,1)S(1)}, bf16[2,256,256]{2,1,0:T(8,128)(2,1)S(1)}, u32[]{:S(2)}, u32[]{:S(2)}) collective-permute-start(bf16[2,256,256]{2,1,0:T(8,128)(2,1)S(1)} %collective-permute-done.19.refs_14_), channel_id=1, source_target_pairs={{0,2},{1,3},{2,0},{3,1},{4,6},{5,7},{6,4},{7,5},{8,10},{9,11},{10,... | collective-permute-start | bytes 786440 | tf_op jit(solution)/shard_map/ppermute | solution.py:447
  44.3 9.3 %collective-permute-start.25 = (bf16[2,256,256]{2,1,0:T(8,128)(2,1)S(1)}, bf16[2,256,256]{2,1,0:T(8,128)(2,1)S(1)}, u32[]{:S(2)}, u32[]{:S(2)}) collective-permute-start(bf16[2,256,256]{2,1,0:T(8,128)(2,1)S(1)} %collective-permute-done.21.refs_16_), channel_id=1, source_target_pairs={{0,8},{8,16},{16,24},{24,28},{28,20},{20,12},{12,4},{4,0},{1,9},{9... | collective-permute-start | bytes 786440 | tf_op jit(solution)/shard_map/ppermute | solution.py:405
  46.1 9.5 %collective-permute-start.27 = (bf16[2,256,256]{2,1,0:T(8,128)(2,1)S(1)}, bf16[2,256,256]{2,1,0:T(8,128)(2,1)S(1)}, u32[]{:S(2)}, u32[]{:S(2)}) collective-permute-start(bf16[2,256,256]{2,1,0:T(8,128)(2,1)S(1)} %collective-permute-done.23.refs_18_.refs_1_), channel_id=1, source_target_pairs={{8,0},{16,8},{24,16},{28,24},{20,28},{12,20},{4,12},{0,4},{9,1},{1... | collective-permute-start | bytes 786440 | tf_op jit(solution)/shard_map/ppermute | solution.py:406
  48.6 17.4 %collective-permute-start.22 = (bf16[2,256,256]{2,1,0:T(8,128)(2,1)S(1)}, bf16[2,256,256]{2,1,0:T(8,128)(2,1)S(1)}, u32[]{:S(2)}, u32[]{:S(2)}) collective-permute-start(bf16[2,256,256]{2,1,0:T(8,128)(2,1)S(1)} %collective-permute-done.21.refs_16_), channel_id=1, source_target_pairs={{0,2},{1,3},{2,0},{3,1},{4,6},{5,7},{6,4},{7,5},{8,10},{9,11},{10,... | collective-permute-start | bytes 786440 | tf_op jit(solution)/shard_map/ppermute | solution.py:447
  50.2 17.9 %collective-permute-start.24 = (bf16[2,256,256]{2,1,0:T(8,128)(2,1)S(1)}, bf16[2,256,256]{2,1,0:T(8,128)(2,1)S(1)}, u32[]{:S(2)}, u32[]{:S(2)}) collective-permute-start(bf16[2,256,256]{2,1,0:T(8,128)(2,1)S(1)} %collective-permute-done.23.refs_18_.refs_1_), channel_id=1, source_target_pairs={{0,2},{1,3},{2,0},{3,1},{4,6},{5,7},{6,4},{7,5},{8,10},{9,11},{10,... | collective-permute-start | bytes 786440 | tf_op jit(solution)/shard_map/ppermute | solution.py:447
  55.6 12.0 %collective-permute-start.29 = (bf16[256,256]{1,0:T(8,128)(2,1)S(1)}, bf16[256,256]{1,0:T(8,128)(2,1)S(1)}, u32[]{:S(2)}, u32[]{:S(2)}) collective-permute-start(bf16[256,256]{1,0:T(8,128)(2,1)S(1)} %slice_bitcast_fusion.3), channel_id=1, source_target_pairs={{0,8},{8,16},{16,24},{24,28},{28,20},{20,12},{12,4},{4,0},{1,9},{9... | collective-permute-start | bytes 393224 | tf_op jit(solution)/shard_map/ppermute | solution.py:405
  58.5 25.9 %collective-permute-start.26 = (bf16[2,256,256]{2,1,0:T(8,128)(2,1)S(1)}, bf16[2,256,256]{2,1,0:T(8,128)(2,1)S(1)}, u32[]{:S(2)}, u32[]{:S(2)}) collective-permute-start(bf16[2,256,256]{2,1,0:T(8,128)(2,1)S(1)} %collective-permute-done.25.refs_20_.refs_3_), channel_id=1, source_target_pairs={{0,2},{1,3},{2,0},{3,1},{4,6},{5,7},{6,4},{7,5},{8,10},{9,11},{10,... | collective-permute-start | bytes 786440 | tf_op jit(solution)/shard_map/ppermute | solution.py:447
  60.0 24.4 %collective-permute-start.28 = (bf16[2,256,256]{2,1,0:T(8,128)(2,1)S(1)}, bf16[2,256,256]{2,1,0:T(8,128)(2,1)S(1)}, u32[]{:S(2)}, u32[]{:S(2)}) collective-permute-start(bf16[2,256,256]{2,1,0:T(8,128)(2,1)S(1)} %collective-permute-done.27.refs_22_.refs_5_), channel_id=1, source_target_pairs={{0,2},{1,3},{2,0},{3,1},{4,6},{5,7},{6,4},{7,5},{8,10},{9,11},{10,... | collective-permute-start | bytes 786440 | tf_op jit(solution)/shard_map/ppermute | solution.py:447
  66.1 18.3 %collective-permute-start.15 = (bf16[416,256]{1,0:T(8,128)(2,1)S(1)}, bf16[416,256]{1,0:T(8,128)(2,1)S(1)}, u32[]{:S(2)}, u32[]{:S(2)}) collective-permute-start(bf16[416,256]{1,0:T(8,128)(2,1)S(1)} %get-tuple-element.25.refs_8_), channel_id=1, source_target_pairs={{0,2},{1,3},{2,0},{3,1},{4,6},{5,7},{6,4},{7,5},{8,10},{9,11},{10,... | collective-permute-start | bytes 638984 | tf_op jit(solution)/shard_map/ppermute | solution.py:447
  67.6 16.8 %collective-permute-start.30 = (bf16[256,256]{1,0:T(8,128)(2,1)S(1)}, bf16[256,256]{1,0:T(8,128)(2,1)S(1)}, u32[]{:S(2)}, u32[]{:S(2)}) collective-permute-start(bf16[256,256]{1,0:T(8,128)(2,1)S(1)} %collective-permute-done.29.refs_24_), channel_id=1, source_target_pairs={{0,2},{1,3},{2,0},{3,1},{4,6},{5,7},{6,4},{7,5},{8,10},{9,11},{10,... | collective-permute-start | bytes 393224 | tf_op jit(solution)/shard_map/ppermute | solution.py:447
  69.3 12.0 %collective-permute-start.13 = (f32[2,512]{1,0:T(2,128)S(1)}, f32[2,512]{1,0:T(2,128)S(1)}, u32[]{:S(2)}, u32[]{:S(2)}) collective-permute-start(f32[2,512]{1,0:T(2,128)S(1)} %get-tuple-element.24.refs_4_), channel_id=1, source_target_pairs={{0,2},{1,3},{2,0},{3,1},{4,6},{5,7},{6,4},{7,5},{8,10},{9,11},{10,... | collective-permute-start | bytes 12296 | tf_op jit(solution)/shard_map/ppermute | solution.py:534
  85.9 27.4 %collective-permute-start.31 = (bf16[416,2048]{1,0:T(8,128)(2,1)S(1)}, bf16[416,2048]{1,0:T(8,128)(2,1)S(1)}, u32[]{:S(2)}, u32[]{:S(2)}) collective-permute-start(bf16[416,2048]{1,0:T(8,128)(2,1)S(1)} %shard_map.96.refs_3_), channel_id=1, source_target_pairs={{0,1},{1,0},{2,3},{3,2},{4,5},{5,4},{6,7},{7,6},{8,9},{9,8},{10,11... | collective-permute-start | bytes 5111816 | tf_op jit(solution)/shard_map/ppermute | solution.py:566
  86.1 8.6 %collective-permute-start.32 = (bf16[2,256,256]{2,1,0:T(8,128)(2,1)S(1)}, bf16[2,256,256]{2,1,0:T(8,128)(2,1)S(1)}, u32[]{:S(2)}, u32[]{:S(2)}) collective-permute-start(bf16[2,256,256]{2,1,0:T(8,128)(2,1)S(1)} %get-tuple-element.28.refs_0_), channel_id=1, source_target_pairs={{0,8},{8,16},{16,24},{24,28},{28,20},{20,12},{12,4},{4,0},{1,9},{9... | collective-permute-start | bytes 786440 | tf_op jit(solution)/shard_map/ppermute | solution.py:405
  86.1 8.9 %collective-permute-start.33 = (bf16[2,256,256]{2,1,0:T(8,128)(2,1)S(1)}, bf16[2,256,256]{2,1,0:T(8,128)(2,1)S(1)}, u32[]{:S(2)}, u32[]{:S(2)}) collective-permute-start(bf16[2,256,256]{2,1,0:T(8,128)(2,1)S(1)} %get-tuple-element.28.refs_0_), channel_id=1, source_target_pairs={{8,0},{16,8},{24,16},{28,24},{20,28},{12,20},{4,12},{0,4},{9,1},{1... | collective-permute-start | bytes 786440 | tf_op jit(solution)/shard_map/ppermute | solution.py:406
  94.7 7.8 %collective-permute-start.34 = (bf16[2,256,256]{2,1,0:T(8,128)(2,1)S(1)}, bf16[2,256,256]{2,1,0:T(8,128)(2,1)S(1)}, u32[]{:S(2)}, u32[]{:S(2)}) collective-permute-start(bf16[2,256,256]{2,1,0:T(8,128)(2,1)S(1)} %collective-permute-done.32.refs_1_), channel_id=1, source_target_pairs={{0,8},{8,16},{16,24},{24,28},{28,20},{20,12},{12,4},{4,0},{1,9},{9... | collective-permute-start | bytes 786440 | tf_op jit(solution)/shard_map/ppermute | solution.py:405
  95.0 8.0 %collective-permute-start.35 = (bf16[2,256,256]{2,1,0:T(8,128)(2,1)S(1)}, bf16[2,256,256]{2,1,0:T(8,128)(2,1)S(1)}, u32[]{:S(2)}, u32[]{:S(2)}) collective-permute-start(bf16[2,256,256]{2,1,0:T(8,128)(2,1)S(1)} %collective-permute-done.33.refs_2_), channel_id=1, source_target_pairs={{8,0},{16,8},{24,16},{28,24},{20,28},{12,20},{4,12},{0,4},{9,1},{1... | collective-permute-start | bytes 786440 | tf_op jit(solution)/shard_map/ppermute | solution.py:406
  102.4 6.9 %collective-permute-start.36 = (bf16[2,256,256]{2,1,0:T(8,128)(2,1)S(1)}, bf16[2,256,256]{2,1,0:T(8,128)(2,1)S(1)}, u32[]{:S(2)}, u32[]{:S(2)}) collective-permute-start(bf16[2,256,256]{2,1,0:T(8,128)(2,1)S(1)} %collective-permute-done.34.refs_3_), channel_id=1, source_target_pairs={{0,8},{8,16},{16,24},{24,28},{28,20},{20,12},{12,4},{4,0},{1,9},{9... | collective-permute-start | bytes 786440 | tf_op jit(solution)/shard_map/ppermute | solution.py:405
  103.0 7.2 %collective-permute-start.37 = (bf16[2,256,256]{2,1,0:T(8,128)(2,1)S(1)}, bf16[2,256,256]{2,1,0:T(8,128)(2,1)S(1)}, u32[]{:S(2)}, u32[]{:S(2)}) collective-permute-start(bf16[2,256,256]{2,1,0:T(8,128)(2,1)S(1)} %collective-permute-done.35.refs_4_), channel_id=1, source_target_pairs={{8,0},{16,8},{24,16},{28,24},{20,28},{12,20},{4,12},{0,4},{9,1},{1... | collective-permute-start | bytes 786440 | tf_op jit(solution)/shard_map/ppermute | solution.py:406
  111.5 8.2 %collective-permute-start.44 = (bf16[256,256]{1,0:T(8,128)(2,1)S(1)}, bf16[256,256]{1,0:T(8,128)(2,1)S(1)}, u32[]{:S(2)}, u32[]{:S(2)}) collective-permute-start(bf16[256,256]{1,0:T(8,128)(2,1)S(1)} %slice_bitcast_fusion), channel_id=1, source_target_pairs={{8,0},{16,8},{24,16},{28,24},{20,28},{12,20},{4,12},{0,4},{9,1},{1... | collective-permute-start | bytes 393224 | tf_op jit(solution)/shard_map/ppermute | solution.py:406
  118.0 7.2 %collective-permute-start.43 = (bf16[384,256]{1,0:T(8,128)(2,1)S(1)}, bf16[384,256]{1,0:T(8,128)(2,1)S(1)}, u32[]{:S(2)}, u32[]{:S(2)}) collective-permute-start(bf16[384,256]{1,0:T(8,128)(2,1)S(1)} %get-tuple-element.30.refs_8_), channel_id=1, source_target_pairs={{0,2},{1,3},{2,0},{3,1},{4,6},{5,7},{6,4},{7,5},{8,10},{9,11},{10,... | collective-permute-start | bytes 589832 | tf_op jit(solution)/shard_map/ppermute | solution.py:447
  (25 other events, 196.4 us)
